TPU v7x, 32 devices: a whole 2x2x4 slice. The times are simulated.
32 devices in a mesh: kv: 8 (over z, y), tp: 4 (over x, core).
Axes of the slice: x: 2, y: 2, z: 4, core: 2. Of those that a mesh axis runs over, the one named last changes fastest.
Arguments:
- tokens: bfloat16 [2048, 4096], P('kv'), may hold values from -6 to 6
- norm_gain: float32 [4096], replicated, may hold values from 0.1 to 1.9
- w_query: bfloat16 [4096, 2048], P('kv', 'tp'), may hold values from -0.09375 to 0.09375
- w_forget: bfloat16 [4096, 2048], P('kv', 'tp'), may hold values from -0.09375 to 0.09375
- w_value: bfloat16 [4096, 2048], P('kv', 'tp'), may hold values from -0.09375 to 0.09375
- w_gate: bfloat16 [4096, 2048], P('kv', 'tp'), may hold values from -0.09375 to 0.09375
- lower_bound: float32 [2048], P('tp'), may hold values from 0 to 0.9
- head_gain: float32 [2048], P('tp'), may hold values from 0.1 to 1.9
- w_out: bfloat16 [2048, 4096], P('kv', 'tp'), may hold values from -0.125 to 0.125
- state: float32 [512, 16, 128, 128], P('kv', 'tp'), may hold values from -4 to 4
- prev_forget: bfloat16 [512, 4, 2048], P('kv', None, 'tp'), may hold values from -8 to 8
- prev_value: bfloat16 [512, 4, 2048], P('kv', None, 'tp'), may hold values from -6 to 6
- accepted: int32 [512], P('kv'), may hold values from 0 to 4
Outputs:
- mixed: bfloat16 [2048, 4096], P('kv', 'tp')
- taken_state: float32 [512, 16, 128, 128], P('kv', 'tp')
All inputs are finite; a program needn't handle non-finite values.
Results may differ from a plain program's by a relative error of at most 0.015.
Values may be sent and summed in bfloat16 or wider, within the bound.
No kernel may reach another device: no remote copies, remote signals or barrier semaphores. Data moves between devices by JAX's collectives and lax.ppermute only.
A program may use at most 128 MiB of HBM per device.

v0:
```python
import jax
import jax.numpy as jnp
import numpy as np
from jax import lax
from jax.experimental import pallas as pl
from jax.experimental.pallas import tpu as pltpu
from jax.sharding import PartitionSpec as P


EPSILON = 1e-06
F32 = jnp.float32
BF16 = jnp.bfloat16
VMEM = pl.BlockSpec(memory_space=pltpu.VMEM)
SMEM = pl.BlockSpec(memory_space=pltpu.SMEM)


def forget_of(pre_act, bounds):
    return bounds + (1.0 - bounds) * jax.nn.sigmoid(pre_act)


def norm_kernel(tokens, gain, own, *rest, ring, inner, share):
    mine, scratch = rest[:-1], rest[-1]
    rows, width = tokens.shape
    step = 16
    block = own.shape[-1]
    part = rows // share
    chunk = min(width, 512)

    def one(i, carry):
        here = pl.ds(pl.multiple_of(i * step, step), step)
        total = jnp.zeros((step, 128), F32)
        for at in range(0, width, chunk):
            x = tokens[here, at : at + chunk].astype(F32)
            x = x * x
            for k in range(0, chunk, 128):
                total = total + x[:, k : k + 128]
        scale = lax.rsqrt(jnp.sum(total, axis=-1, keepdims=True) / width + EPSILON)
        for at in range(0, width, chunk):
            x = tokens[here, at : at + chunk].astype(F32)
            scratch[here, at : at + chunk] = (x * scale * gain[:, at : at + chunk]).astype(BF16)
        return carry

    lax.fori_loop(0, rows // step, one, 0)
    me, lane = lax.axis_index("kv"), lax.axis_index("tp")
    group, member = lax.div(me, inner), lax.rem(me, inner)
    here = pl.ds(pl.multiple_of(lax.rem(lane, share) * part, part), part)
    for r in range(ring):
        owner = jnp.bitwise_xor(group, r)
        for turn in range(inner):
            column = owner * inner + lax.rem(member + turn, inner)
            cols = pl.ds(pl.multiple_of(column * block, block), block)
            if r == 0:
                own[turn] = scratch[:, cols]
            else:
                mine[r - 1][turn] = scratch[here, cols]


def project_kernel(own, *rest, ring, inner, share):
    others = rest[: (ring - 1) * share]
    weights = rest[(ring - 1) * share : (ring - 1) * share + inner]
    outs, lhs = rest[(ring - 1) * share + inner : -1], rest[-1]
    rows, block = own.shape[1], own.shape[2]
    part = rows // share
    lane = lax.rem(lax.axis_index("tp"), share)
    for turn in range(inner):
        cols = slice(turn * block, (turn + 1) * block)
        lhs[0:rows, cols] = own[turn]
        for r in range(ring - 1):
            for other in range(share):
                at = (r + 1) * rows + jnp.bitwise_xor(lane, other) * part
                lhs[pl.ds(pl.multiple_of(at, part), part), cols] = others[r * share + other][turn]
    level = 0
    for r in range(ring):
        here = slice(r * rows, (r + 1) * rows)
        total = None
        for turn in range(inner):
            product = jnp.dot(
                lhs[here, turn * block : (turn + 1) * block],
                weights[turn][...],
                preferred_element_type=F32,
            )
            total = product if total is None else total + product
        if r == 0:
            outs[0][...] = total
        else:
            level = r.bit_length()
            outs[level][r - (1 << (level - 1))] = total.astype(BF16)


def position_of(shape, proposals):
    return lax.rem(lax.broadcasted_iota(jnp.int32, shape, 0), proposals)


def taken_kernel(accepted, state, forget, values, bounds, taken, rounded, *, proposals):
    seqs, heads, keys, vals = state.shape
    rows = seqs * proposals
    first = pl.program_id(0) * seqs
    position = position_of((rows, keys), proposals)
    owner = lax.broadcasted_iota(jnp.int32, (rows, keys), 0) // proposals
    count = jnp.zeros((rows, keys), jnp.int32)
    for seq in range(seqs):
        count = jnp.where(owner == seq, accepted[first + seq], count)
    kept = position < count
    for head in range(heads):
        cols = slice(head * keys, (head + 1) * keys)
        gate = forget_of(forget[:, cols].astype(F32), bounds[:, cols])
        decay = jnp.where(kept, gate, 1.0)
        after = jnp.ones_like(decay)
        for ahead in range(1, proposals):
            moved = pltpu.roll(decay, rows - ahead, axis=0)
            after = after * jnp.where(position < proposals - ahead, moved, 1.0)
        decay_columns = (decay * after).T
        weight = (jnp.where(kept, 1.0 - gate, 0.0) * after).T
        high = weight.astype(BF16)
        low = (weight - high.astype(F32)).astype(BF16)
        new = values[:, head * vals : (head + 1) * vals]
        spread = jnp.concatenate(
            [jnp.where(owner == seq, new, jnp.zeros_like(new)) for seq in range(seqs)], axis=1
        )
        added = jnp.dot(
            jnp.concatenate([high, low], axis=1),
            jnp.concatenate([spread, spread], axis=0),
            preferred_element_type=F32,
        )
        for seq in range(seqs):
            at = seq * proposals
            total = (
                decay_columns[:, at : at + 1] * state[seq, head] + added[:, seq * vals : (seq + 1) * vals]
            )
            taken[seq, head] = total
            rounded[seq, head] = total.astype(BF16)


def recur_kernel(*refs, parts, proposals):
    q_parts, f_parts, v_parts = refs[:parts], refs[parts : 2 * parts], refs[2 * parts : 3 * parts]
    taken, bounds, gain, out = refs[3 * parts :]
    seqs, heads, keys, vals = taken.shape
    rows = seqs * proposals
    position = position_of((rows, keys), proposals)
    group = 4
    tile = group * proposals
    tile_seq = lax.broadcasted_iota(jnp.int32, (tile, keys), 0) // proposals

    def total_of(pieces, cols):
        total = pieces[0][:, cols]
        for piece in pieces[1:]:
            total = total + piece[0, :, cols].astype(F32)
        return total

    for head in range(heads):
        cols = slice(head * keys, (head + 1) * keys)
        query = total_of(q_parts, cols) * keys ** (-0.5)
        gate = forget_of(total_of(f_parts, cols), bounds[:, cols])
        value = total_of(v_parts, cols)
        key = 1.0 - gate
        through = query
        result = jnp.sum(query * key, axis=-1, keepdims=True) * value
        for lag in range(1, proposals):
            through = through * jnp.where(
                position >= lag, pltpu.roll(gate, lag - 1, axis=0) if lag > 1 else gate, 0.0
            )
            score = jnp.sum(through * pltpu.roll(key, lag, axis=0), axis=-1, keepdims=True)
            result = result + score * pltpu.roll(value, lag, axis=0)
        grown = gate
        for lag in range(1, proposals):
            grown = grown * jnp.where(position >= lag, pltpu.roll(gate, lag, axis=0), 1.0)
        reach = (query * grown).astype(BF16)
        pieces = []
        for at in range(0, seqs, group):
            part = reach[at * proposals : (at + group) * proposals, :]
            lhs = jnp.concatenate(
                [jnp.where(tile_seq == s, part, jnp.zeros_like(part)) for s in range(group)], axis=1
            )
            here = taken[at : at + group, head].reshape(group * keys, vals)
            pieces.append(jnp.dot(lhs, here, preferred_element_type=F32))
        result = result + jnp.concatenate(pieces, axis=0)
        scale = lax.rsqrt(jnp.mean(result * result, axis=-1, keepdims=True) + EPSILON)
        out[:, cols] = result * scale * gain[:, cols]


def mix_kernel(order, *refs, lanes, ids, inner):
    heads, weights = refs[:lanes], refs[lanes:-2]
    out, lhs = refs[-2:]
    height = weights[0].shape[1]
    per = heads[0].shape[1] // height
    mine = lax.axis_index("tp")
    me = lax.axis_index("kv")
    group, member = lax.div(me, inner), lax.rem(me, inner)
    for head, other in zip(heads, ids):
        lane = jnp.bitwise_xor(mine, other)
        for k in range(per):
            lhs[lane * per + k] = head[:, k * height : (k + 1) * height]
    total = None
    slot = 0
    for at in range(0, len(weights), inner):
        for k in range(weights[at].shape[0]):
            for turn in range(inner):
                place = order[group, slot] * inner + lax.rem(member + turn, inner)
                product = jnp.dot(lhs[place], weights[at + turn][k], preferred_element_type=F32)
                total = product if total is None else total + product
            slot += 1
    out[...] = total.astype(out.dtype)


def on_device(
    tokens,
    norm_gain,
    w_query,
    w_forget,
    w_value,
    w_gate,
    lower_bound,
    head_gain,
    w_out,
    state,
    prev_forget,
    prev_value,
    accepted,
    *,
    kv,
    tp,
):
    seqs, heads, keys, vals = state.shape
    proposals = prev_forget.shape[1]
    rows = tokens.shape[0]
    width = heads * keys
    inner, ring, share = cut_of(kv, tp)

    def groups(pairs):
        return [(a * inner + m, b * inner + m) for a, b in pairs for m in range(inner)]

    def around(turn):
        return [(g * inner + (m + turn) % inner, g * inner + m) for g in range(ring) for m in range(inner)]

    def mirrored(size, start, stop):
        pairs = []
        for base in range(0, ring, 2 * size):
            last = base + 2 * size - 1
            pairs += [(base + start, base + stop), (last - start, last - stop)]
        return groups(pairs)

    def swap(value, bit):
        return lax.ppermute(value, "tp", [(t, t ^ bit) for t in range(tp)])

    sets = []
    for weight in (w_forget, w_value, w_query, w_gate):
        sets.append([weight] + [lax.ppermute(weight, "kv", around(t)) for t in range(1, inner)])

    block = w_query.shape[0]
    part = rows // share
    shapes = [jax.ShapeDtypeStruct((inner, rows, block), BF16)]
    shapes += [jax.ShapeDtypeStruct((inner, part, block), BF16)] * (ring - 1)
    normed = pl.pallas_call(
        lambda *refs: norm_kernel(*refs, ring=ring, inner=inner, share=share),
        out_shape=shapes,
        in_specs=[VMEM, VMEM],
        out_specs=[VMEM] * ring,
        scratch_shapes=[pltpu.VMEM(tokens.shape, BF16)],
        name="norm",
    )(tokens, norm_gain.reshape(1, -1))
    own, mine = normed[0], normed[1:]
    others = []
    for r in range(1, ring):
        got = lax.ppermute(mine[r - 1], "kv", groups([(g, g ^ r) for g in range(ring)]))
        others.append(got)
        for bit in range(1, share):
            others.append(swap(got, bit))

    bounds = lower_bound.reshape(1, width)
    some = 8 if seqs % 8 == 0 else seqs
    some_rows = some * proposals
    state_spec = pl.BlockSpec((some, heads, keys, vals), lambda i: (i, 0, 0, 0))
    row_spec = pl.BlockSpec((some_rows, width), lambda i: (i, 0))
    one_spec = pl.BlockSpec((1, width), lambda i: (0, 0))
    taken, rounded = pl.pallas_call(
        lambda *refs: taken_kernel(*refs, proposals=proposals),
        out_shape=[jax.ShapeDtypeStruct(state.shape, F32), jax.ShapeDtypeStruct(state.shape, BF16)],
        grid=(seqs // some,),
        in_specs=[SMEM, state_spec, row_spec, row_spec, one_spec],
        out_specs=[state_spec, state_spec],
        name="taken",
    )(accepted, state, prev_forget.reshape(rows, width), prev_value.reshape(rows, width), bounds)

    def added(a, b):
        return (a.astype(F32) + b.astype(F32)).astype(BF16)

    def summed(weights):
        levels = [1 << k for k in range((ring - 1).bit_length())]
        shapes = [jax.ShapeDtypeStruct((rows, width), F32)]
        shapes += [jax.ShapeDtypeStruct((size, rows, width), BF16) for size in levels]
        products = pl.pallas_call(
            lambda *refs: project_kernel(*refs, ring=ring, inner=inner, share=share),
            out_shape=shapes,
            in_specs=[VMEM] * (1 + len(others) + inner),
            out_specs=[VMEM] * len(shapes),
            scratch_shapes=[pltpu.VMEM((ring * rows, inner * block), BF16)],
            name="project",
        )(own, *others, *weights)
        pieces = [(products[0], 0)]
        held = {size: products[1 + k] for k, size in enumerate(levels)}
        for size in reversed(levels):
            out = held[size]
            for hop in range(1, size):
                got = lax.ppermute(out, "kv", mirrored(size, hop - 1, hop))
                turn = (hop - 1) ^ hop
                out = added(out, jnp.stack([got[k ^ turn] for k in range(size)]))
            got = lax.ppermute(out, "kv", mirrored(size, size - 1, size))
            pieces.append((got, size - 1))
            for lower in levels:
                if lower < size:
                    kept = [got[(j ^ (2 * size - 1)) - size] for j in range(lower, 2 * lower)]
                    held[lower] = added(held[lower], jnp.stack(kept))
        return pieces

    forget_parts, value_parts, query_parts, gate_parts = [summed(weights) for weights in sets]

    blocks = []
    cur = w_out[None]
    size, step = 1, 0
    while size < ring:
        got = lax.ppermute(cur, "kv", mirrored(size, size - 1, size))
        step += 1
        total = got
        for hop in range(1, size):
            got = lax.ppermute(got, "kv", mirrored(size, size - hop, size - hop - 1))
            step += 1
            total = total + got
        if size == 1:
            cur = jnp.concatenate([cur, total])
            fresh = cur
        else:
            fresh = total
            if 2 * size < ring:
                cur = jnp.concatenate([cur, total])
        blocks.append(fresh)
        size *= 2
    if ring == 1:
        blocks = [cur]
    weights = []
    for fresh in blocks:
        weights += [fresh] + [lax.ppermute(fresh, "kv", around(t)) for t in range(1, inner)]

    def specs_of(pieces):
        specs, arrays = [], []
        for array, index in pieces:
            arrays.append(array)
            if array.ndim == 2:
                specs.append(row_spec)
            else:
                specs.append(pl.BlockSpec((1, some_rows, width), lambda i, index=index: (index, i, 0)))
        return specs, arrays

    specs, arrays = [], []
    for pieces in (query_parts, forget_parts, value_parts):
        more_specs, more = specs_of(pieces)
        specs += more_specs
        arrays += more
    parts = len(query_parts)
    scaled = pl.pallas_call(
        lambda *refs: recur_kernel(*refs, parts=parts, proposals=proposals),
        out_shape=jax.ShapeDtypeStruct((rows, width), F32),
        grid=(seqs // some,),
        in_specs=specs + [state_spec, one_spec, one_spec],
        out_specs=row_spec,
        name="recur",
    )(*arrays, rounded, bounds, head_gain.reshape(1, width))
    gate = gate_parts[0][0]
    for array, index in gate_parts[1:]:
        gate = gate + array[index].astype(F32)
    head_out = (scaled * jax.nn.silu(gate)).astype(BF16)

    gathered, ids = [head_out], [0]
    bit = tp // 2
    while bit:
        gathered += [swap(piece, bit) for piece in gathered]
        ids += [i ^ bit for i in ids]
        bit //= 2
    table = jnp.asarray(order_of(ring), jnp.int32)
    height = w_out.shape[0]
    mixed = pl.pallas_call(
        lambda *refs: mix_kernel(*refs, lanes=tp, ids=ids, inner=inner),
        out_shape=jax.ShapeDtypeStruct((rows, w_out.shape[1]), BF16),
        in_specs=[SMEM] + [VMEM] * (tp + len(weights)),
        out_specs=VMEM,
        scratch_shapes=[pltpu.VMEM((kv, rows, height), BF16)],
        name="mix",
    )(table, *gathered, *weights)
    return (mixed, taken)


def cut_of(kv, tp):
    inner = 2 if kv % 2 == 0 else 1
    return inner, kv // inner, 2 if tp % 2 == 0 else 1


def order_of(ring):
    order = [[g] for g in range(ring)]
    size = 1
    while size < ring:
        order = [
            order[g] + order[(g // (2 * size)) * 2 * size + (size if g % (2 * size) < size else size - 1)]
            for g in range(ring)
        ]
        size *= 2
    return np.array(order, np.int32)


def solution(mesh):
    kv, tp = mesh.shape["kv"], mesh.shape["tp"]

    def body(*args):
        return on_device(*args, kv=kv, tp=tp)

    return jax.shard_map(
        body,
        mesh=mesh,
        in_specs=(
            P("kv", None),
            P(),
            P("kv", "tp"),
            P("kv", "tp"),
            P("kv", "tp"),
            P("kv", "tp"),
            P("tp"),
            P("tp"),
            P("kv", "tp"),
            P("kv", "tp", None, None),
            P("kv", None, "tp"),
            P("kv", None, "tp"),
            P("kv"),
        ),
        out_specs=(P("kv", "tp"), P("kv", "tp", None, None)),
        check_vma=False,
    )
```

profile of v0, /device:TPU:0, one launch (start us, length us, event | category | flops | bytes accessed | tf_op | source)
XLA Modules:
  0.0 201.9 jit_solution(6912115295480591292)
XLA Ops:
  0.6 5.0 %norm.1 = (bf16[2,256,512]{2,1,0:T(8,128)(2,1)}, bf16[2,128,512]{2,1,0:T(8,128)(2,1)}, bf16[2,128,512]{2,1,0:T(8,128)(2,1)}, bf16[2,128,512]{2,1,0:T(8,128)(2,1)}) custom-call(bf16[256,4096]{1,0:T(8,128)(2,1)} %refs_0_.3, f32[1,4096]{1,0:T(1,128)} %bitcast.14), custom_call_target="tpu_custom_call" | custom-call | tf_op jit(solution)/shard_map/norm/pallas_call | solution.py:253
  5.6 3.0 %collective-permute-start = (bf16[2,128,512]{2,1,0:T(8,128)(2,1)}, bf16[2,128,512]{2,1,0:T(8,128)(2,1)S(1)}, u32[]{:S(2)}, u32[]{:S(2)}) collective-permute-start(bf16[2,128,512]{2,1,0:T(8,128)(2,1)} %get-tuple-element.21), channel_id=1, source_target_pairs={{0,8},{4,12},{8,0},{12,4},{16,24},{20,28},{24,16},{28,20},{1,9},{5... | collective-permute-start | bytes 786440 | tf_op jit(solution)/shard_map/ppermute | solution.py:264
  8.7 2.6 %collective-permute-start.2 = (bf16[2,128,512]{2,1,0:T(8,128)(2,1)}, bf16[2,128,512]{2,1,0:T(8,128)(2,1)S(1)}, u32[]{:S(2)}, u32[]{:S(2)}) collective-permute-start(bf16[2,128,512]{2,1,0:T(8,128)(2,1)} %get-tuple-element.22), channel_id=1, source_target_pairs={{0,16},{4,20},{8,24},{12,28},{16,0},{20,4},{24,8},{28,12},{1,17},{... | collective-permute-start | bytes 786440 | tf_op jit(solution)/shard_map/ppermute | solution.py:264
  11.3 1.7 collective-permute-start.14
  13.0 7.1 %collective-permute-done.refs_1_ = bf16[2,128,512]{2,1,0:T(8,128)(2,1)S(1)} collective-permute-done((bf16[2,128,512]{2,1,0:T(8,128)(2,1)}, bf16[2,128,512]{2,1,0:T(8,128)(2,1)S(1)}, u32[]{:S(2)}, u32[]{:S(2)}) %collective-permute-start) | collective-permute-done | bytes 262176 | tf_op jit(solution)/shard_map/ppermute | solution.py:264
  20.1 10.1 %collective-permute-done.2.refs_3_ = bf16[2,128,512]{2,1,0:T(8,128)(2,1)S(1)} collective-permute-done((bf16[2,128,512]{2,1,0:T(8,128)(2,1)}, bf16[2,128,512]{2,1,0:T(8,128)(2,1)S(1)}, u32[]{:S(2)}, u32[]{:S(2)}) %collective-permute-start.2) | collective-permute-done | bytes 262176 | tf_op jit(solution)/shard_map/ppermute | solution.py:264
  30.7 1.5 collective-permute-start.18
  32.8 1.5 collective-permute-start.6
  34.3 4.3 %collective-permute-start.25 = (bf16[1,256,1024]{2,1,0:T(8,128)(2,1)}, bf16[1,256,1024]{2,1,0:T(8,128)(2,1)S(1)}, u32[]{:S(2)}, u32[]{:S(2)}) collective-permute-start(bf16[1,256,1024]{2,1,0:T(8,128)(2,1)} %bitcast.12), channel_id=1, source_target_pairs={{0,8},{4,12},{8,0},{12,4},{16,24},{20,28},{24,16},{28,20},{1,9},{5... | collective-permute-start | bytes 1572872 | tf_op jit(solution)/shard_map/ppermute | solution.py:321
  38.7 0.7 copy-done.14
  39.4 4.1 %project.6 = (f32[256,512]{1,0:T(8,128)}, bf16[1,256,512]{2,1,0:T(8,128)(2,1)}, bf16[2,256,512]{2,1,0:T(8,128)(2,1)}) custom-call(bf16[2,256,512]{2,1,0:T(8,128)(2,1)} %get-tuple-element.20.refs_0_, bf16[2,128,512]{2,1,0:T(8,128)(2,1)} %copy-done, bf16[2,128,512]{2,1,0:T(8,128)(2,1)} %copy-done.3, bf16[2,128,512]{2,1,0:T(8,128)(2,1)} %copy-done.1, ...), custom_call_target="tpu_custom_call" | custom-call | tf_op jit(solution)/shard_map/project/pallas_call | solution.py:291
  43.5 2.0 collective-permute-start.15
  45.7 0.8 copy-done.15
  46.5 4.0 %project.7 = (f32[256,512]{1,0:T(8,128)}, bf16[1,256,512]{2,1,0:T(8,128)(2,1)}, bf16[2,256,512]{2,1,0:T(8,128)(2,1)}) custom-call(bf16[2,256,512]{2,1,0:T(8,128)(2,1)} %get-tuple-element.20.refs_0_, bf16[2,128,512]{2,1,0:T(8,128)(2,1)} %copy-done, bf16[2,128,512]{2,1,0:T(8,128)(2,1)} %copy-done.3, bf16[2,128,512]{2,1,0:T(8,128)(2,1)} %copy-done.1, ...), custom_call_target="tpu_custom_call" | custom-call | tf_op jit(solution)/shard_map/project/pallas_call | solution.py:291
  50.6 6.4 %collective-permute-start.19 = (bf16[2,256,512]{2,1,0:T(8,128)(2,1)}, bf16[2,256,512]{2,1,0:T(8,128)(2,1)S(1)}, u32[]{:S(2)}, u32[]{:S(2)}) collective-permute-start(bf16[2,256,512]{2,1,0:T(8,128)(2,1)} %get-tuple-element.35), channel_id=1, source_target_pairs={{0,8},{4,12},{24,16},{28,20},{1,9},{5,13},{25,17},{29,21},{2,10},{... | collective-permute-start | bytes 1572872 | tf_op jit(solution)/shard_map/ppermute | solution.py:304
  57.1 4.0 %project.5 = (f32[256,512]{1,0:T(8,128)}, bf16[1,256,512]{2,1,0:T(8,128)(2,1)}, bf16[2,256,512]{2,1,0:T(8,128)(2,1)}) custom-call(bf16[2,256,512]{2,1,0:T(8,128)(2,1)} %get-tuple-element.20.refs_0_, bf16[2,128,512]{2,1,0:T(8,128)(2,1)} %copy-done, bf16[2,128,512]{2,1,0:T(8,128)(2,1)} %copy-done.3, bf16[2,128,512]{2,1,0:T(8,128)(2,1)} %copy-done.1, ...), custom_call_target="tpu_custom_call" | custom-call | tf_op jit(solution)/shard_map/project/pallas_call | solution.py:291
  61.1 7.0 %collective-permute-start.11 = (bf16[2,256,512]{2,1,0:T(8,128)(2,1)}, bf16[2,256,512]{2,1,0:T(8,128)(2,1)}, u32[]{:S(2)}, u32[]{:S(2)}) collective-permute-start(bf16[2,256,512]{2,1,0:T(8,128)(2,1)} %get-tuple-element.28), channel_id=1, source_target_pairs={{0,8},{4,12},{24,16},{28,20},{1,9},{5,13},{25,17},{29,21},{2,10},{... | collective-permute-start | bytes 1572872 | tf_op jit(solution)/shard_map/ppermute | solution.py:304
  68.1 4.0 %project.4 = (f32[256,512]{1,0:T(8,128)}, bf16[1,256,512]{2,1,0:T(8,128)(2,1)}, bf16[2,256,512]{2,1,0:T(8,128)(2,1)}) custom-call(bf16[2,256,512]{2,1,0:T(8,128)(2,1)} %get-tuple-element.20.refs_0_, bf16[2,128,512]{2,1,0:T(8,128)(2,1)} %copy-done, bf16[2,128,512]{2,1,0:T(8,128)(2,1)} %copy-done.3, bf16[2,128,512]{2,1,0:T(8,128)(2,1)} %copy-done.1, ...), custom_call_target="tpu_custom_call" | custom-call | tf_op jit(solution)/shard_map/project/pallas_call | solution.py:291
  72.2 5.9 %collective-permute-start.7 = (bf16[2,256,512]{2,1,0:T(8,128)(2,1)}, bf16[2,256,512]{2,1,0:T(8,128)(2,1)S(1)}, u32[]{:S(2)}, u32[]{:S(2)}) collective-permute-start(bf16[2,256,512]{2,1,0:T(8,128)(2,1)} %get-tuple-element.25), channel_id=1, source_target_pairs={{0,8},{4,12},{24,16},{28,20},{1,9},{5,13},{25,17},{29,21},{2,10},{... | collective-permute-start | bytes 1572872 | tf_op jit(solution)/shard_map/ppermute | solution.py:304
  78.1 1.1 pad_maximum_fusion.refs_5_
  79.3 0.7 collective-permute-start.27
  80.1 1.2 add_convert_fusion.1
  81.3 0.7 collective-permute-start.16
  82.0 3.0 %collective-permute-done.11 = bf16[2,256,512]{2,1,0:T(8,128)(2,1)} collective-permute-done((bf16[2,256,512]{2,1,0:T(8,128)(2,1)}, bf16[2,256,512]{2,1,0:T(8,128)(2,1)}, u32[]{:S(2)}, u32[]{:S(2)}) %collective-permute-start.11) | collective-permute-done | bytes 524320 | tf_op jit(solution)/shard_map/ppermute | solution.py:304
  84.9 1.1 fusion.2
  86.0 1.2 add_convert_fusion.2
  87.9 7.0 %collective-permute-done.7 = bf16[2,256,512]{2,1,0:T(8,128)(2,1)S(1)} collective-permute-done((bf16[2,256,512]{2,1,0:T(8,128)(2,1)}, bf16[2,256,512]{2,1,0:T(8,128)(2,1)S(1)}, u32[]{:S(2)}, u32[]{:S(2)}) %collective-permute-start.7) | collective-permute-done | bytes 524320 | tf_op jit(solution)/shard_map/ppermute | solution.py:304
  94.9 1.2 add_convert_fusion.3
  96.9 1.3 collective-permute-start.28
  99.0 1.2 add_convert_fusion.5
  100.2 18.8 %collective-permute-start.17 = (bf16[1,256,512]{2,1,0:T(8,128)(2,1)S(1)}, bf16[1,256,512]{2,1,0:T(8,128)(2,1)}, u32[]{:S(2)}, u32[]{:S(2)}) collective-permute-start(bf16[1,256,512]{2,1,0:T(8,128)(2,1)S(1)} %add_convert_fusion.5), channel_id=1, source_target_pairs={{0,8},{4,12},{8,0},{12,4},{16,24},{20,28},{24,16},{28,20},{1,9},{5... | collective-permute-start | bytes 786440 | tf_op jit(solution)/shard_map/ppermute | solution.py:307
  119.1 1.9 add_convert_fusion.6
  120.9 10.0 %collective-permute-start.13 = (bf16[1,256,512]{2,1,0:T(8,128)(2,1)}, bf16[1,256,512]{2,1,0:T(8,128)(2,1)}, u32[]{:S(2)}, u32[]{:S(2)}) collective-permute-start(bf16[1,256,512]{2,1,0:T(8,128)(2,1)} %add_convert_fusion.6), channel_id=1, source_target_pairs={{0,8},{4,12},{8,0},{12,4},{16,24},{20,28},{24,16},{28,20},{1,9},{5... | collective-permute-start | bytes 786440 | tf_op jit(solution)/shard_map/ppermute | solution.py:307
  130.9 1.9 add_convert_fusion.7
  132.8 9.3 %collective-permute-start.9 = (bf16[1,256,512]{2,1,0:T(8,128)(2,1)}, bf16[1,256,512]{2,1,0:T(8,128)(2,1)}, u32[]{:S(2)}, u32[]{:S(2)}) collective-permute-start(bf16[1,256,512]{2,1,0:T(8,128)(2,1)} %add_convert_fusion.7), channel_id=1, source_target_pairs={{0,8},{4,12},{8,0},{12,4},{16,24},{20,28},{24,16},{28,20},{1,9},{5... | collective-permute-start | bytes 786440 | tf_op jit(solution)/shard_map/ppermute | solution.py:307
  142.2 0.8 add_convert_fusion.4
  143.0 8.0 %collective-permute-start.21 = (bf16[1,256,512]{2,1,0:T(8,128)(2,1)}, bf16[1,256,512]{2,1,0:T(8,128)(2,1)S(1)}, u32[]{:S(2)}, u32[]{:S(2)}) collective-permute-start(bf16[1,256,512]{2,1,0:T(8,128)(2,1)} %add_convert_fusion.4), channel_id=1, source_target_pairs={{0,8},{4,12},{8,0},{12,4},{16,24},{20,28},{24,16},{28,20},{1,9},{5... | collective-permute-start | bytes 786440 | tf_op jit(solution)/shard_map/ppermute | solution.py:307
  151.0 1.6 collective-permute-start.26
  153.6 1.7 reshape.24.refs_2_
  155.4 1.7 reshape.25.refs_3_
  157.1 18.6 %taken.1 = (f32[64,4,128,128]{3,2,1,0:T(8,128)}, bf16[64,4,128,128]{3,2,1,0:T(8,128)(2,1)}) custom-call(s32[64]{0:T(128)} %refs_0_.4, f32[64,4,128,128]{3,2,1,0:T(8,128)} %refs_1_.1, bf16[256,512]{1,0:T(8,128)(2,1)} %reshape.24.refs_2_, bf16[256,512]{1,0:T(8,128)(2,1)} %reshape.25.refs_3_, f32[1,512]{1,0:T(1,128)} %bitcast.15), custom_call_target="tpu_custom_call" | custom-call | tf_op jit(solution)/shard_map/taken/pallas_call | solution.py:275
  175.7 8.7 %recur.1 = f32[256,512]{1,0:T(8,128)} custom-call(f32[256,512]{1,0:T(8,128)} %get-tuple-element.24.refs_0_, bf16[2,256,512]{2,1,0:T(8,128)(2,1)} %copy-done.10, bf16[1,256,512]{2,1,0:T(8,128)(2,1)} %collective-permute-done.9.refs_2_, f32[256,512]{1,0:T(8,128)} %get-tuple-element.27.refs_3_, bf16[2,256,512]{2,1,0:T(8,128)(2,1)} %copy-done.9, ...), custom_call_target="tpu_custom_call" | custom-call | tf_op jit(solution)/shard_map/recur/pallas_call | solution.py:359
  184.4 1.5 multiply_convert_fusion.refs_1_
  185.9 1.6 collective-permute-start.22
  187.5 4.9 %collective-permute-done.22.refs_2_ = bf16[256,512]{1,0:T(8,128)(2,1)S(1)} collective-permute-done((bf16[256,512]{1,0:T(8,128)(2,1)S(1)}, bf16[256,512]{1,0:T(8,128)(2,1)S(1)}, u32[]{:S(2)}, u32[]{:S(2)}) %collective-permute-start.22) | collective-permute-done | bytes 262176 | tf_op jit(solution)/shard_map/ppermute | solution.py:243
  192.4 1.5 collective-permute-done.24.refs_4_
  193.9 3.4 %collective-permute-done.29.refs_8_ = bf16[2,256,1024]{2,1,0:T(8,128)(2,1)} collective-permute-done((bf16[2,256,1024]{2,1,0:T(8,128)(2,1)S(1)}, bf16[2,256,1024]{2,1,0:T(8,128)(2,1)}, u32[]{:S(2)}, u32[]{:S(2)}) %collective-permute-start.29) | collective-permute-done | bytes 1048608 | tf_op jit(solution)/shard_map/ppermute | solution.py:341
  197.3 4.6 %mix.1 = bf16[256,1024]{1,0:T(8,128)(2,1)} custom-call(s32[4,4]{1,0:T(4,128)} %constant.5.clone.refs_0_, bf16[256,512]{1,0:T(8,128)(2,1)} %copy-done.11, bf16[256,512]{1,0:T(8,128)(2,1)} %copy-done.17, bf16[256,512]{1,0:T(8,128)(2,1)} %copy-done.18, bf16[256,512]{1,0:T(8,128)(2,1)} %copy-done.19, bf16[2,256,1024]{2,1,0:T(8,128)(2,1)} %copy-done.7, ...), custom_call_target="tpu_custom_call" | custom-call | tf_op jit(solution)/shard_map/mix/pallas_call | solution.py:380
  (77 shorter events, 4.9 us)
Async XLA Ops:
  5.6 14.4 %collective-permute-start = (bf16[2,128,512]{2,1,0:T(8,128)(2,1)}, bf16[2,128,512]{2,1,0:T(8,128)(2,1)S(1)}, u32[]{:S(2)}, u32[]{:S(2)}) collective-permute-start(bf16[2,128,512]{2,1,0:T(8,128)(2,1)} %get-tuple-element.21), channel_id=1, source_target_pairs={{0,8},{4,12},{8,0},{12,4},{16,24},{20,28},{24,16},{28,20},{1,9},{5... | collective-permute-start | bytes 786440 | tf_op jit(solution)/shard_map/ppermute | solution.py:264
  8.7 21.5 %collective-permute-start.2 = (bf16[2,128,512]{2,1,0:T(8,128)(2,1)}, bf16[2,128,512]{2,1,0:T(8,128)(2,1)S(1)}, u32[]{:S(2)}, u32[]{:S(2)}) collective-permute-start(bf16[2,128,512]{2,1,0:T(8,128)(2,1)} %get-tuple-element.22), channel_id=1, source_target_pairs={{0,16},{4,20},{8,24},{12,28},{16,0},{20,4},{24,8},{28,12},{1,17},{... | collective-permute-start | bytes 786440 | tf_op jit(solution)/shard_map/ppermute | solution.py:264
  11.3 18.9 %collective-permute-start.4 = (bf16[2,128,512]{2,1,0:T(8,128)(2,1)}, bf16[2,128,512]{2,1,0:T(8,128)(2,1)S(1)}, u32[]{:S(2)}, u32[]{:S(2)}) collective-permute-start(bf16[2,128,512]{2,1,0:T(8,128)(2,1)} %get-tuple-element.23), channel_id=1, source_target_pairs={{0,24},{4,28},{8,16},{12,20},{16,8},{20,12},{24,0},{28,4},{1,25},{... | collective-permute-start | bytes 786440 | tf_op jit(solution)/shard_map/ppermute | solution.py:264
  11.3 27.3 %collective-permute-start.14 = (bf16[512,512]{1,0:T(8,128)(2,1)}, bf16[512,512]{1,0:T(8,128)(2,1)S(1)}, u32[]{:S(2)}, u32[]{:S(2)}) collective-permute-start(bf16[512,512]{1,0:T(8,128)(2,1)} %refs_7_.6), channel_id=1, source_target_pairs={{4,0},{0,4},{12,8},{8,12},{20,16},{16,20},{28,24},{24,28},{5,1},{1... | collective-permute-start | bytes 1572872 | tf_op jit(solution)/shard_map/ppermute | solution.py:247
  20.1 18.5 %copy-start = (bf16[2,128,512]{2,1,0:T(8,128)(2,1)}, bf16[2,128,512]{2,1,0:T(8,128)(2,1)S(1)}, u32[]{:S(2)}) copy-start(bf16[2,128,512]{2,1,0:T(8,128)(2,1)S(1)} %collective-permute-done.refs_1_) | copy-start | bytes 786436
  20.1 12.2 %collective-permute-start.1 = (bf16[2,128,512]{2,1,0:T(8,128)(2,1)S(1)}, bf16[2,128,512]{2,1,0:T(8,128)(2,1)S(1)}, u32[]{:S(2)}, u32[]{:S(2)}) collective-permute-start(bf16[2,128,512]{2,1,0:T(8,128)(2,1)S(1)} %collective-permute-done.refs_1_), channel_id=1, source_target_pairs={{0,1},{1,0},{2,3},{3,2},{4,5},{5,4},{6,7},{7,6},{8,9},{9,8},{10,11... | collective-permute-start | bytes 786440 | tf_op jit(solution)/shard_map/ppermute | solution.py:243
  30.2 8.4 %copy-start.1 = (bf16[2,128,512]{2,1,0:T(8,128)(2,1)}, bf16[2,128,512]{2,1,0:T(8,128)(2,1)S(1)}, u32[]{:S(2)}) copy-start(bf16[2,128,512]{2,1,0:T(8,128)(2,1)S(1)} %collective-permute-done.2.refs_3_) | copy-start | bytes 786436
  30.2 2.6 %collective-permute-start.3 = (bf16[2,128,512]{2,1,0:T(8,128)(2,1)S(1)}, bf16[2,128,512]{2,1,0:T(8,128)(2,1)S(1)}, u32[]{:S(2)}, u32[]{:S(2)}) collective-permute-start(bf16[2,128,512]{2,1,0:T(8,128)(2,1)S(1)} %collective-permute-done.2.refs_3_), channel_id=1, source_target_pairs={{0,1},{1,0},{2,3},{3,2},{4,5},{5,4},{6,7},{7,6},{8,9},{9,8},{10,11... | collective-permute-start | bytes 786440 | tf_op jit(solution)/shard_map/ppermute | solution.py:243
  30.2 8.4 %copy-start.2 = (bf16[2,128,512]{2,1,0:T(8,128)(2,1)}, bf16[2,128,512]{2,1,0:T(8,128)(2,1)S(1)}, u32[]{:S(2)}) copy-start(bf16[2,128,512]{2,1,0:T(8,128)(2,1)S(1)} %collective-permute-done.4.refs_5_) | copy-start | bytes 786436
  30.2 4.1 %collective-permute-start.5 = (bf16[2,128,512]{2,1,0:T(8,128)(2,1)S(1)}, bf16[2,128,512]{2,1,0:T(8,128)(2,1)S(1)}, u32[]{:S(2)}, u32[]{:S(2)}) collective-permute-start(bf16[2,128,512]{2,1,0:T(8,128)(2,1)S(1)} %collective-permute-done.4.refs_5_), channel_id=1, source_target_pairs={{0,1},{1,0},{2,3},{3,2},{4,5},{5,4},{6,7},{7,6},{8,9},{9,8},{10,11... | collective-permute-start | bytes 786440 | tf_op jit(solution)/shard_map/ppermute | solution.py:243
  30.7 15.0 %collective-permute-start.18 = (bf16[512,512]{1,0:T(8,128)(2,1)}, bf16[512,512]{1,0:T(8,128)(2,1)S(1)}, u32[]{:S(2)}, u32[]{:S(2)}) collective-permute-start(bf16[512,512]{1,0:T(8,128)(2,1)} %refs_7_.7), channel_id=1, source_target_pairs={{4,0},{0,4},{12,8},{8,12},{20,16},{16,20},{28,24},{24,28},{5,1},{1... | collective-permute-start | bytes 1572872 | tf_op jit(solution)/shard_map/ppermute | solution.py:247
  32.3 6.4 %copy-start.3 = (bf16[2,128,512]{2,1,0:T(8,128)(2,1)}, bf16[2,128,512]{2,1,0:T(8,128)(2,1)S(1)}, u32[]{:S(2)}) copy-start(bf16[2,128,512]{2,1,0:T(8,128)(2,1)S(1)} %collective-permute-done.1.refs_2_) | copy-start | bytes 786436
  32.3 24.8 %collective-permute-start.10 = (bf16[512,512]{1,0:T(8,128)(2,1)}, bf16[512,512]{1,0:T(8,128)(2,1)}, u32[]{:S(2)}, u32[]{:S(2)}) collective-permute-start(bf16[512,512]{1,0:T(8,128)(2,1)} %refs_7_.5), channel_id=1, source_target_pairs={{4,0},{0,4},{12,8},{8,12},{20,16},{16,20},{28,24},{24,28},{5,1},{1... | collective-permute-start | bytes 1572872 | tf_op jit(solution)/shard_map/ppermute | solution.py:247
  32.8 5.9 %copy-start.4 = (bf16[2,128,512]{2,1,0:T(8,128)(2,1)}, bf16[2,128,512]{2,1,0:T(8,128)(2,1)S(1)}, u32[]{:S(2)}) copy-start(bf16[2,128,512]{2,1,0:T(8,128)(2,1)S(1)} %collective-permute-done.3.refs_4_) | copy-start | bytes 786436
  32.8 35.4 %collective-permute-start.6 = (bf16[512,512]{1,0:T(8,128)(2,1)}, bf16[512,512]{1,0:T(8,128)(2,1)}, u32[]{:S(2)}, u32[]{:S(2)}) collective-permute-start(bf16[512,512]{1,0:T(8,128)(2,1)} %refs_7_.4), channel_id=1, source_target_pairs={{4,0},{0,4},{12,8},{8,12},{20,16},{16,20},{28,24},{24,28},{5,1},{1... | collective-permute-start | bytes 1572872 | tf_op jit(solution)/shard_map/ppermute | solution.py:247
  34.3 4.4 %copy-start.5 = (bf16[2,128,512]{2,1,0:T(8,128)(2,1)}, bf16[2,128,512]{2,1,0:T(8,128)(2,1)S(1)}, u32[]{:S(2)}) copy-start(bf16[2,128,512]{2,1,0:T(8,128)(2,1)S(1)} %collective-permute-done.5.refs_6_) | copy-start | bytes 786436
  34.3 43.8 %collective-permute-start.25 = (bf16[1,256,1024]{2,1,0:T(8,128)(2,1)}, bf16[1,256,1024]{2,1,0:T(8,128)(2,1)S(1)}, u32[]{:S(2)}, u32[]{:S(2)}) collective-permute-start(bf16[1,256,1024]{2,1,0:T(8,128)(2,1)} %bitcast.12), channel_id=1, source_target_pairs={{0,8},{4,12},{8,0},{12,4},{16,24},{20,28},{24,16},{28,20},{1,9},{5... | collective-permute-start | bytes 1572872 | tf_op jit(solution)/shard_map/ppermute | solution.py:321
  43.5 36.6 %collective-permute-start.15 = (bf16[2,256,512]{2,1,0:T(8,128)(2,1)}, bf16[2,256,512]{2,1,0:T(8,128)(2,1)S(1)}, u32[]{:S(2)}, u32[]{:S(2)}) collective-permute-start(bf16[2,256,512]{2,1,0:T(8,128)(2,1)} %get-tuple-element.31), channel_id=1, source_target_pairs={{0,8},{4,12},{24,16},{28,20},{1,9},{5,13},{25,17},{29,21},{2,10},{... | collective-permute-start | bytes 1572872 | tf_op jit(solution)/shard_map/ppermute | solution.py:304
  50.6 47.6 %copy-start.12 = (bf16[2,256,512]{2,1,0:T(8,128)(2,1)S(1)}, bf16[2,256,512]{2,1,0:T(8,128)(2,1)}, u32[]{:S(2)}) copy-start(bf16[2,256,512]{2,1,0:T(8,128)(2,1)} %get-tuple-element.35) | copy-start | bytes 1572868
  50.6 91.6 %copy-start.16 = (bf16[1,256,512]{2,1,0:T(8,128)(2,1)S(1)}, bf16[1,256,512]{2,1,0:T(8,128)(2,1)}, u32[]{:S(2)}) copy-start(bf16[1,256,512]{2,1,0:T(8,128)(2,1)} %get-tuple-element.36) | copy-start | bytes 786436
  50.6 46.2 %collective-permute-start.19 = (bf16[2,256,512]{2,1,0:T(8,128)(2,1)}, bf16[2,256,512]{2,1,0:T(8,128)(2,1)S(1)}, u32[]{:S(2)}, u32[]{:S(2)}) collective-permute-start(bf16[2,256,512]{2,1,0:T(8,128)(2,1)} %get-tuple-element.35), channel_id=1, source_target_pairs={{0,8},{4,12},{24,16},{28,20},{1,9},{5,13},{25,17},{29,21},{2,10},{... | collective-permute-start | bytes 1572872 | tf_op jit(solution)/shard_map/ppermute | solution.py:304
  61.1 23.8 %collective-permute-start.11 = (bf16[2,256,512]{2,1,0:T(8,128)(2,1)}, bf16[2,256,512]{2,1,0:T(8,128)(2,1)}, u32[]{:S(2)}, u32[]{:S(2)}) collective-permute-start(bf16[2,256,512]{2,1,0:T(8,128)(2,1)} %get-tuple-element.28), channel_id=1, source_target_pairs={{0,8},{4,12},{24,16},{28,20},{1,9},{5,13},{25,17},{29,21},{2,10},{... | collective-permute-start | bytes 1572872 | tf_op jit(solution)/shard_map/ppermute | solution.py:304
  72.2 22.7 %collective-permute-start.7 = (bf16[2,256,512]{2,1,0:T(8,128)(2,1)}, bf16[2,256,512]{2,1,0:T(8,128)(2,1)S(1)}, u32[]{:S(2)}, u32[]{:S(2)}) collective-permute-start(bf16[2,256,512]{2,1,0:T(8,128)(2,1)} %get-tuple-element.25), channel_id=1, source_target_pairs={{0,8},{4,12},{24,16},{28,20},{1,9},{5,13},{25,17},{29,21},{2,10},{... | collective-permute-start | bytes 1572872 | tf_op jit(solution)/shard_map/ppermute | solution.py:304
  79.3 96.4 %copy-start.7 = (bf16[2,256,1024]{2,1,0:T(8,128)(2,1)}, bf16[2,256,1024]{2,1,0:T(8,128)(2,1)S(1)}, u32[]{:S(2)}) copy-start(bf16[2,256,1024]{2,1,0:T(8,128)(2,1)S(1)} %pad_maximum_fusion.refs_5_) | copy-start | bytes 3145732
  79.3 17.6 %collective-permute-start.27 = (bf16[2,256,1024]{2,1,0:T(8,128)(2,1)S(1)}, bf16[2,256,1024]{2,1,0:T(8,128)(2,1)S(1)}, u32[]{:S(2)}, u32[]{:S(2)}) collective-permute-start(bf16[2,256,1024]{2,1,0:T(8,128)(2,1)S(1)} %pad_maximum_fusion.refs_5_), channel_id=1, source_target_pairs={{8,16},{12,20},{16,8},{20,12},{9,17},{13,21},{17,9},{21,13},{10,18... | collective-permute-start | bytes 3145736 | tf_op jit(solution)/shard_map/ppermute | solution.py:321
  81.3 17.8 %collective-permute-start.16 = (bf16[2,256,512]{2,1,0:T(8,128)(2,1)S(1)}, bf16[2,256,512]{2,1,0:T(8,128)(2,1)S(1)}, u32[]{:S(2)}, u32[]{:S(2)}) collective-permute-start(bf16[2,256,512]{2,1,0:T(8,128)(2,1)S(1)} %add_convert_fusion.1), channel_id=1, source_target_pairs={{8,16},{12,20},{16,8},{20,12},{9,17},{13,21},{17,9},{21,13},{10,18... | collective-permute-start | bytes 1572872 | tf_op jit(solution)/shard_map/ppermute | solution.py:307
  87.2 31.9 %collective-permute-start.12 = (bf16[2,256,512]{2,1,0:T(8,128)(2,1)S(1)}, bf16[2,256,512]{2,1,0:T(8,128)(2,1)S(1)}, u32[]{:S(2)}, u32[]{:S(2)}) collective-permute-start(bf16[2,256,512]{2,1,0:T(8,128)(2,1)S(1)} %add_convert_fusion.2), channel_id=1, source_target_pairs={{8,16},{12,20},{16,8},{20,12},{9,17},{13,21},{17,9},{21,13},{10,18... | collective-permute-start | bytes 1572872 | tf_op jit(solution)/shard_map/ppermute | solution.py:307
  96.1 34.8 %collective-permute-start.8 = (bf16[2,256,512]{2,1,0:T(8,128)(2,1)S(1)}, bf16[2,256,512]{2,1,0:T(8,128)(2,1)S(1)}, u32[]{:S(2)}, u32[]{:S(2)}) collective-permute-start(bf16[2,256,512]{2,1,0:T(8,128)(2,1)S(1)} %add_convert_fusion.3), channel_id=1, source_target_pairs={{8,16},{12,20},{16,8},{20,12},{9,17},{13,21},{17,9},{21,13},{10,18... | collective-permute-start | bytes 1572872 | tf_op jit(solution)/shard_map/ppermute | solution.py:307
  96.9 54.2 %collective-permute-start.28 = (bf16[2,256,1024]{2,1,0:T(8,128)(2,1)S(1)}, bf16[2,256,1024]{2,1,0:T(8,128)(2,1)S(1)}, u32[]{:S(2)}, u32[]{:S(2)}) collective-permute-start(bf16[2,256,1024]{2,1,0:T(8,128)(2,1)S(1)} %collective-permute-done.27), channel_id=1, source_target_pairs={{8,0},{12,4},{16,24},{20,28},{9,1},{13,5},{17,25},{21,29},{10,2},{... | collective-permute-start | bytes 3145736 | tf_op jit(solution)/shard_map/ppermute | solution.py:325
  98.3 43.8 %collective-permute-start.20 = (bf16[2,256,512]{2,1,0:T(8,128)(2,1)S(1)}, bf16[2,256,512]{2,1,0:T(8,128)(2,1)S(1)}, u32[]{:S(2)}, u32[]{:S(2)}) collective-permute-start(bf16[2,256,512]{2,1,0:T(8,128)(2,1)S(1)} %add_convert_fusion), channel_id=1, source_target_pairs={{8,16},{12,20},{16,8},{20,12},{9,17},{13,21},{17,9},{21,13},{10,18... | collective-permute-start | bytes 1572872 | tf_op jit(solution)/shard_map/ppermute | solution.py:307
  99.0 76.7 %copy-start.8 = (bf16[2,256,512]{2,1,0:T(8,128)(2,1)}, bf16[2,256,512]{2,1,0:T(8,128)(2,1)S(1)}, u32[]{:S(2)}) copy-start(bf16[2,256,512]{2,1,0:T(8,128)(2,1)S(1)} %collective-permute-done.16.refs_7_) | copy-start | bytes 1572868
  100.2 52.8 %collective-permute-start.17 = (bf16[1,256,512]{2,1,0:T(8,128)(2,1)S(1)}, bf16[1,256,512]{2,1,0:T(8,128)(2,1)}, u32[]{:S(2)}, u32[]{:S(2)}) collective-permute-start(bf16[1,256,512]{2,1,0:T(8,128)(2,1)S(1)} %add_convert_fusion.5), channel_id=1, source_target_pairs={{0,8},{4,12},{8,0},{12,4},{16,24},{20,28},{24,16},{28,20},{1,9},{5... | collective-permute-start | bytes 786440 | tf_op jit(solution)/shard_map/ppermute | solution.py:307
  119.1 56.7 %copy-start.9 = (bf16[2,256,512]{2,1,0:T(8,128)(2,1)}, bf16[2,256,512]{2,1,0:T(8,128)(2,1)S(1)}, u32[]{:S(2)}) copy-start(bf16[2,256,512]{2,1,0:T(8,128)(2,1)S(1)} %collective-permute-done.12.refs_4_) | copy-start | bytes 1572868
  120.9 54.7 %collective-permute-start.13 = (bf16[1,256,512]{2,1,0:T(8,128)(2,1)}, bf16[1,256,512]{2,1,0:T(8,128)(2,1)}, u32[]{:S(2)}, u32[]{:S(2)}) collective-permute-start(bf16[1,256,512]{2,1,0:T(8,128)(2,1)} %add_convert_fusion.6), channel_id=1, source_target_pairs={{0,8},{4,12},{8,0},{12,4},{16,24},{20,28},{24,16},{28,20},{1,9},{5... | collective-permute-start | bytes 786440 | tf_op jit(solution)/shard_map/ppermute | solution.py:307
  130.9 20.1 %copy-start.10 = (bf16[2,256,512]{2,1,0:T(8,128)(2,1)}, bf16[2,256,512]{2,1,0:T(8,128)(2,1)S(1)}, u32[]{:S(2)}) copy-start(bf16[2,256,512]{2,1,0:T(8,128)(2,1)S(1)} %collective-permute-done.8.refs_1_) | copy-start | bytes 1572868
  132.8 42.9 %collective-permute-start.9 = (bf16[1,256,512]{2,1,0:T(8,128)(2,1)}, bf16[1,256,512]{2,1,0:T(8,128)(2,1)}, u32[]{:S(2)}, u32[]{:S(2)}) collective-permute-start(bf16[1,256,512]{2,1,0:T(8,128)(2,1)} %add_convert_fusion.7), channel_id=1, source_target_pairs={{0,8},{4,12},{8,0},{12,4},{16,24},{20,28},{24,16},{28,20},{1,9},{5... | collective-permute-start | bytes 786440 | tf_op jit(solution)/shard_map/ppermute | solution.py:307
  142.2 8.9 %copy-start.13 = (bf16[2,256,512]{2,1,0:T(8,128)(2,1)}, bf16[2,256,512]{2,1,0:T(8,128)(2,1)S(1)}, u32[]{:S(2)}) copy-start(bf16[2,256,512]{2,1,0:T(8,128)(2,1)S(1)} %collective-permute-done.20) | copy-start | bytes 1572868
  143.0 41.4 %collective-permute-start.21 = (bf16[1,256,512]{2,1,0:T(8,128)(2,1)}, bf16[1,256,512]{2,1,0:T(8,128)(2,1)S(1)}, u32[]{:S(2)}, u32[]{:S(2)}) collective-permute-start(bf16[1,256,512]{2,1,0:T(8,128)(2,1)} %add_convert_fusion.4), channel_id=1, source_target_pairs={{0,8},{4,12},{8,0},{12,4},{16,24},{20,28},{24,16},{28,20},{1,9},{5... | collective-permute-start | bytes 786440 | tf_op jit(solution)/shard_map/ppermute | solution.py:307
  151.0 41.3 %collective-permute-start.26 = (bf16[2,256,1024]{2,1,0:T(8,128)(2,1)S(1)}, bf16[2,256,1024]{2,1,0:T(8,128)(2,1)}, u32[]{:S(2)}, u32[]{:S(2)}) collective-permute-start(bf16[2,256,1024]{2,1,0:T(8,128)(2,1)S(1)} %pad_maximum_fusion.refs_5_), channel_id=1, source_target_pairs={{4,0},{0,4},{12,8},{8,12},{20,16},{16,20},{28,24},{24,28},{5,1},{1... | collective-permute-start | bytes 3145736 | tf_op jit(solution)/shard_map/ppermute | solution.py:341
  153.0 44.2 %copy-start.6 = (bf16[2,256,1024]{2,1,0:T(8,128)(2,1)}, bf16[2,256,1024]{2,1,0:T(8,128)(2,1)S(1)}, u32[]{:S(2)}) copy-start(bf16[2,256,1024]{2,1,0:T(8,128)(2,1)S(1)} %add.48.refs_7_) | copy-start | bytes 3145732
  153.1 44.2 %collective-permute-start.29 = (bf16[2,256,1024]{2,1,0:T(8,128)(2,1)S(1)}, bf16[2,256,1024]{2,1,0:T(8,128)(2,1)}, u32[]{:S(2)}, u32[]{:S(2)}) collective-permute-start(bf16[2,256,1024]{2,1,0:T(8,128)(2,1)S(1)} %add.48.refs_7_), channel_id=1, source_target_pairs={{4,0},{0,4},{12,8},{8,12},{20,16},{16,20},{28,24},{24,28},{5,1},{1... | collective-permute-start | bytes 3145736 | tf_op jit(solution)/shard_map/ppermute | solution.py:341
  185.9 11.4 %copy-start.11 = (bf16[256,512]{1,0:T(8,128)(2,1)}, bf16[256,512]{1,0:T(8,128)(2,1)S(1)}, u32[]{:S(2)}) copy-start(bf16[256,512]{1,0:T(8,128)(2,1)S(1)} %multiply_convert_fusion.refs_1_) | copy-start | bytes 786436
  185.9 6.4 %collective-permute-start.22 = (bf16[256,512]{1,0:T(8,128)(2,1)S(1)}, bf16[256,512]{1,0:T(8,128)(2,1)S(1)}, u32[]{:S(2)}, u32[]{:S(2)}) collective-permute-start(bf16[256,512]{1,0:T(8,128)(2,1)S(1)} %multiply_convert_fusion.refs_1_), channel_id=1, source_target_pairs={{0,2},{1,3},{2,0},{3,1},{4,6},{5,7},{6,4},{7,5},{8,10},{9,11},{10,... | collective-permute-start | bytes 786440 | tf_op jit(solution)/shard_map/ppermute | solution.py:243
  187.5 4.9 %collective-permute-start.23 = (bf16[256,512]{1,0:T(8,128)(2,1)S(1)}, bf16[256,512]{1,0:T(8,128)(2,1)S(1)}, u32[]{:S(2)}, u32[]{:S(2)}) collective-permute-start(bf16[256,512]{1,0:T(8,128)(2,1)S(1)} %multiply_convert_fusion.refs_1_), channel_id=1, source_target_pairs={{0,1},{1,0},{2,3},{3,2},{4,5},{5,4},{6,7},{7,6},{8,9},{9,8},{10,11... | collective-permute-start | bytes 786440 | tf_op jit(solution)/shard_map/ppermute | solution.py:243
  192.4 4.9 %copy-start.17 = (bf16[256,512]{1,0:T(8,128)(2,1)}, bf16[256,512]{1,0:T(8,128)(2,1)S(1)}, u32[]{:S(2)}) copy-start(bf16[256,512]{1,0:T(8,128)(2,1)S(1)} %collective-permute-done.22.refs_2_) | copy-start | bytes 786436
  192.4 1.5 collective-permute-start.24
  192.4 4.9 %copy-start.18 = (bf16[256,512]{1,0:T(8,128)(2,1)}, bf16[256,512]{1,0:T(8,128)(2,1)S(1)}, u32[]{:S(2)}) copy-start(bf16[256,512]{1,0:T(8,128)(2,1)S(1)} %collective-permute-done.23.refs_3_) | copy-start | bytes 786436
  193.9 3.4 %copy-start.19 = (bf16[256,512]{1,0:T(8,128)(2,1)}, bf16[256,512]{1,0:T(8,128)(2,1)S(1)}, u32[]{:S(2)}) copy-start(bf16[256,512]{1,0:T(8,128)(2,1)S(1)} %collective-permute-done.24.refs_4_) | copy-start | bytes 786436
  (2 other events, 1.6 us)
where the time goes:
time: 203 us; the launch traced here: 202 us
  starting transfers between devices  91.8 us (45%)
  Pallas kernels  53.1 us (26%)
  waiting for transfers between devices  37.4 us (18%)
  other arithmetic  12.5 us (6%)
  local copies, waits for them, and re-layouts  6.2 us (3%)
    ppermute x8, starting transfers between devices, summed(): got = lax.ppermute(out, 'kv', mirrored(size, size - 1, size))  48.9 us
    ppermute x4, starting transfers between devices, summed(): got = lax.ppermute(out, 'kv', mirrored(size, hop - 1, hop))  21.3 us
    pallas_call x1, Pallas kernels, on_device(): pl.pallas_call(lambda *refs: taken_kernel(*refs, proposals=proposals), ou...  18.6 us
    ppermute x3, waiting for transfers between devices, on_device(): lax.ppermute(mine[r - 1], 'kv', groups([(g, g ^ r) for g in range(ring)]))  17.2 us
    pallas_call x4, Pallas kernels, summed(): pl.pallas_call(lambda *refs: project_kernel(*refs, ring=ring, inner=inner...  16.2 us
    ppermute x4, waiting for transfers between devices, summed(): got = lax.ppermute(out, 'kv', mirrored(size, hop - 1, hop))  9.97 us
    convert_element_type x8, other arithmetic, added(): return (a.astype(F32) + b.astype(F32)).astype(BF16)  9.47 us
    pallas_call x1, Pallas kernels, on_device(): pl.pallas_call(lambda *refs: recur_kernel(*refs, parts=parts, proposals=p...  8.72 us
  transfers between devices with their start and end apart: 30, of which 9 were waited for; matrix products, arithmetic and copies ran while one was open for 8% of the time, Pallas kernels for 22%

commit v1 on v0

v1 whole, which is shorter than its diff:
```python
import jax
import jax.numpy as jnp
import numpy as np
from jax import lax
from jax.experimental import pallas as pl
from jax.experimental.pallas import tpu as pltpu
from jax.sharding import PartitionSpec as P


EPSILON = 1e-06
F32 = jnp.float32
BF16 = jnp.bfloat16
VMEM = pl.BlockSpec(memory_space=pltpu.VMEM)
SMEM = pl.BlockSpec(memory_space=pltpu.SMEM)
HBM = pl.BlockSpec(memory_space=pltpu.MemorySpace.HBM)


def room(mib):
    return pltpu.CompilerParams(vmem_limit_bytes=mib << 20)


def forget_of(pre_act, bounds):
    return bounds + (1.0 - bounds) * jax.nn.sigmoid(pre_act)


def norm_kernel(tokens, gain, *refs, ring, inner, share, heads):
    weights, own, mine = refs[:4], refs[4], refs[5 : 4 + ring]
    pieces, (scratch, sems) = refs[4 + ring : -2], refs[-2:]
    keys = weights[0].shape[1] // heads
    copies = [
        pltpu.make_async_copy(
            weights[k].at[:, pl.ds(head * keys, keys)],
            pieces[head].at[:, pl.ds(k * keys, keys)],
            sems.at[head * 4 + k],
        )
        for head in range(heads)
        for k in range(4)
    ]
    for copy in copies:
        copy.start()
    rows, width = tokens.shape
    step = 16
    block = own.shape[-1]
    part = rows // share
    chunk = min(width, 512)

    def one(i, carry):
        here = pl.ds(pl.multiple_of(i * step, step), step)
        total = jnp.zeros((step, 128), F32)
        for at in range(0, width, chunk):
            x = tokens[here, at : at + chunk].astype(F32)
            x = x * x
            for k in range(0, chunk, 128):
                total = total + x[:, k : k + 128]
        scale = lax.rsqrt(jnp.sum(total, axis=-1, keepdims=True) / width + EPSILON)
        for at in range(0, width, chunk):
            x = tokens[here, at : at + chunk].astype(F32)
            scratch[here, at : at + chunk] = (x * scale * gain[:, at : at + chunk]).astype(BF16)
        return carry

    lax.fori_loop(0, rows // step, one, 0, unroll=4)
    me, lane = lax.axis_index("kv"), lax.axis_index("tp")
    group, member = lax.div(me, inner), lax.rem(me, inner)
    here = pl.ds(pl.multiple_of(lax.rem(lane, share) * part, part), part)
    for r in range(ring):
        owner = jnp.bitwise_xor(group, r)
        for turn in range(inner):
            column = owner * inner + lax.rem(member + turn, inner)
            cols = pl.ds(pl.multiple_of(column * block, block), block)
            if r == 0:
                own[turn] = scratch[:, cols]
            else:
                mine[r - 1][turn] = scratch[here, cols]
    for copy in copies:
        copy.wait()


def project_kernel(*refs, ring, inner, share, fresh):
    if fresh:
        own, others = refs[0], refs[1 : 1 + (ring - 1) * share]
        weights = refs[1 + (ring - 1) * share :][:inner]
        outs, lhs, stack = refs[1 + (ring - 1) * share + inner : -2], refs[-2], refs[-1]
        rows, block = own.shape[1], own.shape[2]
        part = rows // share
        lane = lax.rem(lax.axis_index("tp"), share)
        for turn in range(inner):
            cols = slice(turn * block, (turn + 1) * block)
            lhs[0:rows, cols] = own[turn]
            for r in range(ring - 1):
                for other in range(share):
                    at = (r + 1) * rows + jnp.bitwise_xor(lane, other) * part
                    lhs[pl.ds(pl.multiple_of(at, part), part), cols] = others[r * share + other][turn]
    else:
        lhs, weights = refs[0], refs[1 : 1 + inner]
        outs, stack = refs[1 + inner : -1], refs[-1]
        block = weights[0].shape[0]
        rows = lhs.shape[0] // ring
    group = lax.div(lax.axis_index("kv"), inner)
    for turn in range(inner):
        stack[turn * block : (turn + 1) * block, :] = weights[turn][...]
    for level in reversed(range(len(outs))):
        size = 1 << max(level - 1, 0)
        start = size if level else 0
        total = jnp.dot(
            lhs[start * rows : (start + size) * rows, :], stack[...], preferred_element_type=F32
        )
        if level:
            for k in range(size):
                at = jnp.bitwise_xor(lax.rem(group, size), k)
                outs[level][at] = total[k * rows : (k + 1) * rows].astype(BF16)
        else:
            outs[0][...] = total


def position_of(shape, proposals):
    return lax.rem(lax.broadcasted_iota(jnp.int32, shape, 0), proposals)


def taken_kernel(accepted, state, forget, values, bounds, taken, held, come, gone, *, proposals, seqs):
    count, heads, keys, vals = state.shape
    steps = count // seqs
    rows = seqs * proposals
    position = position_of((rows, keys), proposals)
    owner = lax.broadcasted_iota(jnp.int32, (rows, keys), 0) // proposals

    def copy_in(i):
        here = pl.ds(i * seqs, seqs)
        return pltpu.make_async_copy(state.at[here], held.at[here], come.at[i])

    def copy_out(i):
        here = pl.ds(i * seqs, seqs)
        return pltpu.make_async_copy(held.at[here], taken.at[here], gone.at[i])

    for i in range(steps):
        copy_in(i).start()

    def one(i, carry):
        first = i * seqs
        old = jnp.concatenate([forget[first + seq].astype(F32) for seq in range(seqs)], axis=0)
        new = jnp.concatenate([values[first + seq].astype(F32) for seq in range(seqs)], axis=0).astype(BF16)
        taking = jnp.zeros((rows, keys), jnp.int32)
        for seq in range(seqs):
            taking = jnp.where(owner == seq, accepted[first + seq], taking)
        kept = position < taking
        decays, addeds = [], []
        for head in range(heads):
            cols = slice(head * keys, (head + 1) * keys)
            gate = forget_of(old[:, cols], bounds[:, cols])
            decay = jnp.where(kept, gate, 1.0)
            after = jnp.ones_like(decay)
            for ahead in range(1, proposals):
                moved = pltpu.roll(decay, rows - ahead, axis=0)
                after = after * jnp.where(position < proposals - ahead, moved, 1.0)
            decays.append((decay * after).T)
            weight = (jnp.where(kept, 1.0 - gate, 0.0) * after).T
            high = weight.astype(BF16)
            low = (weight - high.astype(F32)).astype(BF16)
            value = new[:, head * vals : (head + 1) * vals]
            spread = jnp.concatenate(
                [jnp.where(owner == seq, value, jnp.zeros_like(value)) for seq in range(seqs)], axis=1
            )
            addeds.append(
                jnp.dot(
                    jnp.concatenate([high, low], axis=1),
                    jnp.concatenate([spread, spread], axis=0),
                    preferred_element_type=F32,
                )
            )
        copy_in(i).wait()
        for head in range(heads):
            for seq in range(seqs):
                at = seq * proposals
                held[first + seq, head] = (
                    decays[head][:, at : at + 1] * held[first + seq, head]
                    + addeds[head][:, seq * vals : (seq + 1) * vals]
                )
        copy_out(i).start()
        return carry

    lax.fori_loop(0, steps, one, 0)
    for i in range(steps):
        copy_out(i).wait()


def recur_kernel(*refs, parts, heads, first, proposals, inner):
    pieces = refs[: parts * heads]
    taken, bounds, gain, out = refs[parts * heads :]
    where = lax.div(lax.axis_index("kv"), inner)
    seqs, _, keys, vals = taken.shape
    rows = seqs * proposals
    position = position_of((rows, keys), proposals)
    group = 4
    tile = group * proposals
    tile_seq = lax.broadcasted_iota(jnp.int32, (tile, keys), 0) // proposals

    def total_of(head, k):
        cols = slice(k * keys, (k + 1) * keys)
        total = pieces[head * parts][:, cols]
        for piece in pieces[head * parts + 1 : (head + 1) * parts]:
            total = total + piece[lax.rem(where, piece.shape[0]), :, cols].astype(F32)
        return total

    for head in range(heads):
        cols = slice((first + head) * keys, (first + head + 1) * keys)
        gate = forget_of(total_of(head, 0), bounds[:, cols])
        value = total_of(head, 1)
        query = total_of(head, 2) * keys ** (-0.5)
        key = 1.0 - gate
        through = query
        result = jnp.sum(query * key, axis=-1, keepdims=True) * value
        grown = gate
        before = gate
        for lag in range(1, proposals):
            inside = position >= lag
            through = through * jnp.where(inside, before, 0.0)
            score = jnp.sum(through * pltpu.roll(key, lag, axis=0), axis=-1, keepdims=True)
            result = result + score * pltpu.roll(value, lag, axis=0)
            before = pltpu.roll(gate, lag, axis=0)
            grown = grown * jnp.where(inside, before, 1.0)
        reach = (query * grown).astype(BF16)
        met = []
        for at in range(0, seqs, group):
            part = reach[at * proposals : (at + group) * proposals, :]
            lhs = jnp.concatenate(
                [jnp.where(tile_seq == s, part, jnp.zeros_like(part)) for s in range(group)], axis=1
            )
            here = taken[at : at + group, head].astype(BF16).reshape(group * keys, vals)
            met.append(jnp.dot(lhs, here, preferred_element_type=F32))
        result = result + jnp.concatenate(met, axis=0)
        scale = lax.rsqrt(jnp.mean(result * result, axis=-1, keepdims=True) + EPSILON)
        result = result * scale * gain[:, cols] * jax.nn.silu(total_of(head, 3))
        out[:, head * keys : (head + 1) * keys] = result.astype(BF16)


def mix_kernel(order, *refs, lanes, ids, runs, inner, keys):
    heads, weights = refs[: lanes * len(runs)], refs[lanes * len(runs) : -2]
    out, lhs = refs[-2:]
    height = weights[0].shape[1]
    per = height // keys
    count = sum(len(run) for run in runs)
    mine = lax.axis_index("tp")
    me = lax.axis_index("kv")
    group, member = lax.div(me, inner), lax.rem(me, inner)
    for at, run in enumerate(runs):
        for k, other in enumerate(ids):
            lane = jnp.bitwise_xor(mine, other)
            for j, head in enumerate(run):
                where = lane * (count // per) + head // per
                cols = slice(head % per * keys, (head % per + 1) * keys)
                lhs[where, :, cols] = heads[at * lanes + k][:, j * keys : (j + 1) * keys]
    chunk = min(out.shape[1], 256)
    for n in range(0, out.shape[1], chunk):
        total = None
        slot = 0
        for at in range(0, len(weights), inner):
            for k in range(weights[at].shape[0]):
                for turn in range(inner):
                    place = order[group, slot] * inner + lax.rem(member + turn, inner)
                    product = jnp.dot(
                        lhs[place], weights[at + turn][k, :, n : n + chunk], preferred_element_type=F32
                    )
                    total = product if total is None else total + product
                slot += 1
        out[:, n : n + chunk] = total.astype(out.dtype)


def on_device(
    tokens,
    norm_gain,
    w_query,
    w_forget,
    w_value,
    w_gate,
    lower_bound,
    head_gain,
    w_out,
    state,
    prev_forget,
    prev_value,
    accepted,
    *,
    kv,
    tp,
):
    seqs, heads, keys, vals = state.shape
    proposals = prev_forget.shape[1]
    rows = tokens.shape[0]
    width = heads * keys
    inner, ring, share = cut_of(kv, tp)

    group = lax.axis_index("kv") // inner

    def groups(pairs):
        return [(a * inner + m, b * inner + m) for a, b in pairs for m in range(inner)]

    def around(turn):
        return [(g * inner + (m + turn) % inner, g * inner + m) for g in range(ring) for m in range(inner)]

    def mirrored(size, start, stop):
        pairs = []
        for base in range(0, ring, 2 * size):
            last = base + 2 * size - 1
            pairs += [(base + start, base + stop), (last - start, last - stop)]
        return groups(pairs)

    def swap(value, bit):
        return lax.ppermute(value, "tp", [(t, t ^ bit) for t in range(tp)])

    block = w_query.shape[0]
    part = rows // share
    shapes = [jax.ShapeDtypeStruct((inner, rows, block), BF16)]
    shapes += [jax.ShapeDtypeStruct((inner, part, block), BF16)] * (ring - 1)
    shapes += [jax.ShapeDtypeStruct((block, 4 * keys), BF16)] * heads
    normed = pl.pallas_call(
        lambda *refs: norm_kernel(*refs, ring=ring, inner=inner, share=share, heads=heads),
        out_shape=shapes,
        in_specs=[VMEM, VMEM] + [HBM] * 4,
        out_specs=[VMEM] * len(shapes),
        scratch_shapes=[pltpu.VMEM(tokens.shape, BF16), pltpu.SemaphoreType.DMA((4 * heads,))],
        compiler_params=room(60),
        name="norm",
    )(tokens, norm_gain.reshape(1, -1), w_forget, w_value, w_query, w_gate)
    own, mine = normed[0], normed[1:ring]
    sets = []
    for weight in normed[ring:]:
        sets.append([weight] + [lax.ppermute(weight, "kv", around(t)) for t in range(1, inner)])
    others = []
    for r in range(1, ring):
        got = lax.ppermute(mine[r - 1], "kv", groups([(g, g ^ r) for g in range(ring)]))
        others.append(got)
        for bit in range(1, share):
            others.append(swap(got, bit))

    bounds = lower_bound.reshape(1, width)
    some = 8 if seqs % 8 == 0 else seqs
    one_spec = pl.BlockSpec((1, width), lambda i: (0, 0))
    taken = pl.pallas_call(
        lambda *refs: taken_kernel(*refs, proposals=proposals, seqs=some),
        out_shape=jax.ShapeDtypeStruct(state.shape, F32),
        in_specs=[SMEM, HBM, VMEM, VMEM, VMEM],
        out_specs=HBM,
        scratch_shapes=[
            pltpu.VMEM(state.shape, F32),
            pltpu.SemaphoreType.DMA((seqs // some,)),
            pltpu.SemaphoreType.DMA((seqs // some,)),
        ],
        compiler_params=room(48),
        name="taken",
    )(accepted, state, prev_forget, prev_value, bounds)

    def added(a, b):
        return (a.astype(F32) + b.astype(F32)).astype(BF16)

    tokens_here = []

    def summed(w, weights):
        levels = [1 << k for k in range((ring - 1).bit_length())]
        width = weights[0].shape[1]
        shapes = [jax.ShapeDtypeStruct((rows, width), F32)]
        shapes += [jax.ShapeDtypeStruct((size, rows, width), BF16) for size in levels]
        fresh = w == 0
        if fresh:
            shapes.append(jax.ShapeDtypeStruct((ring * rows, inner * block), BF16))
        operands = [own, *others, *weights] if fresh else [tokens_here[0], *weights]
        products = pl.pallas_call(
            lambda *refs: project_kernel(*refs, ring=ring, inner=inner, share=share, fresh=fresh),
            out_shape=shapes,
            in_specs=[VMEM] * len(operands),
            out_specs=[VMEM] * len(shapes),
            scratch_shapes=[pltpu.VMEM((inner * block, width), BF16)],
            compiler_params=room(16),
            name="project",
        )(*operands)
        if fresh:
            tokens_here.append(products[-1])
        pieces = [products[0]]
        held = {size: products[1 + k] for k, size in enumerate(levels)}
        for size in reversed(levels):
            out = held[size]
            for hop in range(1, size):
                got = lax.ppermute(out, "kv", mirrored(size, hop - 1, hop))
                out = added(out, got)
            got = lax.ppermute(out, "kv", mirrored(size, size - 1, size))
            pieces.append(got)
            for lower in levels:
                if lower < size:
                    start = ((group // lower) ^ 1) * lower % size
                    piece = lax.dynamic_slice_in_dim(got, start, lower, 0)
                    held[lower] = added(held[lower], piece)
        return pieces

    head_parts = [summed(w, weights) for w, weights in enumerate(sets)]

    blocks = []
    cur = w_out[None]
    size, step = 1, 0
    while size < ring:
        got = lax.ppermute(cur, "kv", mirrored(size, size - 1, size))
        step += 1
        total = got
        for hop in range(1, size):
            got = lax.ppermute(got, "kv", mirrored(size, size - hop, size - hop - 1))
            step += 1
            total = total + got
        if size == 1:
            cur = jnp.concatenate([cur, total])
            fresh = cur
        else:
            fresh = total
            if 2 * size < ring:
                cur = jnp.concatenate([cur, total])
        blocks.append(fresh)
        size *= 2
    if ring == 1:
        blocks = [cur]
    weights = []
    for fresh in blocks:
        weights += [fresh] + [lax.ppermute(fresh, "kv", around(t)) for t in range(1, inner)]

    runs = runs_of(heads)
    many = 32 if seqs % 32 == 0 else seqs
    many_rows = many * proposals
    gathered, ids = [], []
    for k, run in enumerate(runs):
        specs, arrays = [], []
        for head in run:
            for array in head_parts[head]:
                arrays.append(array)
                if array.ndim == 2:
                    specs.append(pl.BlockSpec((many_rows, 4 * keys), lambda i: (i, 0)))
                else:
                    specs.append(pl.BlockSpec((array.shape[0], many_rows, 4 * keys), lambda i: (0, i, 0)))
        parts = len(head_parts[0])
        held = len(run)
        place = run[0] // held
        last = k == len(runs) - 1
        head_out = pl.pallas_call(
            lambda *refs, held=held, first=run[0]: recur_kernel(
                *refs, parts=parts, heads=held, first=first, proposals=proposals, inner=inner
            ),
            out_shape=jax.ShapeDtypeStruct((rows, held * keys), BF16),
            grid=(seqs // many,),
            in_specs=specs
            + [pl.BlockSpec((many, held, keys, vals), lambda i, place=place: (i, place, 0, 0)), one_spec, one_spec],
            out_specs=pl.BlockSpec((many_rows, held * keys), lambda i: (i, 0)),
            compiler_params=room(40),
            name="recur",
        )(*arrays, taken, bounds, head_gain.reshape(1, width))
        pieces, ids = [head_out], [0]
        bit = tp // 2
        while bit:
            for j in range(len(ids)):
                if not last:
                    pieces.append(swap(pieces[j], bit))
                else:
                    pieces.append(swap(head_out, ids[j] ^ bit))
            ids += [i ^ bit for i in ids]
            bit //= 2
        gathered += pieces
    table = jnp.asarray(order_of(ring), jnp.int32)
    height = w_out.shape[0]
    mixed = pl.pallas_call(
        lambda *refs: mix_kernel(*refs, lanes=tp, ids=ids, runs=runs, inner=inner, keys=keys),
        out_shape=jax.ShapeDtypeStruct((rows, w_out.shape[1]), BF16),
        in_specs=[SMEM] + [VMEM] * (len(gathered) + len(weights)),
        out_specs=VMEM,
        scratch_shapes=[pltpu.VMEM((kv, rows, height), BF16)],
        compiler_params=room(12),
        name="mix",
    )(table, *gathered, *weights)
    return (mixed, taken)


def cut_of(kv, tp):
    inner = 2 if kv % 2 == 0 else 1
    return inner, kv // inner, 2 if tp % 2 == 0 else 1


def runs_of(heads):
    half = max(1, heads // 2)
    return [list(range(half))] + [[head] for head in range(half, heads)]


def order_of(ring):
    order = [[g] for g in range(ring)]
    size = 1
    while size < ring:
        order = [
            order[g] + order[(g // (2 * size)) * 2 * size + (size if g % (2 * size) < size else size - 1)]
            for g in range(ring)
        ]
        size *= 2
    return np.array(order, np.int32)


def solution(mesh):
    kv, tp = mesh.shape["kv"], mesh.shape["tp"]

    def body(*args):
        return on_device(*args, kv=kv, tp=tp)

    return jax.shard_map(
        body,
        mesh=mesh,
        in_specs=(
            P("kv", None),
            P(),
            P("kv", "tp"),
            P("kv", "tp"),
            P("kv", "tp"),
            P("kv", "tp"),
            P("tp"),
            P("tp"),
            P("kv", "tp"),
            P("kv", "tp", None, None),
            P("kv", None, "tp"),
            P("kv", None, "tp"),
            P("kv"),
        ),
        out_specs=(P("kv", "tp"), P("kv", "tp", None, None)),
        check_vma=False,
    )
```

time: 203 us -> 175 us (0.86)
  starting transfers between devices: 91.8 us -> 66.7 us
  waiting for transfers between devices: 37.4 us -> 50.9 us
  Pallas kernels: 53.1 us -> 40.4 us
  other arithmetic: 12.5 us -> 7.9 us
    ppermute x8, starting transfers between devices: 48.9 us -> 26.6 us  [summed(): got = lax.ppermute(out, 'kv', mirrored(size, size - 1, size))]
    ppermute x4, waiting for transfers between devices: 0.41 us -> 9.73 us  [on_device(): lax.ppermute(weight, 'kv', around(t))]
    pallas_call x4, Pallas kernels: 16.2 us -> 8.38 us  [summed(): pl.pallas_call(lambda *refs: project_kernel(*refs, ring=ring, inner=inner...]
    ppermute x2, waiting for transfers between devices: 0.01 us -> 7.49 us  [on_device(): got = lax.ppermute(cur, 'kv', mirrored(size, size - 1, size))]
    ppermute x3, waiting for transfers between devices: 17.2 us -> 9.84 us  [on_device(): lax.ppermute(mine[r - 1], 'kv', groups([(g, g ^ r) for g in range(ring)]))]
    ppermute x1, waiting for transfers between devices: 0.01 us -> 6.29 us  [on_device(): got = lax.ppermute(got, 'kv', mirrored(size, size - hop, size - hop - 1))]
    unnamed x40 -> x34, local copies, waits for them, and re-layouts: 1.61 us -> 7.51 us
    ppermute x4, starting transfers between devices: 21.3 us -> 15.9 us  [summed(): got = lax.ppermute(out, 'kv', mirrored(size, hop - 1, hop))]
  transfers between devices with their start and end apart: 30 -> 36, of which waited for: 9 -> 13; matrix products, arithmetic and copies ran while one was open for 8% -> 5% of each run, Pallas kernels for 22% -> 22%
where the time goes in v1:
time: 175 us; the launch traced here: 174 us
  starting transfers between devices  66.7 us (38%)
  waiting for transfers between devices  50.9 us (29%)
  Pallas kernels  40.4 us (23%)
  other arithmetic  7.9 us (5%)
  local copies, waits for them, and re-layouts  7.51 us (4%)
    ppermute x8, starting transfers between devices, summed(): got = lax.ppermute(out, 'kv', mirrored(size, size - 1, size))  26.6 us
    ppermute x4, starting transfers between devices, summed(): got = lax.ppermute(out, 'kv', mirrored(size, hop - 1, hop))  15.9 us
    pallas_call x1, Pallas kernels, on_device(): pl.pallas_call(lambda *refs: taken_kernel(*refs, proposals=proposals, seq...  14.6 us
    ppermute x4, waiting for transfers between devices, summed(): got = lax.ppermute(out, 'kv', mirrored(size, hop - 1, hop))  11.5 us
    ppermute x3, waiting for transfers between devices, on_device(): lax.ppermute(mine[r - 1], 'kv', groups([(g, g ^ r) for g in range(ring)]))  9.84 us
    ppermute x4, waiting for transfers between devices, on_device(): lax.ppermute(weight, 'kv', around(t))  9.73 us
    pallas_call x3, Pallas kernels, on_device(): pl.pallas_call(lambda *refs, held=held, first=run[0]: recur_kernel(*refs,...  9.54 us
    pallas_call x4, Pallas kernels, summed(): pl.pallas_call(lambda *refs: project_kernel(*refs, ring=ring, inner=inner...  8.38 us
  transfers between devices with their start and end apart: 36, of which 13 were waited for; matrix products, arithmetic and copies ran while one was open for 5% of the time, Pallas kernels for 22%

profile of v1, /device:TPU:0, one launch (start us, length us, event | category | flops | bytes accessed | tf_op | source)
XLA Modules:
  0.0 174.4 jit_solution(16316063207800149669)
XLA Ops:
  0.7 3.1 %collective-permute-start.31 = (bf16[1,256,1024]{2,1,0:T(8,128)(2,1)}, bf16[1,256,1024]{2,1,0:T(8,128)(2,1)S(1)}, u32[]{:S(2)}, u32[]{:S(2)}) collective-permute-start(bf16[1,256,1024]{2,1,0:T(8,128)(2,1)} %bitcast.11), channel_id=1, source_target_pairs={{0,8},{4,12},{8,0},{12,4},{16,24},{20,28},{24,16},{28,20},{1,9},{5... | collective-permute-start | bytes 1572872 | tf_op jit(solution)/shard_map/ppermute | solution.py:398
  3.8 5.1 %norm.1 = (bf16[2,256,512]{2,1,0:T(8,128)(2,1)}, bf16[2,128,512]{2,1,0:T(8,128)(2,1)}, bf16[2,128,512]{2,1,0:T(8,128)(2,1)}, bf16[2,128,512]{2,1,0:T(8,128)(2,1)...) custom-call(bf16[256,4096]{1,0:T(8,128)(2,1)} %refs_0_.3, ...), custom_call_target="tpu_custom_call" | custom-call | tf_op jit(solution)/shard_map/norm/pallas_call | solution.py:314
  9.0 3.0 %collective-permute-start.2 = (bf16[2,128,512]{2,1,0:T(8,128)(2,1)}, bf16[2,128,512]{2,1,0:T(8,128)(2,1)S(1)}, u32[]{:S(2)}, u32[]{:S(2)}) collective-permute-start(bf16[2,128,512]{2,1,0:T(8,128)(2,1)} %get-tuple-element.25), channel_id=1, source_target_pairs={{0,16},{4,20},{8,24},{12,28},{16,0},{20,4},{24,8},{28,12},{1,17},{... | collective-permute-start | bytes 786440 | tf_op jit(solution)/shard_map/ppermute | solution.py:329
  12.0 1.3 collective-permute-start.4
  13.4 1.5 collective-permute-start.6
  14.9 7.5 %collective-permute-done.31 = bf16[1,256,1024]{2,1,0:T(8,128)(2,1)S(1)} collective-permute-done((bf16[1,256,1024]{2,1,0:T(8,128)(2,1)}, bf16[1,256,1024]{2,1,0:T(8,128)(2,1)S(1)}, u32[]{:S(2)}, u32[]{:S(2)}) %collective-permute-start.31) | collective-permute-done | bytes 524320 | tf_op jit(solution)/shard_map/ppermute | solution.py:398
  22.4 1.1 pad_maximum_fusion.refs_13_
  23.5 1.7 collective-permute-start.33
  25.2 1.9 %collective-permute-done.refs_1_ = bf16[2,128,512]{2,1,0:T(8,128)(2,1)S(1)} collective-permute-done((bf16[2,128,512]{2,1,0:T(8,128)(2,1)}, bf16[2,128,512]{2,1,0:T(8,128)(2,1)S(1)}, u32[]{:S(2)}, u32[]{:S(2)}) %collective-permute-start) | collective-permute-done | bytes 262176 | tf_op jit(solution)/shard_map/ppermute | solution.py:329
  27.7 7.4 %collective-permute-done.4.refs_5_ = bf16[2,128,512]{2,1,0:T(8,128)(2,1)S(1)} collective-permute-done((bf16[2,128,512]{2,1,0:T(8,128)(2,1)}, bf16[2,128,512]{2,1,0:T(8,128)(2,1)S(1)}, u32[]{:S(2)}, u32[]{:S(2)}) %collective-permute-start.4) | collective-permute-done | bytes 262176 | tf_op jit(solution)/shard_map/ppermute | solution.py:329
  35.1 1.5 collective-permute-start.10
  37.1 1.5 collective-permute-start.24
  38.6 1.0 copy-done.7
  39.7 1.0 copy-done.8
  40.7 2.0 %project.4 = (f32[256,512]{1,0:T(8,128)S(1)}, bf16[1,256,512]{2,1,0:T(8,128)(2,1)S(1)}, bf16[2,256,512]{2,1,0:T(8,128)(2,1)}, bf16[1024,1024]{1,0:T(8,128)(2,1)S(1)}) custom-call(bf16[2,256,512]{2,1,0:T(8,128)(2,1)S(1)} %copy-done.7, bf16[2,128,512]{2,1,0:T(8,128)(2,1)S(1)} %collective-permute-done.refs_1_, ...), custom_call_target="tpu_custom_call" | custom-call | tf_op jit(solution)/shard_map/project/pallas_call | solution.py:365
  43.5 5.1 %collective-permute-start.7 = (bf16[2,256,512]{2,1,0:T(8,128)(2,1)}, bf16[2,256,512]{2,1,0:T(8,128)(2,1)}, u32[]{:S(2)}, u32[]{:S(2)}) collective-permute-start(bf16[2,256,512]{2,1,0:T(8,128)(2,1)} %get-tuple-element.29), channel_id=1, source_target_pairs={{0,8},{4,12},{24,16},{28,20},{1,9},{5,13},{25,17},{29,21},{2,10},{... | collective-permute-start | bytes 1572872 | tf_op jit(solution)/shard_map/ppermute | solution.py:381
  48.6 1.5 collective-permute-done.10.refs_2_
  50.1 1.0 copy-done.6
  51.1 1.8 %project.5 = (f32[256,512]{1,0:T(8,128)S(1)}, bf16[1,256,512]{2,1,0:T(8,128)(2,1)S(1)}, bf16[2,256,512]{2,1,0:T(8,128)(2,1)}) custom-call(bf16[1024,1024]{1,0:T(8,128)(2,1)S(1)} %get-tuple-element.31.refs_0_, bf16[512,512]{1,0:T(8,128)(2,1)S(1)} %copy-done.6, bf16[512,512]{1,0:T(8,128)(2,1)S(1)} %collective-permute-done.10.refs_2_), custom_call_target="tpu_custom_call" | custom-call | tf_op jit(solution)/shard_map/project/pallas_call | solution.py:365
  54.4 5.1 %collective-permute-start.11 = (bf16[2,256,512]{2,1,0:T(8,128)(2,1)}, bf16[2,256,512]{2,1,0:T(8,128)(2,1)}, u32[]{:S(2)}, u32[]{:S(2)}) collective-permute-start(bf16[2,256,512]{2,1,0:T(8,128)(2,1)} %get-tuple-element.34), channel_id=1, source_target_pairs={{0,8},{4,12},{24,16},{28,20},{1,9},{5,13},{25,17},{29,21},{2,10},{... | collective-permute-start | bytes 1572872 | tf_op jit(solution)/shard_map/ppermute | solution.py:381
  59.5 1.9 %collective-permute-done.17.refs_2_ = bf16[512,512]{1,0:T(8,128)(2,1)} collective-permute-done((bf16[512,512]{1,0:T(8,128)(2,1)}, bf16[512,512]{1,0:T(8,128)(2,1)}, u32[]{:S(2)}, u32[]{:S(2)}) %collective-permute-start.17) | collective-permute-done | bytes 524320 | tf_op jit(solution)/shard_map/ppermute | solution.py:326
  61.4 1.5 collective-permute-start.32
  62.9 1.0 copy-done.5
  64.0 2.3 %project.6 = (f32[256,512]{1,0:T(8,128)S(1)}, bf16[1,256,512]{2,1,0:T(8,128)(2,1)S(1)}, bf16[2,256,512]{2,1,0:T(8,128)(2,1)S(1)}) custom-call(bf16[1024,1024]{1,0:T(8,128)(2,1)S(1)} %get-tuple-element.31.refs_0_, bf16[512,512]{1,0:T(8,128)(2,1)S(1)} %copy-done.5, bf16[512,512]{1,0:T(8,128)(2,1)} %collective-permute-done.17.refs_2_), custom_call_target="tpu_custom_call" | custom-call | tf_op jit(solution)/shard_map/project/pallas_call | solution.py:365
  66.3 6.3 %collective-permute-done.24.refs_2_ = bf16[512,512]{1,0:T(8,128)(2,1)} collective-permute-done((bf16[512,512]{1,0:T(8,128)(2,1)}, bf16[512,512]{1,0:T(8,128)(2,1)}, u32[]{:S(2)}, u32[]{:S(2)}) %collective-permute-start.24) | collective-permute-done | bytes 524320 | tf_op jit(solution)/shard_map/ppermute | solution.py:326
  72.6 4.3 %collective-permute-start.18 = (bf16[2,256,512]{2,1,0:T(8,128)(2,1)S(1)}, bf16[2,256,512]{2,1,0:T(8,128)(2,1)S(1)}, u32[]{:S(2)}, u32[]{:S(2)}) collective-permute-start(bf16[2,256,512]{2,1,0:T(8,128)(2,1)S(1)} %get-tuple-element.38), channel_id=1, source_target_pairs={{0,8},{4,12},{24,16},{28,20},{1,9},{5,13},{25,17},{29,21},{2,10},{... | collective-permute-start | bytes 1572872 | tf_op jit(solution)/shard_map/ppermute | solution.py:381
  78.0 2.3 %project.7 = (f32[256,512]{1,0:T(8,128)S(1)}, bf16[1,256,512]{2,1,0:T(8,128)(2,1)S(1)}, bf16[2,256,512]{2,1,0:T(8,128)(2,1)S(1)}) custom-call(bf16[1024,1024]{1,0:T(8,128)(2,1)S(1)} %get-tuple-element.31.refs_0_, bf16[512,512]{1,0:T(8,128)(2,1)S(1)} %copy-done.4, bf16[512,512]{1,0:T(8,128)(2,1)} %collective-permute-done.24.refs_2_), custom_call_target="tpu_custom_call" | custom-call | tf_op jit(solution)/shard_map/project/pallas_call | solution.py:365
  80.3 1.3 collective-permute-start.25
  81.7 1.3 collective-permute-start.34
  83.0 1.3 add_convert_fusion.3
  85.0 1.3 add_convert_fusion.2
  86.4 2.9 %collective-permute-done.18 = bf16[2,256,512]{2,1,0:T(8,128)(2,1)S(1)} collective-permute-done((bf16[2,256,512]{2,1,0:T(8,128)(2,1)S(1)}, bf16[2,256,512]{2,1,0:T(8,128)(2,1)S(1)}, u32[]{:S(2)}, u32[]{:S(2)}) %collective-permute-start.18) | collective-permute-done | bytes 524320 | tf_op jit(solution)/shard_map/ppermute | solution.py:381
  90.1 8.6 %collective-permute-done.25 = bf16[2,256,512]{2,1,0:T(8,128)(2,1)S(1)} collective-permute-done((bf16[2,256,512]{2,1,0:T(8,128)(2,1)S(1)}, bf16[2,256,512]{2,1,0:T(8,128)(2,1)S(1)}, u32[]{:S(2)}, u32[]{:S(2)}) %collective-permute-start.25) | collective-permute-done | bytes 524320 | tf_op jit(solution)/shard_map/ppermute | solution.py:381
  101.5 6.3 %collective-permute-done.34 = bf16[2,256,1024]{2,1,0:T(8,128)(2,1)S(1)} collective-permute-done((bf16[2,256,1024]{2,1,0:T(8,128)(2,1)}, bf16[2,256,1024]{2,1,0:T(8,128)(2,1)S(1)}, u32[]{:S(2)}, u32[]{:S(2)}) %collective-permute-start.34) | collective-permute-done | bytes 1048608 | tf_op jit(solution)/shard_map/ppermute | solution.py:402
  107.8 1.5 collective-permute-start.9
  109.3 1.6 add.52.refs_15_
  110.9 1.6 collective-permute-start.35
  113.5 13.0 %collective-permute-start.13 = (bf16[1,256,512]{2,1,0:T(8,128)(2,1)S(1)}, bf16[1,256,512]{2,1,0:T(8,128)(2,1)S(1)}, u32[]{:S(2)}, u32[]{:S(2)}) collective-permute-start(bf16[1,256,512]{2,1,0:T(8,128)(2,1)S(1)} %add_convert_fusion.6), channel_id=1, source_target_pairs={{0,8},{4,12},{8,0},{12,4},{16,24},{20,28},{24,16},{28,20},{1,9},{5... | collective-permute-start | bytes 786440 | tf_op jit(solution)/shard_map/ppermute | solution.py:383
  126.6 9.1 %collective-permute-start.20 = (bf16[1,256,512]{2,1,0:T(8,128)(2,1)S(1)}, bf16[1,256,512]{2,1,0:T(8,128)(2,1)S(1)}, u32[]{:S(2)}, u32[]{:S(2)}) collective-permute-start(bf16[1,256,512]{2,1,0:T(8,128)(2,1)S(1)} %add_convert_fusion.5), channel_id=1, source_target_pairs={{0,8},{4,12},{8,0},{12,4},{16,24},{20,28},{24,16},{28,20},{1,9},{5... | collective-permute-start | bytes 786440 | tf_op jit(solution)/shard_map/ppermute | solution.py:383
  136.0 14.6 %taken.1.refs_6_.refs_3_ = f32[64,4,128,128]{3,2,1,0:T(8,128)} custom-call(s32[64]{0:T(128)S(1)} %copy-done.16, f32[64,4,128,128]{3,2,1,0:T(8,128)} %refs_1_.1, bf16[64,4,512]{2,1,0:T(4,128)(2,1)S(1)} %copy-done.9, bf16[64,4,512]{2,1,0:T(4,128)(2,1)S(1)} %copy-done.10, f32[1,512]{1,0:T(1,128)S(1)} %bitcast.4), custom_call_target="tpu_custom_call" | custom-call | tf_op jit(solution)/shard_map/taken/pallas_call | solution.py:337
  150.7 4.2 %recur.3.refs_1_ = bf16[256,256]{1,0:T(8,128)(2,1)S(1)} custom-call(f32[256,512]{1,0:T(8,128)S(1)} %copy-done.1, bf16[2,256,512]{2,1,0:T(8,128)(2,1)S(1)} %collective-permute-done.8.refs_1_, bf16[1,256,512]{2,1,0:T(8,128)(2,1)S(1)} %collective-permute-done.9.refs_2_, f32[256,512]{1,0:T(8,128)S(1)} %copy-done.3, ...), custom_call_target="tpu_custom_call" | custom-call | tf_op jit(solution)/shard_map/recur/pallas_call | solution.py:437
  154.9 1.6 collective-permute-start.14
  156.4 2.7 %recur.4.refs_5_ = bf16[256,128]{1,0:T(8,128)(2,1)S(1)} custom-call(f32[256,512]{1,0:T(8,128)S(1)} %get-tuple-element.37.refs_0_, bf16[2,256,512]{2,1,0:T(8,128)(2,1)S(1)} %collective-permute-done.19.refs_1_, bf16[1,256,512]{2,1,0:T(8,128)(2,1)S(1)} %collective-permute-done.20.refs_2_, f32[64,4,128,128]{3,2,1,0:T(8,128)} %taken.1.refs_6_.refs_3_, ...), custom_call_target="tpu_custom_call" | custom-call | tf_op jit(solution)/shard_map/recur/pallas_call | solution.py:437
  159.7 2.7 %recur.5.refs_9_ = bf16[256,128]{1,0:T(8,128)(2,1)S(1)} custom-call(f32[256,512]{1,0:T(8,128)S(1)} %get-tuple-element.41.refs_0_, bf16[2,256,512]{2,1,0:T(8,128)(2,1)S(1)} %collective-permute-done.26.refs_1_, bf16[1,256,512]{2,1,0:T(8,128)(2,1)S(1)} %collective-permute-done.27.refs_2_, f32[64,4,128,128]{3,2,1,0:T(8,128)} %taken.1.refs_6_.refs_3_, ...), custom_call_target="tpu_custom_call" | custom-call | tf_op jit(solution)/shard_map/recur/pallas_call | solution.py:437
  165.0 2.7 %collective-permute-done.28.refs_10_ = bf16[256,128]{1,0:T(8,128)(2,1)S(1)} collective-permute-done((bf16[256,128]{1,0:T(8,128)(2,1)S(1)}, bf16[256,128]{1,0:T(8,128)(2,1)S(1)}, u32[]{:S(2)}, u32[]{:S(2)}) %collective-permute-start.28) | collective-permute-done | bytes 65568 | tf_op jit(solution)/shard_map/ppermute | solution.py:307
  167.7 1.1 collective-permute-start.23
  168.9 2.8 %collective-permute-done.30.refs_12_ = bf16[256,128]{1,0:T(8,128)(2,1)S(1)} collective-permute-done((bf16[256,128]{1,0:T(8,128)(2,1)S(1)}, bf16[256,128]{1,0:T(8,128)(2,1)S(1)}, u32[]{:S(2)}, u32[]{:S(2)}) %collective-permute-start.30) | collective-permute-done | bytes 65568 | tf_op jit(solution)/shard_map/ppermute | solution.py:307
  171.7 2.7 %mix.1 = bf16[256,1024]{1,0:T(8,128)(2,1)} custom-call(s32[4,4]{1,0:T(4,128)S(1)} %copy-done.15, bf16[256,256]{1,0:T(8,128)(2,1)S(1)} %recur.3.refs_1_, bf16[256,256]{1,0:T(8,128)(2,1)S(1)} %collective-permute-done.14.refs_2_, bf16[256,256]{1,0:T(8,128)(2,1)S(1)} %collective-permute-done.15.refs_3_, bf16[256,256]{1,0:T(8,128)(2,1)S(1)} %collective-permute-done.16.refs_4_, ...), custom_call_target="tpu_custom_call" | custom-call | tf_op jit(solution)/shard_map/mix/pallas_call | solution.py:462
  (78 shorter events, 13.2 us)
Async XLA Ops:
  0.6 135.3 %copy-start.16 = (s32[64]{0:T(128)S(1)}, s32[64]{0:T(128)}, u32[]{:S(2)}) copy-start(s32[64]{0:T(128)} %refs_0_.4) | copy-start | bytes 772
  0.6 135.3 %copy-start.9 = (bf16[64,4,512]{2,1,0:T(4,128)(2,1)S(1)}, bf16[64,4,512]{2,1,0:T(4,128)(2,1)}, u32[]{:S(2)}) copy-start(bf16[64,4,512]{2,1,0:T(4,128)(2,1)} %refs_2_.3) | copy-start | bytes 786436
  0.7 135.3 %copy-start.13 = (f32[512]{0:T(512)S(1)}, f32[512]{0:T(512)}, u32[]{:S(2)}) copy-start(f32[512]{0:T(512)} %param.20) | copy-start | bytes 6148
  0.7 21.7 %collective-permute-start.31 = (bf16[1,256,1024]{2,1,0:T(8,128)(2,1)}, bf16[1,256,1024]{2,1,0:T(8,128)(2,1)S(1)}, u32[]{:S(2)}, u32[]{:S(2)}) collective-permute-start(bf16[1,256,1024]{2,1,0:T(8,128)(2,1)} %bitcast.11), channel_id=1, source_target_pairs={{0,8},{4,12},{8,0},{12,4},{16,24},{20,28},{24,16},{28,20},{1,9},{5... | collective-permute-start | bytes 1572872 | tf_op jit(solution)/shard_map/ppermute | solution.py:398
  8.9 18.2 %collective-permute-start = (bf16[2,128,512]{2,1,0:T(8,128)(2,1)}, bf16[2,128,512]{2,1,0:T(8,128)(2,1)S(1)}, u32[]{:S(2)}, u32[]{:S(2)}) collective-permute-start(bf16[2,128,512]{2,1,0:T(8,128)(2,1)} %get-tuple-element.24), channel_id=1, source_target_pairs={{0,8},{4,12},{8,0},{12,4},{16,24},{20,28},{24,16},{28,20},{1,9},{5... | collective-permute-start | bytes 786440 | tf_op jit(solution)/shard_map/ppermute | solution.py:329
  9.0 18.7 %collective-permute-start.2 = (bf16[2,128,512]{2,1,0:T(8,128)(2,1)}, bf16[2,128,512]{2,1,0:T(8,128)(2,1)S(1)}, u32[]{:S(2)}, u32[]{:S(2)}) collective-permute-start(bf16[2,128,512]{2,1,0:T(8,128)(2,1)} %get-tuple-element.25), channel_id=1, source_target_pairs={{0,16},{4,20},{8,24},{12,28},{16,0},{20,4},{24,8},{28,12},{1,17},{... | collective-permute-start | bytes 786440 | tf_op jit(solution)/shard_map/ppermute | solution.py:329
  12.0 23.0 %collective-permute-start.4 = (bf16[2,128,512]{2,1,0:T(8,128)(2,1)}, bf16[2,128,512]{2,1,0:T(8,128)(2,1)S(1)}, u32[]{:S(2)}, u32[]{:S(2)}) collective-permute-start(bf16[2,128,512]{2,1,0:T(8,128)(2,1)} %get-tuple-element.26), channel_id=1, source_target_pairs={{0,24},{4,28},{8,16},{12,20},{16,8},{20,12},{24,0},{28,4},{1,25},{... | collective-permute-start | bytes 786440 | tf_op jit(solution)/shard_map/ppermute | solution.py:329
  13.4 25.2 %collective-permute-start.6 = (bf16[512,512]{1,0:T(8,128)(2,1)}, bf16[512,512]{1,0:T(8,128)(2,1)S(1)}, u32[]{:S(2)}, u32[]{:S(2)}) collective-permute-start(bf16[512,512]{1,0:T(8,128)(2,1)} %get-tuple-element.27.refs_7_), channel_id=1, source_target_pairs={{4,0},{0,4},{12,8},{8,12},{20,16},{16,20},{28,24},{24,28},{5,1},{1... | collective-permute-start | bytes 1572872 | tf_op jit(solution)/shard_map/ppermute | solution.py:326
  23.5 58.1 %collective-permute-start.33 = (bf16[2,256,1024]{2,1,0:T(8,128)(2,1)S(1)}, bf16[2,256,1024]{2,1,0:T(8,128)(2,1)}, u32[]{:S(2)}, u32[]{:S(2)}) collective-permute-start(bf16[2,256,1024]{2,1,0:T(8,128)(2,1)S(1)} %pad_maximum_fusion.refs_13_), channel_id=1, source_target_pairs={{8,16},{12,20},{16,8},{20,12},{9,17},{13,21},{17,9},{21,13},{10,18... | collective-permute-start | bytes 3145736 | tf_op jit(solution)/shard_map/ppermute | solution.py:398
  27.2 7.9 %collective-permute-start.1 = (bf16[2,128,512]{2,1,0:T(8,128)(2,1)S(1)}, bf16[2,128,512]{2,1,0:T(8,128)(2,1)S(1)}, u32[]{:S(2)}, u32[]{:S(2)}) collective-permute-start(bf16[2,128,512]{2,1,0:T(8,128)(2,1)S(1)} %collective-permute-done.refs_1_), channel_id=1, source_target_pairs={{0,1},{1,0},{2,3},{3,2},{4,5},{5,4},{6,7},{7,6},{8,9},{9,8},{10,11... | collective-permute-start | bytes 786440 | tf_op jit(solution)/shard_map/ppermute | solution.py:307
  27.7 8.9 %collective-permute-start.3 = (bf16[2,128,512]{2,1,0:T(8,128)(2,1)S(1)}, bf16[2,128,512]{2,1,0:T(8,128)(2,1)S(1)}, u32[]{:S(2)}, u32[]{:S(2)}) collective-permute-start(bf16[2,128,512]{2,1,0:T(8,128)(2,1)S(1)} %collective-permute-done.2.refs_3_), channel_id=1, source_target_pairs={{0,1},{1,0},{2,3},{3,2},{4,5},{5,4},{6,7},{7,6},{8,9},{9,8},{10,11... | collective-permute-start | bytes 786440 | tf_op jit(solution)/shard_map/ppermute | solution.py:307
  35.1 2.0 %collective-permute-start.5 = (bf16[2,128,512]{2,1,0:T(8,128)(2,1)S(1)}, bf16[2,128,512]{2,1,0:T(8,128)(2,1)S(1)}, u32[]{:S(2)}, u32[]{:S(2)}) collective-permute-start(bf16[2,128,512]{2,1,0:T(8,128)(2,1)S(1)} %collective-permute-done.4.refs_5_), channel_id=1, source_target_pairs={{0,1},{1,0},{2,3},{3,2},{4,5},{5,4},{6,7},{7,6},{8,9},{9,8},{10,11... | collective-permute-start | bytes 786440 | tf_op jit(solution)/shard_map/ppermute | solution.py:307
  35.1 15.0 %collective-permute-start.10 = (bf16[512,512]{1,0:T(8,128)(2,1)}, bf16[512,512]{1,0:T(8,128)(2,1)S(1)}, u32[]{:S(2)}, u32[]{:S(2)}) collective-permute-start(bf16[512,512]{1,0:T(8,128)(2,1)} %get-tuple-element.32.refs_1_), channel_id=1, source_target_pairs={{4,0},{0,4},{12,8},{8,12},{20,16},{16,20},{28,24},{24,28},{5,1},{1... | collective-permute-start | bytes 1572872 | tf_op jit(solution)/shard_map/ppermute | solution.py:326
  36.6 24.8 %collective-permute-start.17 = (bf16[512,512]{1,0:T(8,128)(2,1)}, bf16[512,512]{1,0:T(8,128)(2,1)}, u32[]{:S(2)}, u32[]{:S(2)}) collective-permute-start(bf16[512,512]{1,0:T(8,128)(2,1)} %get-tuple-element.36.refs_1_), channel_id=1, source_target_pairs={{4,0},{0,4},{12,8},{8,12},{20,16},{16,20},{28,24},{24,28},{5,1},{1... | collective-permute-start | bytes 1572872 | tf_op jit(solution)/shard_map/ppermute | solution.py:326
  37.1 35.5 %collective-permute-start.24 = (bf16[512,512]{1,0:T(8,128)(2,1)}, bf16[512,512]{1,0:T(8,128)(2,1)}, u32[]{:S(2)}, u32[]{:S(2)}) collective-permute-start(bf16[512,512]{1,0:T(8,128)(2,1)} %get-tuple-element.40.refs_1_), channel_id=1, source_target_pairs={{4,0},{0,4},{12,8},{8,12},{20,16},{16,20},{28,24},{24,28},{5,1},{1... | collective-permute-start | bytes 1572872 | tf_op jit(solution)/shard_map/ppermute | solution.py:326
  38.6 1.0 copy-start.7
  43.5 9.4 %copy-start.11 = (bf16[1,256,512]{2,1,0:T(8,128)(2,1)}, bf16[1,256,512]{2,1,0:T(8,128)(2,1)S(1)}, u32[]{:S(2)}) copy-start(bf16[1,256,512]{2,1,0:T(8,128)(2,1)S(1)} %get-tuple-element.30) | copy-start | bytes 786436
  43.5 36.9 %collective-permute-start.7 = (bf16[2,256,512]{2,1,0:T(8,128)(2,1)}, bf16[2,256,512]{2,1,0:T(8,128)(2,1)}, u32[]{:S(2)}, u32[]{:S(2)}) collective-permute-start(bf16[2,256,512]{2,1,0:T(8,128)(2,1)} %get-tuple-element.29), channel_id=1, source_target_pairs={{0,8},{4,12},{24,16},{28,20},{1,9},{5,13},{25,17},{29,21},{2,10},{... | collective-permute-start | bytes 1572872 | tf_op jit(solution)/shard_map/ppermute | solution.py:381
  50.1 1.0 copy-start.6
  54.4 29.9 %collective-permute-start.11 = (bf16[2,256,512]{2,1,0:T(8,128)(2,1)}, bf16[2,256,512]{2,1,0:T(8,128)(2,1)}, u32[]{:S(2)}, u32[]{:S(2)}) collective-permute-start(bf16[2,256,512]{2,1,0:T(8,128)(2,1)} %get-tuple-element.34), channel_id=1, source_target_pairs={{0,8},{4,12},{24,16},{28,20},{1,9},{5,13},{25,17},{29,21},{2,10},{... | collective-permute-start | bytes 1572872 | tf_op jit(solution)/shard_map/ppermute | solution.py:381
  61.4 101.0 %collective-permute-start.32 = (bf16[2,256,1024]{2,1,0:T(8,128)(2,1)S(1)}, bf16[2,256,1024]{2,1,0:T(8,128)(2,1)S(1)}, u32[]{:S(2)}, u32[]{:S(2)}) collective-permute-start(bf16[2,256,1024]{2,1,0:T(8,128)(2,1)S(1)} %pad_maximum_fusion.refs_13_), channel_id=1, source_target_pairs={{4,0},{0,4},{12,8},{8,12},{20,16},{16,20},{28,24},{24,28},{5,1},{1... | collective-permute-start | bytes 3145736 | tf_op jit(solution)/shard_map/ppermute | solution.py:418
  64.0 72.0 %copy-start.10 = (bf16[64,4,512]{2,1,0:T(4,128)(2,1)S(1)}, bf16[64,4,512]{2,1,0:T(4,128)(2,1)}, u32[]{:S(2)}) copy-start(bf16[64,4,512]{2,1,0:T(4,128)(2,1)} %refs_3_.3) | copy-start | bytes 786436
  72.6 16.6 %collective-permute-start.18 = (bf16[2,256,512]{2,1,0:T(8,128)(2,1)S(1)}, bf16[2,256,512]{2,1,0:T(8,128)(2,1)S(1)}, u32[]{:S(2)}, u32[]{:S(2)}) collective-permute-start(bf16[2,256,512]{2,1,0:T(8,128)(2,1)S(1)} %get-tuple-element.38), channel_id=1, source_target_pairs={{0,8},{4,12},{24,16},{28,20},{1,9},{5,13},{25,17},{29,21},{2,10},{... | collective-permute-start | bytes 1572872 | tf_op jit(solution)/shard_map/ppermute | solution.py:381
  77.0 1.0 copy-start.4
  80.3 18.4 %collective-permute-start.25 = (bf16[2,256,512]{2,1,0:T(8,128)(2,1)S(1)}, bf16[2,256,512]{2,1,0:T(8,128)(2,1)S(1)}, u32[]{:S(2)}, u32[]{:S(2)}) collective-permute-start(bf16[2,256,512]{2,1,0:T(8,128)(2,1)S(1)} %get-tuple-element.42), channel_id=1, source_target_pairs={{0,8},{4,12},{24,16},{28,20},{1,9},{5,13},{25,17},{29,21},{2,10},{... | collective-permute-start | bytes 1572872 | tf_op jit(solution)/shard_map/ppermute | solution.py:381
  81.7 26.1 %collective-permute-start.34 = (bf16[2,256,1024]{2,1,0:T(8,128)(2,1)}, bf16[2,256,1024]{2,1,0:T(8,128)(2,1)S(1)}, u32[]{:S(2)}, u32[]{:S(2)}) collective-permute-start(bf16[2,256,1024]{2,1,0:T(8,128)(2,1)} %collective-permute-done.33), channel_id=1, source_target_pairs={{8,0},{12,4},{16,24},{20,28},{9,1},{13,5},{17,25},{21,29},{10,2},{... | collective-permute-start | bytes 3145736 | tf_op jit(solution)/shard_map/ppermute | solution.py:402
  84.3 15.2 %collective-permute-start.8 = (bf16[2,256,512]{2,1,0:T(8,128)(2,1)S(1)}, bf16[2,256,512]{2,1,0:T(8,128)(2,1)S(1)}, u32[]{:S(2)}, u32[]{:S(2)}) collective-permute-start(bf16[2,256,512]{2,1,0:T(8,128)(2,1)S(1)} %add_convert_fusion.3), channel_id=1, source_target_pairs={{8,16},{12,20},{16,8},{20,12},{9,17},{13,21},{17,9},{21,13},{10,18... | collective-permute-start | bytes 1572872 | tf_op jit(solution)/shard_map/ppermute | solution.py:383
  89.3 21.7 %collective-permute-start.12 = (bf16[2,256,512]{2,1,0:T(8,128)(2,1)S(1)}, bf16[2,256,512]{2,1,0:T(8,128)(2,1)S(1)}, u32[]{:S(2)}, u32[]{:S(2)}) collective-permute-start(bf16[2,256,512]{2,1,0:T(8,128)(2,1)S(1)} %add_convert_fusion.2), channel_id=1, source_target_pairs={{8,16},{12,20},{16,8},{20,12},{9,17},{13,21},{17,9},{21,13},{10,18... | collective-permute-start | bytes 1572872 | tf_op jit(solution)/shard_map/ppermute | solution.py:383
  98.7 14.8 %collective-permute-start.19 = (bf16[2,256,512]{2,1,0:T(8,128)(2,1)S(1)}, bf16[2,256,512]{2,1,0:T(8,128)(2,1)S(1)}, u32[]{:S(2)}, u32[]{:S(2)}) collective-permute-start(bf16[2,256,512]{2,1,0:T(8,128)(2,1)S(1)} %add_convert_fusion.1), channel_id=1, source_target_pairs={{8,16},{12,20},{16,8},{20,12},{9,17},{13,21},{17,9},{21,13},{10,18... | collective-permute-start | bytes 1572872 | tf_op jit(solution)/shard_map/ppermute | solution.py:383
  99.6 27.1 %collective-permute-start.26 = (bf16[2,256,512]{2,1,0:T(8,128)(2,1)S(1)}, bf16[2,256,512]{2,1,0:T(8,128)(2,1)S(1)}, u32[]{:S(2)}, u32[]{:S(2)}) collective-permute-start(bf16[2,256,512]{2,1,0:T(8,128)(2,1)S(1)} %add_convert_fusion), channel_id=1, source_target_pairs={{8,16},{12,20},{16,8},{20,12},{9,17},{13,21},{17,9},{21,13},{10,18... | collective-permute-start | bytes 1572872 | tf_op jit(solution)/shard_map/ppermute | solution.py:383
  107.8 28.1 %collective-permute-start.9 = (bf16[1,256,512]{2,1,0:T(8,128)(2,1)S(1)}, bf16[1,256,512]{2,1,0:T(8,128)(2,1)S(1)}, u32[]{:S(2)}, u32[]{:S(2)}) collective-permute-start(bf16[1,256,512]{2,1,0:T(8,128)(2,1)S(1)} %add_convert_fusion.7), channel_id=1, source_target_pairs={{0,8},{4,12},{8,0},{12,4},{16,24},{20,28},{24,16},{28,20},{1,9},{5... | collective-permute-start | bytes 786440 | tf_op jit(solution)/shard_map/ppermute | solution.py:383
  110.9 60.8 %collective-permute-start.35 = (bf16[2,256,1024]{2,1,0:T(8,128)(2,1)S(1)}, bf16[2,256,1024]{2,1,0:T(8,128)(2,1)S(1)}, u32[]{:S(2)}, u32[]{:S(2)}) collective-permute-start(bf16[2,256,1024]{2,1,0:T(8,128)(2,1)S(1)} %add.52.refs_15_), channel_id=1, source_target_pairs={{4,0},{0,4},{12,8},{8,12},{20,16},{16,20},{28,24},{24,28},{5,1},{1... | collective-permute-start | bytes 3145736 | tf_op jit(solution)/shard_map/ppermute | solution.py:418
  113.5 37.1 %collective-permute-start.13 = (bf16[1,256,512]{2,1,0:T(8,128)(2,1)S(1)}, bf16[1,256,512]{2,1,0:T(8,128)(2,1)S(1)}, u32[]{:S(2)}, u32[]{:S(2)}) collective-permute-start(bf16[1,256,512]{2,1,0:T(8,128)(2,1)S(1)} %add_convert_fusion.6), channel_id=1, source_target_pairs={{0,8},{4,12},{8,0},{12,4},{16,24},{20,28},{24,16},{28,20},{1,9},{5... | collective-permute-start | bytes 786440 | tf_op jit(solution)/shard_map/ppermute | solution.py:383
  126.6 29.8 %collective-permute-start.20 = (bf16[1,256,512]{2,1,0:T(8,128)(2,1)S(1)}, bf16[1,256,512]{2,1,0:T(8,128)(2,1)S(1)}, u32[]{:S(2)}, u32[]{:S(2)}) collective-permute-start(bf16[1,256,512]{2,1,0:T(8,128)(2,1)S(1)} %add_convert_fusion.5), channel_id=1, source_target_pairs={{0,8},{4,12},{8,0},{12,4},{16,24},{20,28},{24,16},{28,20},{1,9},{5... | collective-permute-start | bytes 786440 | tf_op jit(solution)/shard_map/ppermute | solution.py:383
  135.8 23.9 %collective-permute-start.27 = (bf16[1,256,512]{2,1,0:T(8,128)(2,1)S(1)}, bf16[1,256,512]{2,1,0:T(8,128)(2,1)S(1)}, u32[]{:S(2)}, u32[]{:S(2)}) collective-permute-start(bf16[1,256,512]{2,1,0:T(8,128)(2,1)S(1)} %add_convert_fusion.4), channel_id=1, source_target_pairs={{0,8},{4,12},{8,0},{12,4},{16,24},{20,28},{24,16},{28,20},{1,9},{5... | collective-permute-start | bytes 786440 | tf_op jit(solution)/shard_map/ppermute | solution.py:383
  135.9 14.7 %copy-start.1 = (f32[256,512]{1,0:T(8,128)S(1)}, f32[256,512]{1,0:T(8,128)}, u32[]{:S(2)}) copy-start(f32[256,512]{1,0:T(8,128)} %copy-done) | copy-start | bytes 1572868
  135.9 14.7 %copy-start.3 = (f32[256,512]{1,0:T(8,128)S(1)}, f32[256,512]{1,0:T(8,128)}, u32[]{:S(2)}) copy-start(f32[256,512]{1,0:T(8,128)} %copy-done.2) | copy-start | bytes 1572868
  136.0 14.7 %copy-start.14 = (f32[512]{0:T(512)S(1)}, f32[512]{0:T(512)}, u32[]{:S(2)}) copy-start(f32[512]{0:T(512)} %param.21) | copy-start | bytes 6148
  154.9 9.6 %collective-permute-start.14 = (bf16[256,256]{1,0:T(8,128)(2,1)S(1)}, bf16[256,256]{1,0:T(8,128)(2,1)S(1)}, u32[]{:S(2)}, u32[]{:S(2)}) collective-permute-start(bf16[256,256]{1,0:T(8,128)(2,1)S(1)} %recur.3.refs_1_), channel_id=1, source_target_pairs={{0,2},{1,3},{2,0},{3,1},{4,6},{5,7},{6,4},{7,5},{8,10},{9,11},{10,... | collective-permute-start | bytes 393224 | tf_op jit(solution)/shard_map/ppermute | solution.py:307
  156.4 15.3 %copy-start.15 = (s32[4,4]{1,0:T(4,128)S(1)}, s32[4,4]{1,0:T(4,128)}, u32[]{:S(2)}) copy-start(s32[4,4]{1,0:T(4,128)} %constant.54.clone.refs_0_) | copy-start | bytes 196
  159.1 4.3 %collective-permute-start.21 = (bf16[256,128]{1,0:T(8,128)(2,1)S(1)}, bf16[256,128]{1,0:T(8,128)(2,1)S(1)}, u32[]{:S(2)}, u32[]{:S(2)}) collective-permute-start(bf16[256,128]{1,0:T(8,128)(2,1)S(1)} %recur.4.refs_5_), channel_id=1, source_target_pairs={{0,2},{1,3},{2,0},{3,1},{4,6},{5,7},{6,4},{7,5},{8,10},{9,11},{10,... | collective-permute-start | bytes 196616 | tf_op jit(solution)/shard_map/ppermute | solution.py:307
  159.7 4.8 %collective-permute-start.22 = (bf16[256,128]{1,0:T(8,128)(2,1)S(1)}, bf16[256,128]{1,0:T(8,128)(2,1)S(1)}, u32[]{:S(2)}, u32[]{:S(2)}) collective-permute-start(bf16[256,128]{1,0:T(8,128)(2,1)S(1)} %recur.4.refs_5_), channel_id=1, source_target_pairs={{0,1},{1,0},{2,3},{3,2},{4,5},{5,4},{6,7},{7,6},{8,9},{9,8},{10,11... | collective-permute-start | bytes 196616 | tf_op jit(solution)/shard_map/ppermute | solution.py:307
  162.4 9.3 %collective-permute-start.15 = (bf16[256,256]{1,0:T(8,128)(2,1)S(1)}, bf16[256,256]{1,0:T(8,128)(2,1)S(1)}, u32[]{:S(2)}, u32[]{:S(2)}) collective-permute-start(bf16[256,256]{1,0:T(8,128)(2,1)S(1)} %recur.3.refs_1_), channel_id=1, source_target_pairs={{0,1},{1,0},{2,3},{3,2},{4,5},{5,4},{6,7},{7,6},{8,9},{9,8},{10,11... | collective-permute-start | bytes 393224 | tf_op jit(solution)/shard_map/ppermute | solution.py:307
  163.4 4.3 %collective-permute-start.28 = (bf16[256,128]{1,0:T(8,128)(2,1)S(1)}, bf16[256,128]{1,0:T(8,128)(2,1)S(1)}, u32[]{:S(2)}, u32[]{:S(2)}) collective-permute-start(bf16[256,128]{1,0:T(8,128)(2,1)S(1)} %recur.5.refs_9_), channel_id=1, source_target_pairs={{0,2},{1,3},{2,0},{3,1},{4,6},{5,7},{6,4},{7,5},{8,10},{9,11},{10,... | collective-permute-start | bytes 196616 | tf_op jit(solution)/shard_map/ppermute | solution.py:307
  164.5 3.2 %collective-permute-start.29 = (bf16[256,128]{1,0:T(8,128)(2,1)S(1)}, bf16[256,128]{1,0:T(8,128)(2,1)S(1)}, u32[]{:S(2)}, u32[]{:S(2)}) collective-permute-start(bf16[256,128]{1,0:T(8,128)(2,1)S(1)} %recur.5.refs_9_), channel_id=1, source_target_pairs={{0,1},{1,0},{2,3},{3,2},{4,5},{5,4},{6,7},{7,6},{8,9},{9,8},{10,11... | collective-permute-start | bytes 196616 | tf_op jit(solution)/shard_map/ppermute | solution.py:307
  164.5 7.2 %collective-permute-start.16 = (bf16[256,256]{1,0:T(8,128)(2,1)S(1)}, bf16[256,256]{1,0:T(8,128)(2,1)S(1)}, u32[]{:S(2)}, u32[]{:S(2)}) collective-permute-start(bf16[256,256]{1,0:T(8,128)(2,1)S(1)} %collective-permute-done.14.refs_2_), channel_id=1, source_target_pairs={{0,1},{1,0},{2,3},{3,2},{4,5},{5,4},{6,7},{7,6},{8,9},{9,8},{10,11... | collective-permute-start | bytes 393224 | tf_op jit(solution)/shard_map/ppermute | solution.py:307
  167.7 4.0 %collective-permute-start.30 = (bf16[256,128]{1,0:T(8,128)(2,1)S(1)}, bf16[256,128]{1,0:T(8,128)(2,1)S(1)}, u32[]{:S(2)}, u32[]{:S(2)}) collective-permute-start(bf16[256,128]{1,0:T(8,128)(2,1)S(1)} %recur.5.refs_9_), channel_id=1, source_target_pairs={{0,3},{1,2},{2,1},{3,0},{4,7},{5,6},{6,5},{7,4},{8,11},{9,10},{10,... | collective-permute-start | bytes 196616 | tf_op jit(solution)/shard_map/ppermute | solution.py:307
  167.7 4.0 %collective-permute-start.23 = (bf16[256,128]{1,0:T(8,128)(2,1)S(1)}, bf16[256,128]{1,0:T(8,128)(2,1)S(1)}, u32[]{:S(2)}, u32[]{:S(2)}) collective-permute-start(bf16[256,128]{1,0:T(8,128)(2,1)S(1)} %collective-permute-done.21.refs_6_), channel_id=1, source_target_pairs={{0,1},{1,0},{2,3},{3,2},{4,5},{5,4},{6,7},{7,6},{8,9},{9,8},{10,11... | collective-permute-start | bytes 196616 | tf_op jit(solution)/shard_map/ppermute | solution.py:307
  (5 other events, 4.4 us)

commit v2 on v1

--- a/solution.py
+++ b/solution.py
@@ -15,6 +15,10 @@
 HBM = pl.BlockSpec(memory_space=pltpu.MemorySpace.HBM)
 
 
+def in_hbm(*arrays):
+    return [pltpu.with_memory_space_constraint(array, pltpu.MemorySpace.HBM) for array in arrays]
+
+
 def room(mib):
     return pltpu.CompilerParams(vmem_limit_bytes=mib << 20)
 
@@ -25,7 +29,7 @@
 
 def norm_kernel(tokens, gain, *refs, ring, inner, share, heads):
     weights, own, mine = refs[:4], refs[4], refs[5 : 4 + ring]
-    pieces, (scratch, sems) = refs[4 + ring : -2], refs[-2:]
+    pieces, (raw, scratch, sems, come) = refs[4 + ring : -4], refs[-4:]
     keys = weights[0].shape[1] // heads
     copies = [
         pltpu.make_async_copy(
@@ -36,10 +40,16 @@
         for head in range(heads)
         for k in range(4)
     ]
-    for copy in copies:
-        copy.start()
     rows, width = tokens.shape
     step = 16
+    lots = come.shape[0]
+    fetches = [
+        pltpu.make_async_copy(tokens.at[here], raw.at[here], come.at[lot])
+        for lot in range(lots)
+        for here in [pl.ds(lot * (rows // lots), rows // lots)]
+    ]
+    for copy in fetches + copies:
+        copy.start()
     block = own.shape[-1]
     part = rows // share
     chunk = min(width, 512)
@@ -48,17 +58,20 @@
         here = pl.ds(pl.multiple_of(i * step, step), step)
         total = jnp.zeros((step, 128), F32)
         for at in range(0, width, chunk):
-            x = tokens[here, at : at + chunk].astype(F32)
+            x = raw[here, at : at + chunk].astype(F32)
             x = x * x
             for k in range(0, chunk, 128):
                 total = total + x[:, k : k + 128]
         scale = lax.rsqrt(jnp.sum(total, axis=-1, keepdims=True) / width + EPSILON)
         for at in range(0, width, chunk):
-            x = tokens[here, at : at + chunk].astype(F32)
+            x = raw[here, at : at + chunk].astype(F32)
             scratch[here, at : at + chunk] = (x * scale * gain[:, at : at + chunk]).astype(BF16)
         return carry
 
-    lax.fori_loop(0, rows // step, one, 0, unroll=4)
+    for lot in range(lots):
+        fetches[lot].wait()
+        first = lot * (rows // lots) // step
+        lax.fori_loop(first, first + rows // lots // step, one, 0, unroll=4)
     me, lane = lax.axis_index("kv"), lax.axis_index("tp")
     group, member = lax.div(me, inner), lax.rem(me, inner)
     here = pl.ds(pl.multiple_of(lax.rem(lane, share) * part, part), part)
@@ -116,7 +129,9 @@
     return lax.rem(lax.broadcasted_iota(jnp.int32, shape, 0), proposals)
 
 
-def taken_kernel(accepted, state, forget, values, bounds, taken, held, come, gone, *, proposals, seqs):
+def taken_kernel(
+    accepted, state, prev_forget, prev_value, bounds, taken, held, forget, values, come, gone, side, *, proposals, seqs
+):
     count, heads, keys, vals = state.shape
     steps = count // seqs
     rows = seqs * proposals
@@ -131,11 +146,25 @@
         here = pl.ds(i * seqs, seqs)
         return pltpu.make_async_copy(held.at[here], taken.at[here], gone.at[i])
 
-    for i in range(steps):
+    fetches = [
+        pltpu.make_async_copy(prev_forget, forget, side.at[0]),
+        pltpu.make_async_copy(prev_value, values, side.at[1]),
+    ]
+    for copy in fetches:
+        copy.start()
+    ahead = min(3, steps)
+    for i in range(ahead):
         copy_in(i).start()
+    for copy in fetches:
+        copy.wait()
 
     def one(i, carry):
         first = i * seqs
+
+        @pl.when(i + ahead < steps)
+        def _():
+            copy_in(i + ahead).start()
+
         old = jnp.concatenate([forget[first + seq].astype(F32) for seq in range(seqs)], axis=0)
         new = jnp.concatenate([values[first + seq].astype(F32) for seq in range(seqs)], axis=0).astype(BF16)
         taking = jnp.zeros((rows, keys), jnp.int32)
@@ -148,9 +177,9 @@
             gate = forget_of(old[:, cols], bounds[:, cols])
             decay = jnp.where(kept, gate, 1.0)
             after = jnp.ones_like(decay)
-            for ahead in range(1, proposals):
-                moved = pltpu.roll(decay, rows - ahead, axis=0)
-                after = after * jnp.where(position < proposals - ahead, moved, 1.0)
+            for lead in range(1, proposals):
+                moved = pltpu.roll(decay, rows - lead, axis=0)
+                after = after * jnp.where(position < proposals - lead, moved, 1.0)
             decays.append((decay * after).T)
             weight = (jnp.where(kept, 1.0 - gate, 0.0) * after).T
             high = weight.astype(BF16)
@@ -182,9 +211,16 @@
         copy_out(i).wait()
 
 
-def recur_kernel(*refs, parts, heads, first, proposals, inner):
-    pieces = refs[: parts * heads]
-    taken, bounds, gain, out = refs[parts * heads :]
+def recur_kernel(*refs, parts, head, proposals, inner, spare):
+    pieces, (taken, bounds, gain) = refs[:parts], refs[parts : parts + 3]
+    rest = refs[parts + 3 :]
+    if spare:
+        last, *rest = rest
+        *rest, ready = rest
+        ready[...] = last[...].astype(BF16)
+    out = rest[-1]
+    if len(rest) > 1:
+        out[:, : rest[0].shape[1]] = rest[0][...]
     where = lax.div(lax.axis_index("kv"), inner)
     seqs, _, keys, vals = taken.shape
     rows = seqs * proposals
@@ -193,43 +229,42 @@
     tile = group * proposals
     tile_seq = lax.broadcasted_iota(jnp.int32, (tile, keys), 0) // proposals
 
-    def total_of(head, k):
-        cols = slice(k * keys, (k + 1) * keys)
-        total = pieces[head * parts][:, cols]
-        for piece in pieces[head * parts + 1 : (head + 1) * parts]:
-            total = total + piece[lax.rem(where, piece.shape[0]), :, cols].astype(F32)
+    def total_of(k):
+        here = slice(k * keys, (k + 1) * keys)
+        total = pieces[0][:, here]
+        for piece in pieces[1:]:
+            total = total + piece[lax.rem(where, piece.shape[0]), :, here].astype(F32)
         return total
 
-    for head in range(heads):
-        cols = slice((first + head) * keys, (first + head + 1) * keys)
-        gate = forget_of(total_of(head, 0), bounds[:, cols])
-        value = total_of(head, 1)
-        query = total_of(head, 2) * keys ** (-0.5)
-        key = 1.0 - gate
-        through = query
-        result = jnp.sum(query * key, axis=-1, keepdims=True) * value
-        grown = gate
-        before = gate
-        for lag in range(1, proposals):
-            inside = position >= lag
-            through = through * jnp.where(inside, before, 0.0)
-            score = jnp.sum(through * pltpu.roll(key, lag, axis=0), axis=-1, keepdims=True)
-            result = result + score * pltpu.roll(value, lag, axis=0)
-            before = pltpu.roll(gate, lag, axis=0)
-            grown = grown * jnp.where(inside, before, 1.0)
-        reach = (query * grown).astype(BF16)
-        met = []
-        for at in range(0, seqs, group):
-            part = reach[at * proposals : (at + group) * proposals, :]
-            lhs = jnp.concatenate(
-                [jnp.where(tile_seq == s, part, jnp.zeros_like(part)) for s in range(group)], axis=1
-            )
-            here = taken[at : at + group, head].astype(BF16).reshape(group * keys, vals)
-            met.append(jnp.dot(lhs, here, preferred_element_type=F32))
-        result = result + jnp.concatenate(met, axis=0)
-        scale = lax.rsqrt(jnp.mean(result * result, axis=-1, keepdims=True) + EPSILON)
-        result = result * scale * gain[:, cols] * jax.nn.silu(total_of(head, 3))
-        out[:, head * keys : (head + 1) * keys] = result.astype(BF16)
+    cols = slice(head * keys, (head + 1) * keys)
+    gate = forget_of(total_of(0), bounds[:, cols])
+    value = total_of(1)
+    query = total_of(2) * keys ** (-0.5)
+    key = 1.0 - gate
+    through = query
+    result = jnp.sum(query * key, axis=-1, keepdims=True) * value
+    grown = gate
+    before = gate
+    for lag in range(1, proposals):
+        inside = position >= lag
+        through = through * jnp.where(inside, before, 0.0)
+        score = jnp.sum(through * pltpu.roll(key, lag, axis=0), axis=-1, keepdims=True)
+        result = result + score * pltpu.roll(value, lag, axis=0)
+        before = pltpu.roll(gate, lag, axis=0)
+        grown = grown * jnp.where(inside, before, 1.0)
+    reach = (query * grown).astype(BF16)
+    met = []
+    for at in range(0, seqs, group):
+        part = reach[at * proposals : (at + group) * proposals, :]
+        lhs = jnp.concatenate(
+            [jnp.where(tile_seq == s, part, jnp.zeros_like(part)) for s in range(group)], axis=1
+        )
+        here = taken[at : at + group, 0].astype(BF16).reshape(group * keys, vals)
+        met.append(jnp.dot(lhs, here, preferred_element_type=F32))
+    result = result + jnp.concatenate(met, axis=0)
+    scale = lax.rsqrt(jnp.mean(result * result, axis=-1, keepdims=True) + EPSILON)
+    result = result * scale * gain[:, cols] * jax.nn.silu(total_of(3))
+    out[:, out.shape[1] - keys :] = result.astype(BF16)
 
 
 def mix_kernel(order, *refs, lanes, ids, runs, inner, keys):
@@ -314,12 +349,17 @@
     normed = pl.pallas_call(
         lambda *refs: norm_kernel(*refs, ring=ring, inner=inner, share=share, heads=heads),
         out_shape=shapes,
-        in_specs=[VMEM, VMEM] + [HBM] * 4,
+        in_specs=[HBM, VMEM] + [HBM] * 4,
         out_specs=[VMEM] * len(shapes),
-        scratch_shapes=[pltpu.VMEM(tokens.shape, BF16), pltpu.SemaphoreType.DMA((4 * heads,))],
-        compiler_params=room(60),
+        scratch_shapes=[
+            pltpu.VMEM(tokens.shape, BF16),
+            pltpu.VMEM(tokens.shape, BF16),
+            pltpu.SemaphoreType.DMA((4 * heads,)),
+            pltpu.SemaphoreType.DMA((4 if rows % 256 == 0 else 1,)),
+        ],
+        compiler_params=room(16),
         name="norm",
-    )(tokens, norm_gain.reshape(1, -1), w_forget, w_value, w_query, w_gate)
+    )(*in_hbm(tokens, norm_gain.reshape(1, -1), w_forget, w_value, w_query, w_gate))
     own, mine = normed[0], normed[1:ring]
     sets = []
     for weight in normed[ring:]:
@@ -337,16 +377,19 @@
     taken = pl.pallas_call(
         lambda *refs: taken_kernel(*refs, proposals=proposals, seqs=some),
         out_shape=jax.ShapeDtypeStruct(state.shape, F32),
-        in_specs=[SMEM, HBM, VMEM, VMEM, VMEM],
+        in_specs=[SMEM, HBM, HBM, HBM, VMEM],
         out_specs=HBM,
         scratch_shapes=[
             pltpu.VMEM(state.shape, F32),
+            pltpu.VMEM(prev_forget.shape, BF16),
+            pltpu.VMEM(prev_value.shape, BF16),
             pltpu.SemaphoreType.DMA((seqs // some,)),
             pltpu.SemaphoreType.DMA((seqs // some,)),
+            pltpu.SemaphoreType.DMA((2,)),
         ],
-        compiler_params=room(48),
+        compiler_params=room(24),
         name="taken",
-    )(accepted, state, prev_forget, prev_value, bounds)
+    )(*in_hbm(accepted, state, prev_forget, prev_value, bounds))
 
     def added(a, b):
         return (a.astype(F32) + b.astype(F32)).astype(BF16)
@@ -420,32 +463,54 @@
     runs = runs_of(heads)
     many = 32 if seqs % 32 == 0 else seqs
     many_rows = many * proposals
+    parts = len(head_parts[0])
     gathered, ids = [], []
+    ready = None
     for k, run in enumerate(runs):
-        specs, arrays = [], []
+        last = k == len(runs) - 1
+        head_out = None
         for head in run:
-            for array in head_parts[head]:
-                arrays.append(array)
+            spare = head == 0 and heads > 1
+            source = in_hbm(taken)[0] if ready is None or head < heads - 1 else ready
+            arrays = [*head_parts[head], source, bounds, head_gain.reshape(1, width)]
+
+            def spec_of(array):
                 if array.ndim == 2:
-                    specs.append(pl.BlockSpec((many_rows, 4 * keys), lambda i: (i, 0)))
-                else:
-                    specs.append(pl.BlockSpec((array.shape[0], many_rows, 4 * keys), lambda i: (0, i, 0)))
-        parts = len(head_parts[0])
-        held = len(run)
-        place = run[0] // held
-        last = k == len(runs) - 1
-        head_out = pl.pallas_call(
-            lambda *refs, held=held, first=run[0]: recur_kernel(
-                *refs, parts=parts, heads=held, first=first, proposals=proposals, inner=inner
-            ),
-            out_shape=jax.ShapeDtypeStruct((rows, held * keys), BF16),
-            grid=(seqs // many,),
-            in_specs=specs
-            + [pl.BlockSpec((many, held, keys, vals), lambda i, place=place: (i, place, 0, 0)), one_spec, one_spec],
-            out_specs=pl.BlockSpec((many_rows, held * keys), lambda i: (i, 0)),
-            compiler_params=room(40),
-            name="recur",
-        )(*arrays, taken, bounds, head_gain.reshape(1, width))
+                    return pl.BlockSpec((many_rows, array.shape[1]), lambda i: (i, 0))
+                return pl.BlockSpec((array.shape[0], many_rows, array.shape[2]), lambda i: (0, i, 0))
+
+            def state_of(index):
+                return pl.BlockSpec((many, 1, keys, vals), lambda i: (i, index, 0, 0))
+
+            specs = [spec_of(array) for array in head_parts[head]]
+            specs += [state_of(0 if source is ready else head), one_spec, one_spec]
+            cols = keys
+            shapes = []
+            if spare:
+                arrays.append(in_hbm(taken)[0])
+                specs.append(state_of(heads - 1))
+            if head_out is not None:
+                arrays.append(head_out)
+                specs.append(spec_of(head_out))
+                cols += head_out.shape[1]
+            shapes.append(jax.ShapeDtypeStruct((rows, cols), BF16))
+            outs = [pl.BlockSpec((many_rows, cols), lambda i: (i, 0))]
+            if spare:
+                shapes.append(jax.ShapeDtypeStruct((seqs, 1, keys, vals), BF16))
+                outs.append(state_of(0))
+            head_out, *more = pl.pallas_call(
+                lambda *refs, head=head, spare=spare: recur_kernel(
+                    *refs, parts=parts, head=head, proposals=proposals, inner=inner, spare=spare
+                ),
+                out_shape=shapes,
+                grid=(seqs // many,),
+                in_specs=specs,
+                out_specs=outs,
+                compiler_params=room(20),
+                name="recur",
+            )(*arrays)
+            if spare:
+                ready = more[0]
         pieces, ids = [head_out], [0]
         bit = tp // 2
         while bit:
@@ -477,8 +542,7 @@
 
 
 def runs_of(heads):
-    half = max(1, heads // 2)
-    return [list(range(half))] + [[head] for head in range(half, heads)]
+    return [list(range(heads - 1)), [heads - 1]] if heads > 1 else [[0]]
 
 
 def order_of(ring):

time: 175 us -> 182 us (1.040)
  waiting for transfers between devices: 50.9 us -> 63.1 us
  local copies, waits for them, and re-layouts: 7.51 us -> 2.39 us
  other arithmetic: 7.9 us -> 4.99 us
  Pallas kernels: 40.4 us -> 42.9 us
    ppermute x4, waiting for transfers between devices: 9.73 us -> 15.3 us  [on_device(): lax.ppermute(weight, 'kv', around(t))]
    unnamed x34 -> x20, local copies, waits for them, and re-layouts: 7.51 us -> 2.39 us
    ppermute x8, starting transfers between devices: 26.6 us -> 31.3 us  [summed(): got = lax.ppermute(out, 'kv', mirrored(size, size - 1, size))]
    ppermute x12 -> x9, waiting for transfers between devices: 6.02 us -> 10.5 us  [swap(): return lax.ppermute(value, 'tp', [(t, t ^ bit) for t in range(tp)])]
    ppermute x4, starting transfers between devices: 15.9 us -> 13.2 us  [summed(): got = lax.ppermute(out, 'kv', mirrored(size, hop - 1, hop))]
    convert_element_type x8, other arithmetic: 5.13 us -> 3.26 us  [added(): return (a.astype(F32) + b.astype(F32)).astype(BF16)]
    ppermute x12 -> x9, starting transfers between devices: 5.43 us -> 4.23 us  [swap(): return lax.ppermute(value, 'tp', [(t, t ^ bit) for t in range(tp)])]
    pallas_call x3 -> x4, Pallas kernels: 9.54 us -> 10.3 us  [on_device(): pl.pallas_call(lambda *refs, head=head, spare=spare: recur_kernel(*refs,...]
  transfers between devices with their start and end apart: 36 -> 33, of which waited for: 13 -> 12; matrix products, arithmetic and copies ran while one was open for 5% -> 3% of each run, Pallas kernels for 22% -> 22%
where the time goes in v2:
time: 182 us
  starting transfers between devices  67.4 us (37%)
  waiting for transfers between devices  63.1 us (35%)
  Pallas kernels  42.9 us (24%)
  other arithmetic  4.99 us (3%)
  local copies, waits for them, and re-layouts  2.39 us (1%)
    ppermute x8, starting transfers between devices, summed(): got = lax.ppermute(out, 'kv', mirrored(size, size - 1, size))  31.3 us
    pallas_call x1, Pallas kernels, on_device(): pl.pallas_call(lambda *refs: taken_kernel(*refs, proposals=proposals, seq...  16.4 us
    ppermute x4, waiting for transfers between devices, on_device(): lax.ppermute(weight, 'kv', around(t))  15.3 us
    ppermute x4, waiting for transfers between devices, summed(): got = lax.ppermute(out, 'kv', mirrored(size, hop - 1, hop))  13.2 us
    ppermute x4, starting transfers between devices, summed(): got = lax.ppermute(out, 'kv', mirrored(size, hop - 1, hop))  13.2 us
    ppermute x3, waiting for transfers between devices, on_device(): lax.ppermute(mine[r - 1], 'kv', groups([(g, g ^ r) for g in range(ring)]))  10.8 us
    ppermute x9, waiting for transfers between devices, swap(): return lax.ppermute(value, 'tp', [(t, t ^ bit) for t in range(tp)])  10.5 us
    pallas_call x4, Pallas kernels, on_device(): pl.pallas_call(lambda *refs, head=head, spare=spare: recur_kernel(*refs,...  10.3 us
  transfers between devices with their start and end apart: 33, of which 12 were waited for; matrix products, arithmetic and copies ran while one was open for 3% of the time, Pallas kernels for 22%

profile of v2, /device:TPU:0, one launch (start us, length us, event | category | flops | bytes accessed | tf_op | source)
XLA Modules:
  0.0 181.8 jit_solution(12687575822496083847)
XLA Ops:
  0.6 3.1 %collective-permute-start.28 = (bf16[1,256,1024]{2,1,0:T(8,128)(2,1)}, bf16[1,256,1024]{2,1,0:T(8,128)(2,1)S(1)}, u32[]{:S(2)}, u32[]{:S(2)}) collective-permute-start(bf16[1,256,1024]{2,1,0:T(8,128)(2,1)} %bitcast.13), channel_id=1, source_target_pairs={{0,8},{4,12},{8,0},{12,4},{16,24},{20,28},{24,16},{28,20},{1,9},{5... | collective-permute-start | bytes 1572872 | tf_op jit(solution)/shard_map/ppermute | solution.py:441
  3.8 4.7 %norm.1 = (bf16[2,256,512]{2,1,0:T(8,128)(2,1)S(1)}, bf16[2,128,512]{2,1,0:T(8,128)(2,1)S(1)}, bf16[2,128,512]{2,1,0:T(8,128)(2,1)S(1)}, bf16[2,128,512]{2,1,0:T...) custom-call(bf16[256,4096]{1,0:T(8,128)(2,1)} %refs_0_.3, ...), custom_call_target="tpu_custom_call" | custom-call | tf_op jit(solution)/shard_map/norm/pallas_call | solution.py:349
  8.5 3.0 %collective-permute-start.2 = (bf16[2,128,512]{2,1,0:T(8,128)(2,1)S(1)}, bf16[2,128,512]{2,1,0:T(8,128)(2,1)S(1)}, u32[]{:S(2)}, u32[]{:S(2)}) collective-permute-start(bf16[2,128,512]{2,1,0:T(8,128)(2,1)S(1)} %get-tuple-element.27), channel_id=1, source_target_pairs={{0,16},{4,20},{8,24},{12,28},{16,0},{20,4},{24,8},{28,12},{1,17},{... | collective-permute-start | bytes 786440 | tf_op jit(solution)/shard_map/ppermute | solution.py:369
  11.6 1.3 collective-permute-start.4
  12.9 1.5 collective-permute-start.6
  14.4 7.9 %collective-permute-done.28 = bf16[1,256,1024]{2,1,0:T(8,128)(2,1)S(1)} collective-permute-done((bf16[1,256,1024]{2,1,0:T(8,128)(2,1)}, bf16[1,256,1024]{2,1,0:T(8,128)(2,1)S(1)}, u32[]{:S(2)}, u32[]{:S(2)}) %collective-permute-start.28) | collective-permute-done | bytes 524320 | tf_op jit(solution)/shard_map/ppermute | solution.py:441
  22.5 1.7 collective-permute-start.30
  24.1 3.0 %collective-permute-done.refs_1_ = bf16[2,128,512]{2,1,0:T(8,128)(2,1)S(1)} collective-permute-done((bf16[2,128,512]{2,1,0:T(8,128)(2,1)S(1)}, bf16[2,128,512]{2,1,0:T(8,128)(2,1)S(1)}, u32[]{:S(2)}, u32[]{:S(2)}) %collective-permute-start) | collective-permute-done | bytes 262176 | tf_op jit(solution)/shard_map/ppermute | solution.py:369
  27.6 7.4 %collective-permute-done.4.refs_5_ = bf16[2,128,512]{2,1,0:T(8,128)(2,1)S(1)} collective-permute-done((bf16[2,128,512]{2,1,0:T(8,128)(2,1)S(1)}, bf16[2,128,512]{2,1,0:T(8,128)(2,1)S(1)}, u32[]{:S(2)}, u32[]{:S(2)}) %collective-permute-start.4) | collective-permute-done | bytes 262176 | tf_op jit(solution)/shard_map/ppermute | solution.py:369
  35.0 1.5 collective-permute-start.11
  37.1 1.5 collective-permute-start.7
  38.6 2.0 %project.4 = (f32[256,512]{1,0:T(8,128)S(1)}, bf16[1,256,512]{2,1,0:T(8,128)(2,1)S(1)}, bf16[2,256,512]{2,1,0:T(8,128)(2,1)}, bf16[1024,1024]{1,0:T(8,128)(2,1)S(1)}) custom-call(bf16[2,256,512]{2,1,0:T(8,128)(2,1)S(1)} %get-tuple-element.25.refs_0_, bf16[2,128,512]{2,1,0:T(8,128)(2,1)S(1)} %collective-permute-done.refs_1_, ...), custom_call_target="tpu_custom_call" | custom-call | tf_op jit(solution)/shard_map/project/pallas_call | solution.py:408
  40.6 0.8 copy-done
  41.4 4.2 %collective-permute-start.15 = (bf16[2,256,512]{2,1,0:T(8,128)(2,1)}, bf16[2,256,512]{2,1,0:T(8,128)(2,1)}, u32[]{:S(2)}, u32[]{:S(2)}) collective-permute-start(bf16[2,256,512]{2,1,0:T(8,128)(2,1)} %get-tuple-element.40), channel_id=1, source_target_pairs={{0,8},{4,12},{24,16},{28,20},{1,9},{5,13},{25,17},{29,21},{2,10},{... | collective-permute-start | bytes 1572872 | tf_op jit(solution)/shard_map/ppermute | solution.py:424
  45.6 4.2 %collective-permute-done.11.refs_2_ = bf16[512,512]{1,0:T(8,128)(2,1)S(1)} collective-permute-done((bf16[512,512]{1,0:T(8,128)(2,1)S(1)}, bf16[512,512]{1,0:T(8,128)(2,1)S(1)}, u32[]{:S(2)}, u32[]{:S(2)}) %collective-permute-start.11) | collective-permute-done | bytes 524320 | tf_op jit(solution)/shard_map/ppermute | solution.py:366
  49.8 1.8 %project.6 = (f32[256,512]{1,0:T(8,128)S(1)}, bf16[1,256,512]{2,1,0:T(8,128)(2,1)S(1)}, bf16[2,256,512]{2,1,0:T(8,128)(2,1)}) custom-call(bf16[1024,1024]{1,0:T(8,128)(2,1)S(1)} %get-tuple-element.30.refs_0_, bf16[512,512]{1,0:T(8,128)(2,1)S(1)} %get-tuple-element.35.refs_1_, bf16[512,512]{1,0:T(8,128)(2,1)S(1)} %collective-permute-done.11.refs_2_), custom_call_target="tpu_custom_call" | custom-call | tf_op jit(solution)/shard_map/project/pallas_call | solution.py:408
  51.7 0.8 copy-done.2
  53.2 4.2 %collective-permute-start.12 = (bf16[2,256,512]{2,1,0:T(8,128)(2,1)}, bf16[2,256,512]{2,1,0:T(8,128)(2,1)}, u32[]{:S(2)}, u32[]{:S(2)}) collective-permute-start(bf16[2,256,512]{2,1,0:T(8,128)(2,1)} %get-tuple-element.37), channel_id=1, source_target_pairs={{0,8},{4,12},{24,16},{28,20},{1,9},{5,13},{25,17},{29,21},{2,10},{... | collective-permute-start | bytes 1572872 | tf_op jit(solution)/shard_map/ppermute | solution.py:424
  57.4 3.8 %collective-permute-done.21.refs_2_ = bf16[512,512]{1,0:T(8,128)(2,1)} collective-permute-done((bf16[512,512]{1,0:T(8,128)(2,1)}, bf16[512,512]{1,0:T(8,128)(2,1)}, u32[]{:S(2)}, u32[]{:S(2)}) %collective-permute-start.21) | collective-permute-done | bytes 524320 | tf_op jit(solution)/shard_map/ppermute | solution.py:366
  61.2 1.5 collective-permute-start.29
  62.7 2.4 %project.7 = (f32[256,512]{1,0:T(8,128)S(1)}, bf16[1,256,512]{2,1,0:T(8,128)(2,1)S(1)}, bf16[2,256,512]{2,1,0:T(8,128)(2,1)S(1)}) custom-call(bf16[1024,1024]{1,0:T(8,128)(2,1)S(1)} %get-tuple-element.30.refs_0_, bf16[512,512]{1,0:T(8,128)(2,1)} %get-tuple-element.43.refs_1_, bf16[512,512]{1,0:T(8,128)(2,1)} %collective-permute-done.21.refs_2_), custom_call_target="tpu_custom_call" | custom-call | tf_op jit(solution)/shard_map/project/pallas_call | solution.py:408
  65.1 7.3 %collective-permute-done.7.refs_2_ = bf16[512,512]{1,0:T(8,128)(2,1)} collective-permute-done((bf16[512,512]{1,0:T(8,128)(2,1)}, bf16[512,512]{1,0:T(8,128)(2,1)}, u32[]{:S(2)}, u32[]{:S(2)}) %collective-permute-start.7) | collective-permute-done | bytes 524320 | tf_op jit(solution)/shard_map/ppermute | solution.py:366
  72.4 3.4 %collective-permute-start.22 = (bf16[2,256,512]{2,1,0:T(8,128)(2,1)S(1)}, bf16[2,256,512]{2,1,0:T(8,128)(2,1)S(1)}, u32[]{:S(2)}, u32[]{:S(2)}) collective-permute-start(bf16[2,256,512]{2,1,0:T(8,128)(2,1)S(1)} %get-tuple-element.45), channel_id=1, source_target_pairs={{0,8},{4,12},{24,16},{28,20},{1,9},{5,13},{25,17},{29,21},{2,10},{... | collective-permute-start | bytes 1572872 | tf_op jit(solution)/shard_map/ppermute | solution.py:424
  75.8 2.5 %project.5 = (f32[256,512]{1,0:T(8,128)S(1)}, bf16[1,256,512]{2,1,0:T(8,128)(2,1)S(1)}, bf16[2,256,512]{2,1,0:T(8,128)(2,1)S(1)}) custom-call(bf16[1024,1024]{1,0:T(8,128)(2,1)S(1)} %get-tuple-element.30.refs_0_, bf16[512,512]{1,0:T(8,128)(2,1)} %get-tuple-element.31.refs_1_, bf16[512,512]{1,0:T(8,128)(2,1)} %collective-permute-done.7.refs_2_), custom_call_target="tpu_custom_call" | custom-call | tf_op jit(solution)/shard_map/project/pallas_call | solution.py:408
  78.3 1.3 collective-permute-start.8
  79.7 1.3 collective-permute-start.31
  81.0 1.3 add_convert_fusion.1
  83.0 1.3 add_convert_fusion.2
  84.4 13.2 %collective-permute-done.8 = bf16[2,256,512]{2,1,0:T(8,128)(2,1)S(1)} collective-permute-done((bf16[2,256,512]{2,1,0:T(8,128)(2,1)S(1)}, bf16[2,256,512]{2,1,0:T(8,128)(2,1)S(1)}, u32[]{:S(2)}, u32[]{:S(2)}) %collective-permute-start.8) | collective-permute-done | bytes 524320 | tf_op jit(solution)/shard_map/ppermute | solution.py:424
  99.3 1.0 collective-permute-start.23
  100.4 5.4 %collective-permute-done.31 = bf16[2,256,1024]{2,1,0:T(8,128)(2,1)S(1)} collective-permute-done((bf16[2,256,1024]{2,1,0:T(8,128)(2,1)}, bf16[2,256,1024]{2,1,0:T(8,128)(2,1)S(1)}, u32[]{:S(2)}, u32[]{:S(2)}) %collective-permute-start.31) | collective-permute-done | bytes 1048608 | tf_op jit(solution)/shard_map/ppermute | solution.py:445
  105.7 5.3 %collective-permute-start.17 = (bf16[1,256,512]{2,1,0:T(8,128)(2,1)S(1)}, bf16[1,256,512]{2,1,0:T(8,128)(2,1)S(1)}, u32[]{:S(2)}, u32[]{:S(2)}) collective-permute-start(bf16[1,256,512]{2,1,0:T(8,128)(2,1)S(1)} %add_convert_fusion.5), channel_id=1, source_target_pairs={{0,8},{4,12},{8,0},{12,4},{16,24},{20,28},{24,16},{28,20},{1,9},{5... | collective-permute-start | bytes 786440 | tf_op jit(solution)/shard_map/ppermute | solution.py:426
  111.1 1.6 add.52.refs_11_
  112.7 1.6 collective-permute-start.32
  114.4 14.0 %collective-permute-start.14 = (bf16[1,256,512]{2,1,0:T(8,128)(2,1)S(1)}, bf16[1,256,512]{2,1,0:T(8,128)(2,1)S(1)}, u32[]{:S(2)}, u32[]{:S(2)}) collective-permute-start(bf16[1,256,512]{2,1,0:T(8,128)(2,1)S(1)} %add_convert_fusion.6), channel_id=1, source_target_pairs={{0,8},{4,12},{8,0},{12,4},{16,24},{20,28},{24,16},{28,20},{1,9},{5... | collective-permute-start | bytes 786440 | tf_op jit(solution)/shard_map/ppermute | solution.py:426
  128.5 8.8 %collective-permute-start.10 = (bf16[1,256,512]{2,1,0:T(8,128)(2,1)S(1)}, bf16[1,256,512]{2,1,0:T(8,128)(2,1)S(1)}, u32[]{:S(2)}, u32[]{:S(2)}) collective-permute-start(bf16[1,256,512]{2,1,0:T(8,128)(2,1)S(1)} %add_convert_fusion.7), channel_id=1, source_target_pairs={{0,8},{4,12},{8,0},{12,4},{16,24},{20,28},{24,16},{28,20},{1,9},{5... | collective-permute-start | bytes 786440 | tf_op jit(solution)/shard_map/ppermute | solution.py:426
  137.3 16.4 %taken.1.refs_3_.refs_6_ = f32[64,4,128,128]{3,2,1,0:T(8,128)} custom-call(s32[64]{0:T(128)} %refs_0_.4, f32[64,4,128,128]{3,2,1,0:T(8,128)} %refs_1_.1, bf16[64,4,512]{2,1,0:T(4,128)(2,1)} %refs_2_.3, bf16[64,4,512]{2,1,0:T(4,128)(2,1)} %refs_3_.3, f32[1,512]{1,0:T(1,128)} %bitcast.4), custom_call_target="tpu_custom_call" | custom-call | tf_op jit(solution)/shard_map/taken/pallas_call | solution.py:377
  154.0 4.1 %recur.4 = (bf16[256,128]{1,0:T(8,128)(2,1)S(1)}, bf16[64,1,128,128]{3,2,1,0:T(8,128)(2,1)S(1)}) custom-call(f32[256,512]{1,0:T(8,128)S(1)} %copy-done.1, bf16[2,256,512]{2,1,0:T(8,128)(2,1)S(1)} %collective-permute-done.16.refs_1_, bf16[1,256,512]{2,1,0:T(8,128)(2,1)S(1)} %collective-permute-done.17.refs_2_, f32[64,4,128,128]{3,2,1,0:T(8,128)} %taken.1.refs_3_.refs_6_, ...), custom_call_target="tpu_custom_call" | custom-call | tf_op jit(solution)/shard_map/recur/pallas_call | solution.py:501
  158.1 2.7 %recur.5.refs_6_ = bf16[256,256]{1,0:T(8,128)(2,1)S(1)} custom-call(f32[256,512]{1,0:T(8,128)S(1)} %copy-done.3, bf16[2,256,512]{2,1,0:T(8,128)(2,1)S(1)} %collective-permute-done.13.refs_1_, bf16[1,256,512]{2,1,0:T(8,128)(2,1)S(1)} %collective-permute-done.14.refs_2_, f32[64,4,128,128]{3,2,1,0:T(8,128)} %taken.1.refs_3_.refs_6_, f32[1,512]{1,0:T(1,128)S(1)} %bitcast.6, ...), custom_call_target="tpu_custom_call" | custom-call | tf_op jit(solution)/shard_map/recur/pallas_call | solution.py:501
  160.8 2.7 %recur.6.refs_1_ = bf16[256,384]{1,0:T(8,128)(2,1)S(1)} custom-call(f32[256,512]{1,0:T(8,128)S(1)} %get-tuple-element.32.refs_0_, bf16[2,256,512]{2,1,0:T(8,128)(2,1)S(1)} %collective-permute-done.9.refs_1_, bf16[1,256,512]{2,1,0:T(8,128)(2,1)S(1)} %collective-permute-done.10.refs_2_, f32[64,4,128,128]{3,2,1,0:T(8,128)} %taken.1.refs_3_.refs_6_, ...), custom_call_target="tpu_custom_call" | custom-call | tf_op jit(solution)/shard_map/recur/pallas_call | solution.py:501
  163.5 1.6 collective-permute-start.18
  165.1 4.2 %collective-permute-done.18.refs_2_ = bf16[256,384]{1,0:T(8,128)(2,1)S(1)} collective-permute-done((bf16[256,384]{1,0:T(8,128)(2,1)S(1)}, bf16[256,384]{1,0:T(8,128)(2,1)S(1)}, u32[]{:S(2)}, u32[]{:S(2)}) %collective-permute-start.18) | collective-permute-done | bytes 196640 | tf_op jit(solution)/shard_map/ppermute | solution.py:342
  169.2 0.8 recur.7.refs_5_
  170.1 1.6 collective-permute-start.25
  171.9 2.8 %collective-permute-done.25.refs_6_ = bf16[256,128]{1,0:T(8,128)(2,1)S(1)} collective-permute-done((bf16[256,128]{1,0:T(8,128)(2,1)S(1)}, bf16[256,128]{1,0:T(8,128)(2,1)S(1)}, u32[]{:S(2)}, u32[]{:S(2)}) %collective-permute-start.25) | collective-permute-done | bytes 65568 | tf_op jit(solution)/shard_map/ppermute | solution.py:342
  174.7 0.8 collective-permute-start.27
  175.4 3.6 %collective-permute-done.27.refs_8_ = bf16[256,128]{1,0:T(8,128)(2,1)S(1)} collective-permute-done((bf16[256,128]{1,0:T(8,128)(2,1)S(1)}, bf16[256,128]{1,0:T(8,128)(2,1)S(1)}, u32[]{:S(2)}, u32[]{:S(2)}) %collective-permute-start.27) | collective-permute-done | bytes 65568 | tf_op jit(solution)/shard_map/ppermute | solution.py:342
  179.0 2.7 %mix.1 = bf16[256,1024]{1,0:T(8,128)(2,1)} custom-call(s32[4,4]{1,0:T(4,128)S(1)} %copy-done.8, bf16[256,384]{1,0:T(8,128)(2,1)S(1)} %recur.6.refs_1_, bf16[256,384]{1,0:T(8,128)(2,1)S(1)} %collective-permute-done.18.refs_2_, bf16[256,384]{1,0:T(8,128)(2,1)S(1)} %collective-permute-done.19.refs_3_, bf16[256,384]{1,0:T(8,128)(2,1)S(1)} %collective-permute-done.20.refs_4_, ...), custom_call_target="tpu_custom_call" | custom-call | tf_op jit(solution)/shard_map/mix/pallas_call | solution.py:527
  (59 shorter events, 5.0 us)
Async XLA Ops:
  0.6 21.7 %collective-permute-start.28 = (bf16[1,256,1024]{2,1,0:T(8,128)(2,1)}, bf16[1,256,1024]{2,1,0:T(8,128)(2,1)S(1)}, u32[]{:S(2)}, u32[]{:S(2)}) collective-permute-start(bf16[1,256,1024]{2,1,0:T(8,128)(2,1)} %bitcast.13), channel_id=1, source_target_pairs={{0,8},{4,12},{8,0},{12,4},{16,24},{20,28},{24,16},{28,20},{1,9},{5... | collective-permute-start | bytes 1572872 | tf_op jit(solution)/shard_map/ppermute | solution.py:441
  3.7 18.6 %copy-start.9 = (bf16[256,1024]{1,0:T(8,128)(2,1)S(1)}, bf16[256,1024]{1,0:T(8,128)(2,1)}, u32[]{:S(2)}) copy-start(bf16[256,1024]{1,0:T(8,128)(2,1)} %param.22) | copy-start | bytes 1572868
  8.5 18.7 %collective-permute-start = (bf16[2,128,512]{2,1,0:T(8,128)(2,1)S(1)}, bf16[2,128,512]{2,1,0:T(8,128)(2,1)S(1)}, u32[]{:S(2)}, u32[]{:S(2)}) collective-permute-start(bf16[2,128,512]{2,1,0:T(8,128)(2,1)S(1)} %get-tuple-element.26), channel_id=1, source_target_pairs={{0,8},{4,12},{8,0},{12,4},{16,24},{20,28},{24,16},{28,20},{1,9},{5... | collective-permute-start | bytes 786440 | tf_op jit(solution)/shard_map/ppermute | solution.py:369
  8.5 19.0 %collective-permute-start.2 = (bf16[2,128,512]{2,1,0:T(8,128)(2,1)S(1)}, bf16[2,128,512]{2,1,0:T(8,128)(2,1)S(1)}, u32[]{:S(2)}, u32[]{:S(2)}) collective-permute-start(bf16[2,128,512]{2,1,0:T(8,128)(2,1)S(1)} %get-tuple-element.27), channel_id=1, source_target_pairs={{0,16},{4,20},{8,24},{12,28},{16,0},{20,4},{24,8},{28,12},{1,17},{... | collective-permute-start | bytes 786440 | tf_op jit(solution)/shard_map/ppermute | solution.py:369
  11.6 23.5 %collective-permute-start.4 = (bf16[2,128,512]{2,1,0:T(8,128)(2,1)S(1)}, bf16[2,128,512]{2,1,0:T(8,128)(2,1)S(1)}, u32[]{:S(2)}, u32[]{:S(2)}) collective-permute-start(bf16[2,128,512]{2,1,0:T(8,128)(2,1)S(1)} %get-tuple-element.28), channel_id=1, source_target_pairs={{0,24},{4,28},{8,16},{12,20},{16,8},{20,12},{24,0},{28,4},{1,25},{... | collective-permute-start | bytes 786440 | tf_op jit(solution)/shard_map/ppermute | solution.py:369
  12.9 25.7 %collective-permute-start.6 = (bf16[512,512]{1,0:T(8,128)(2,1)S(1)}, bf16[512,512]{1,0:T(8,128)(2,1)S(1)}, u32[]{:S(2)}, u32[]{:S(2)}) collective-permute-start(bf16[512,512]{1,0:T(8,128)(2,1)S(1)} %get-tuple-element.29.refs_7_), channel_id=1, source_target_pairs={{4,0},{0,4},{12,8},{8,12},{20,16},{16,20},{28,24},{24,28},{5,1},{1... | collective-permute-start | bytes 1572872 | tf_op jit(solution)/shard_map/ppermute | solution.py:366
  22.5 57.2 %collective-permute-start.30 = (bf16[2,256,1024]{2,1,0:T(8,128)(2,1)S(1)}, bf16[2,256,1024]{2,1,0:T(8,128)(2,1)}, u32[]{:S(2)}, u32[]{:S(2)}) collective-permute-start(bf16[2,256,1024]{2,1,0:T(8,128)(2,1)S(1)} %pad_maximum_fusion.refs_9_), channel_id=1, source_target_pairs={{8,16},{12,20},{16,8},{20,12},{9,17},{13,21},{17,9},{21,13},{10,18... | collective-permute-start | bytes 3145736 | tf_op jit(solution)/shard_map/ppermute | solution.py:441
  27.1 7.9 %collective-permute-start.1 = (bf16[2,128,512]{2,1,0:T(8,128)(2,1)S(1)}, bf16[2,128,512]{2,1,0:T(8,128)(2,1)S(1)}, u32[]{:S(2)}, u32[]{:S(2)}) collective-permute-start(bf16[2,128,512]{2,1,0:T(8,128)(2,1)S(1)} %collective-permute-done.refs_1_), channel_id=1, source_target_pairs={{0,1},{1,0},{2,3},{3,2},{4,5},{5,4},{6,7},{7,6},{8,9},{9,8},{10,11... | collective-permute-start | bytes 786440 | tf_op jit(solution)/shard_map/ppermute | solution.py:342
  27.6 9.0 %collective-permute-start.3 = (bf16[2,128,512]{2,1,0:T(8,128)(2,1)S(1)}, bf16[2,128,512]{2,1,0:T(8,128)(2,1)S(1)}, u32[]{:S(2)}, u32[]{:S(2)}) collective-permute-start(bf16[2,128,512]{2,1,0:T(8,128)(2,1)S(1)} %collective-permute-done.2.refs_3_), channel_id=1, source_target_pairs={{0,1},{1,0},{2,3},{3,2},{4,5},{5,4},{6,7},{7,6},{8,9},{9,8},{10,11... | collective-permute-start | bytes 786440 | tf_op jit(solution)/shard_map/ppermute | solution.py:342
  35.0 2.0 %collective-permute-start.5 = (bf16[2,128,512]{2,1,0:T(8,128)(2,1)S(1)}, bf16[2,128,512]{2,1,0:T(8,128)(2,1)S(1)}, u32[]{:S(2)}, u32[]{:S(2)}) collective-permute-start(bf16[2,128,512]{2,1,0:T(8,128)(2,1)S(1)} %collective-permute-done.4.refs_5_), channel_id=1, source_target_pairs={{0,1},{1,0},{2,3},{3,2},{4,5},{5,4},{6,7},{7,6},{8,9},{9,8},{10,11... | collective-permute-start | bytes 786440 | tf_op jit(solution)/shard_map/ppermute | solution.py:342
  35.0 14.8 %collective-permute-start.11 = (bf16[512,512]{1,0:T(8,128)(2,1)S(1)}, bf16[512,512]{1,0:T(8,128)(2,1)S(1)}, u32[]{:S(2)}, u32[]{:S(2)}) collective-permute-start(bf16[512,512]{1,0:T(8,128)(2,1)S(1)} %get-tuple-element.35.refs_1_), channel_id=1, source_target_pairs={{4,0},{0,4},{12,8},{8,12},{20,16},{16,20},{28,24},{24,28},{5,1},{1... | collective-permute-start | bytes 1572872 | tf_op jit(solution)/shard_map/ppermute | solution.py:366
  36.6 24.6 %collective-permute-start.21 = (bf16[512,512]{1,0:T(8,128)(2,1)}, bf16[512,512]{1,0:T(8,128)(2,1)}, u32[]{:S(2)}, u32[]{:S(2)}) collective-permute-start(bf16[512,512]{1,0:T(8,128)(2,1)} %get-tuple-element.43.refs_1_), channel_id=1, source_target_pairs={{4,0},{0,4},{12,8},{8,12},{20,16},{16,20},{28,24},{24,28},{5,1},{1... | collective-permute-start | bytes 1572872 | tf_op jit(solution)/shard_map/ppermute | solution.py:366
  37.1 35.3 %collective-permute-start.7 = (bf16[512,512]{1,0:T(8,128)(2,1)}, bf16[512,512]{1,0:T(8,128)(2,1)}, u32[]{:S(2)}, u32[]{:S(2)}) collective-permute-start(bf16[512,512]{1,0:T(8,128)(2,1)} %get-tuple-element.31.refs_1_), channel_id=1, source_target_pairs={{4,0},{0,4},{12,8},{8,12},{20,16},{16,20},{28,24},{24,28},{5,1},{1... | collective-permute-start | bytes 1572872 | tf_op jit(solution)/shard_map/ppermute | solution.py:366
  40.6 0.8 copy-start
  41.4 36.9 %collective-permute-start.15 = (bf16[2,256,512]{2,1,0:T(8,128)(2,1)}, bf16[2,256,512]{2,1,0:T(8,128)(2,1)}, u32[]{:S(2)}, u32[]{:S(2)}) collective-permute-start(bf16[2,256,512]{2,1,0:T(8,128)(2,1)} %get-tuple-element.40), channel_id=1, source_target_pairs={{0,8},{4,12},{24,16},{28,20},{1,9},{5,13},{25,17},{29,21},{2,10},{... | collective-permute-start | bytes 1572872 | tf_op jit(solution)/shard_map/ppermute | solution.py:424
  51.6 0.8 copy-start.2
  52.5 0.7 copy-start.4
  53.2 29.1 %collective-permute-start.12 = (bf16[2,256,512]{2,1,0:T(8,128)(2,1)}, bf16[2,256,512]{2,1,0:T(8,128)(2,1)}, u32[]{:S(2)}, u32[]{:S(2)}) collective-permute-start(bf16[2,256,512]{2,1,0:T(8,128)(2,1)} %get-tuple-element.37), channel_id=1, source_target_pairs={{0,8},{4,12},{24,16},{28,20},{1,9},{5,13},{25,17},{29,21},{2,10},{... | collective-permute-start | bytes 1572872 | tf_op jit(solution)/shard_map/ppermute | solution.py:424
  61.2 110.5 %collective-permute-start.29 = (bf16[2,256,1024]{2,1,0:T(8,128)(2,1)S(1)}, bf16[2,256,1024]{2,1,0:T(8,128)(2,1)S(1)}, u32[]{:S(2)}, u32[]{:S(2)}) collective-permute-start(bf16[2,256,1024]{2,1,0:T(8,128)(2,1)S(1)} %pad_maximum_fusion.refs_9_), channel_id=1, source_target_pairs={{4,0},{0,4},{12,8},{8,12},{20,16},{16,20},{28,24},{24,28},{5,1},{1... | collective-permute-start | bytes 3145736 | tf_op jit(solution)/shard_map/ppermute | solution.py:461
  72.4 26.0 %collective-permute-start.22 = (bf16[2,256,512]{2,1,0:T(8,128)(2,1)S(1)}, bf16[2,256,512]{2,1,0:T(8,128)(2,1)S(1)}, u32[]{:S(2)}, u32[]{:S(2)}) collective-permute-start(bf16[2,256,512]{2,1,0:T(8,128)(2,1)S(1)} %get-tuple-element.45), channel_id=1, source_target_pairs={{0,8},{4,12},{24,16},{28,20},{1,9},{5,13},{25,17},{29,21},{2,10},{... | collective-permute-start | bytes 1572872 | tf_op jit(solution)/shard_map/ppermute | solution.py:424
  78.3 19.2 %collective-permute-start.8 = (bf16[2,256,512]{2,1,0:T(8,128)(2,1)S(1)}, bf16[2,256,512]{2,1,0:T(8,128)(2,1)S(1)}, u32[]{:S(2)}, u32[]{:S(2)}) collective-permute-start(bf16[2,256,512]{2,1,0:T(8,128)(2,1)S(1)} %get-tuple-element.33), channel_id=1, source_target_pairs={{0,8},{4,12},{24,16},{28,20},{1,9},{5,13},{25,17},{29,21},{2,10},{... | collective-permute-start | bytes 1572872 | tf_op jit(solution)/shard_map/ppermute | solution.py:424
  79.7 26.1 %collective-permute-start.31 = (bf16[2,256,1024]{2,1,0:T(8,128)(2,1)}, bf16[2,256,1024]{2,1,0:T(8,128)(2,1)S(1)}, u32[]{:S(2)}, u32[]{:S(2)}) collective-permute-start(bf16[2,256,1024]{2,1,0:T(8,128)(2,1)} %collective-permute-done.30), channel_id=1, source_target_pairs={{8,0},{12,4},{16,24},{20,28},{9,1},{13,5},{17,25},{21,29},{10,2},{... | collective-permute-start | bytes 3145736 | tf_op jit(solution)/shard_map/ppermute | solution.py:445
  82.3 16.9 %collective-permute-start.16 = (bf16[2,256,512]{2,1,0:T(8,128)(2,1)S(1)}, bf16[2,256,512]{2,1,0:T(8,128)(2,1)S(1)}, u32[]{:S(2)}, u32[]{:S(2)}) collective-permute-start(bf16[2,256,512]{2,1,0:T(8,128)(2,1)S(1)} %add_convert_fusion.1), channel_id=1, source_target_pairs={{8,16},{12,20},{16,8},{20,12},{9,17},{13,21},{17,9},{21,13},{10,18... | collective-permute-start | bytes 1572872 | tf_op jit(solution)/shard_map/ppermute | solution.py:426
  97.6 15.2 %collective-permute-start.13 = (bf16[2,256,512]{2,1,0:T(8,128)(2,1)S(1)}, bf16[2,256,512]{2,1,0:T(8,128)(2,1)S(1)}, u32[]{:S(2)}, u32[]{:S(2)}) collective-permute-start(bf16[2,256,512]{2,1,0:T(8,128)(2,1)S(1)} %add_convert_fusion.2), channel_id=1, source_target_pairs={{8,16},{12,20},{16,8},{20,12},{9,17},{13,21},{17,9},{21,13},{10,18... | collective-permute-start | bytes 1572872 | tf_op jit(solution)/shard_map/ppermute | solution.py:426
  98.4 16.0 %collective-permute-start.9 = (bf16[2,256,512]{2,1,0:T(8,128)(2,1)S(1)}, bf16[2,256,512]{2,1,0:T(8,128)(2,1)S(1)}, u32[]{:S(2)}, u32[]{:S(2)}) collective-permute-start(bf16[2,256,512]{2,1,0:T(8,128)(2,1)S(1)} %add_convert_fusion.3), channel_id=1, source_target_pairs={{8,16},{12,20},{16,8},{20,12},{9,17},{13,21},{17,9},{21,13},{10,18... | collective-permute-start | bytes 1572872 | tf_op jit(solution)/shard_map/ppermute | solution.py:426
  99.2 15.1 %copy-start.5 = (bf16[1,256,512]{2,1,0:T(8,128)(2,1)S(1)}, bf16[1,256,512]{2,1,0:T(8,128)(2,1)}, u32[]{:S(2)}) copy-start(bf16[1,256,512]{2,1,0:T(8,128)(2,1)} %copy-done.4) | copy-start | bytes 786436
  99.3 29.2 %collective-permute-start.23 = (bf16[2,256,512]{2,1,0:T(8,128)(2,1)S(1)}, bf16[2,256,512]{2,1,0:T(8,128)(2,1)S(1)}, u32[]{:S(2)}, u32[]{:S(2)}) collective-permute-start(bf16[2,256,512]{2,1,0:T(8,128)(2,1)S(1)} %add_convert_fusion), channel_id=1, source_target_pairs={{8,16},{12,20},{16,8},{20,12},{9,17},{13,21},{17,9},{21,13},{10,18... | collective-permute-start | bytes 1572872 | tf_op jit(solution)/shard_map/ppermute | solution.py:426
  105.7 48.1 %collective-permute-start.17 = (bf16[1,256,512]{2,1,0:T(8,128)(2,1)S(1)}, bf16[1,256,512]{2,1,0:T(8,128)(2,1)S(1)}, u32[]{:S(2)}, u32[]{:S(2)}) collective-permute-start(bf16[1,256,512]{2,1,0:T(8,128)(2,1)S(1)} %add_convert_fusion.5), channel_id=1, source_target_pairs={{0,8},{4,12},{8,0},{12,4},{16,24},{20,28},{24,16},{28,20},{1,9},{5... | collective-permute-start | bytes 786440 | tf_op jit(solution)/shard_map/ppermute | solution.py:426
  112.7 66.3 %collective-permute-start.32 = (bf16[2,256,1024]{2,1,0:T(8,128)(2,1)S(1)}, bf16[2,256,1024]{2,1,0:T(8,128)(2,1)S(1)}, u32[]{:S(2)}, u32[]{:S(2)}) collective-permute-start(bf16[2,256,1024]{2,1,0:T(8,128)(2,1)S(1)} %add.52.refs_11_), channel_id=1, source_target_pairs={{4,0},{0,4},{12,8},{8,12},{20,16},{16,20},{28,24},{24,28},{5,1},{1... | collective-permute-start | bytes 3145736 | tf_op jit(solution)/shard_map/ppermute | solution.py:461
  114.4 43.7 %collective-permute-start.14 = (bf16[1,256,512]{2,1,0:T(8,128)(2,1)S(1)}, bf16[1,256,512]{2,1,0:T(8,128)(2,1)S(1)}, u32[]{:S(2)}, u32[]{:S(2)}) collective-permute-start(bf16[1,256,512]{2,1,0:T(8,128)(2,1)S(1)} %add_convert_fusion.6), channel_id=1, source_target_pairs={{0,8},{4,12},{8,0},{12,4},{16,24},{20,28},{24,16},{28,20},{1,9},{5... | collective-permute-start | bytes 786440 | tf_op jit(solution)/shard_map/ppermute | solution.py:426
  128.5 32.3 %collective-permute-start.10 = (bf16[1,256,512]{2,1,0:T(8,128)(2,1)S(1)}, bf16[1,256,512]{2,1,0:T(8,128)(2,1)S(1)}, u32[]{:S(2)}, u32[]{:S(2)}) collective-permute-start(bf16[1,256,512]{2,1,0:T(8,128)(2,1)S(1)} %add_convert_fusion.7), channel_id=1, source_target_pairs={{0,8},{4,12},{8,0},{12,4},{16,24},{20,28},{24,16},{28,20},{1,9},{5... | collective-permute-start | bytes 786440 | tf_op jit(solution)/shard_map/ppermute | solution.py:426
  137.3 16.6 %copy-start.1 = (f32[256,512]{1,0:T(8,128)S(1)}, f32[256,512]{1,0:T(8,128)}, u32[]{:S(2)}) copy-start(f32[256,512]{1,0:T(8,128)} %copy-done) | copy-start | bytes 1572868
  137.3 16.6 %copy-start.6 = (f32[512]{0:T(512)S(1)}, f32[512]{0:T(512)}, u32[]{:S(2)}) copy-start(f32[512]{0:T(512)} %param.20) | copy-start | bytes 6148
  137.3 16.6 %copy-start.7 = (f32[512]{0:T(512)S(1)}, f32[512]{0:T(512)}, u32[]{:S(2)}) copy-start(f32[512]{0:T(512)} %param.21) | copy-start | bytes 6148
  153.8 15.4 %collective-permute-start.24 = (bf16[1,256,512]{2,1,0:T(8,128)(2,1)S(1)}, bf16[1,256,512]{2,1,0:T(8,128)(2,1)S(1)}, u32[]{:S(2)}, u32[]{:S(2)}) collective-permute-start(bf16[1,256,512]{2,1,0:T(8,128)(2,1)S(1)} %add_convert_fusion.4), channel_id=1, source_target_pairs={{0,8},{4,12},{8,0},{12,4},{16,24},{20,28},{24,16},{28,20},{1,9},{5... | collective-permute-start | bytes 786440 | tf_op jit(solution)/shard_map/ppermute | solution.py:426
  154.0 4.1 %copy-start.3 = (f32[256,512]{1,0:T(8,128)S(1)}, f32[256,512]{1,0:T(8,128)}, u32[]{:S(2)}) copy-start(f32[256,512]{1,0:T(8,128)} %copy-done.2) | copy-start | bytes 1572868
  163.5 15.5 %copy-start.8 = (s32[4,4]{1,0:T(4,128)S(1)}, s32[4,4]{1,0:T(4,128)}, u32[]{:S(2)}) copy-start(s32[4,4]{1,0:T(4,128)} %constant.54.clone.refs_0_) | copy-start | bytes 196
  163.5 5.7 %collective-permute-start.18 = (bf16[256,384]{1,0:T(8,128)(2,1)S(1)}, bf16[256,384]{1,0:T(8,128)(2,1)S(1)}, u32[]{:S(2)}, u32[]{:S(2)}) collective-permute-start(bf16[256,384]{1,0:T(8,128)(2,1)S(1)} %recur.6.refs_1_), channel_id=1, source_target_pairs={{0,2},{1,3},{2,0},{3,1},{4,6},{5,7},{6,4},{7,5},{8,10},{9,11},{10,... | collective-permute-start | bytes 589832 | tf_op jit(solution)/shard_map/ppermute | solution.py:342
  165.1 13.9 %collective-permute-start.19 = (bf16[256,384]{1,0:T(8,128)(2,1)S(1)}, bf16[256,384]{1,0:T(8,128)(2,1)S(1)}, u32[]{:S(2)}, u32[]{:S(2)}) collective-permute-start(bf16[256,384]{1,0:T(8,128)(2,1)S(1)} %recur.6.refs_1_), channel_id=1, source_target_pairs={{0,1},{1,0},{2,3},{3,2},{4,5},{5,4},{6,7},{7,6},{8,9},{9,8},{10,11... | collective-permute-start | bytes 589832 | tf_op jit(solution)/shard_map/ppermute | solution.py:342
  169.2 9.8 %collective-permute-start.20 = (bf16[256,384]{1,0:T(8,128)(2,1)S(1)}, bf16[256,384]{1,0:T(8,128)(2,1)S(1)}, u32[]{:S(2)}, u32[]{:S(2)}) collective-permute-start(bf16[256,384]{1,0:T(8,128)(2,1)S(1)} %collective-permute-done.18.refs_2_), channel_id=1, source_target_pairs={{0,1},{1,0},{2,3},{3,2},{4,5},{5,4},{6,7},{7,6},{8,9},{9,8},{10,11... | collective-permute-start | bytes 589832 | tf_op jit(solution)/shard_map/ppermute | solution.py:342
  170.1 4.6 %collective-permute-start.25 = (bf16[256,128]{1,0:T(8,128)(2,1)S(1)}, bf16[256,128]{1,0:T(8,128)(2,1)S(1)}, u32[]{:S(2)}, u32[]{:S(2)}) collective-permute-start(bf16[256,128]{1,0:T(8,128)(2,1)S(1)} %recur.7.refs_5_), channel_id=1, source_target_pairs={{0,2},{1,3},{2,0},{3,1},{4,6},{5,7},{6,4},{7,5},{8,10},{9,11},{10,... | collective-permute-start | bytes 196616 | tf_op jit(solution)/shard_map/ppermute | solution.py:342
  171.7 3.8 %collective-permute-start.26 = (bf16[256,128]{1,0:T(8,128)(2,1)S(1)}, bf16[256,128]{1,0:T(8,128)(2,1)S(1)}, u32[]{:S(2)}, u32[]{:S(2)}) collective-permute-start(bf16[256,128]{1,0:T(8,128)(2,1)S(1)} %recur.7.refs_5_), channel_id=1, source_target_pairs={{0,1},{1,0},{2,3},{3,2},{4,5},{5,4},{6,7},{7,6},{8,9},{9,8},{10,11... | collective-permute-start | bytes 196616 | tf_op jit(solution)/shard_map/ppermute | solution.py:342
  174.7 4.3 %collective-permute-start.27 = (bf16[256,128]{1,0:T(8,128)(2,1)S(1)}, bf16[256,128]{1,0:T(8,128)(2,1)S(1)}, u32[]{:S(2)}, u32[]{:S(2)}) collective-permute-start(bf16[256,128]{1,0:T(8,128)(2,1)S(1)} %recur.7.refs_5_), channel_id=1, source_target_pairs={{0,3},{1,2},{2,1},{3,0},{4,7},{5,6},{6,5},{7,4},{8,11},{9,10},{10,... | collective-permute-start | bytes 196616 | tf_op jit(solution)/shard_map/ppermute | solution.py:342

commit v3 on v2

--- a/solution.py
+++ b/solution.py
@@ -130,9 +130,10 @@
 
 
 def taken_kernel(
-    accepted, state, prev_forget, prev_value, bounds, taken, held, forget, values, come, gone, side, *, proposals, seqs
+    accepted, state, prev_forget, prev_value, bounds, *refs, proposals, seqs, start
 ):
-    count, heads, keys, vals = state.shape
+    taken, held, forget, values, come, gone, side = refs[-7:]
+    count, heads, keys, vals = held.shape
     steps = count // seqs
     rows = seqs * proposals
     position = position_of((rows, keys), proposals)
@@ -140,19 +141,19 @@
 
     def copy_in(i):
         here = pl.ds(i * seqs, seqs)
-        return pltpu.make_async_copy(state.at[here], held.at[here], come.at[i])
+        return pltpu.make_async_copy(state.at[pl.ds(start + i * seqs, seqs)], held.at[here], come.at[i])
 
     def copy_out(i):
         here = pl.ds(i * seqs, seqs)
-        return pltpu.make_async_copy(held.at[here], taken.at[here], gone.at[i])
+        return pltpu.make_async_copy(held.at[here], taken.at[pl.ds(start + i * seqs, seqs)], gone.at[i])
 
     fetches = [
-        pltpu.make_async_copy(prev_forget, forget, side.at[0]),
-        pltpu.make_async_copy(prev_value, values, side.at[1]),
+        pltpu.make_async_copy(prev_forget.at[pl.ds(start, count)], forget, side.at[0]),
+        pltpu.make_async_copy(prev_value.at[pl.ds(start, count)], values, side.at[1]),
     ]
     for copy in fetches:
         copy.start()
-    ahead = min(3, steps)
+    ahead = min(2, steps)
     for i in range(ahead):
         copy_in(i).start()
     for copy in fetches:
@@ -169,7 +170,7 @@
         new = jnp.concatenate([values[first + seq].astype(F32) for seq in range(seqs)], axis=0).astype(BF16)
         taking = jnp.zeros((rows, keys), jnp.int32)
         for seq in range(seqs):
-            taking = jnp.where(owner == seq, accepted[first + seq], taking)
+            taking = jnp.where(owner == seq, accepted[start + first + seq], taking)
         kept = position < taking
         decays, addeds = [], []
         for head in range(heads):
@@ -374,22 +375,31 @@
     bounds = lower_bound.reshape(1, width)
     some = 8 if seqs % 8 == 0 else seqs
     one_spec = pl.BlockSpec((1, width), lambda i: (0, 0))
-    taken = pl.pallas_call(
-        lambda *refs: taken_kernel(*refs, proposals=proposals, seqs=some),
-        out_shape=jax.ShapeDtypeStruct(state.shape, F32),
-        in_specs=[SMEM, HBM, HBM, HBM, VMEM],
-        out_specs=HBM,
-        scratch_shapes=[
-            pltpu.VMEM(state.shape, F32),
-            pltpu.VMEM(prev_forget.shape, BF16),
-            pltpu.VMEM(prev_value.shape, BF16),
-            pltpu.SemaphoreType.DMA((seqs // some,)),
-            pltpu.SemaphoreType.DMA((seqs // some,)),
-            pltpu.SemaphoreType.DMA((2,)),
-        ],
-        compiler_params=room(24),
-        name="taken",
-    )(*in_hbm(accepted, state, prev_forget, prev_value, bounds))
+    steps = seqs // some
+    middle = max(1, steps * 5 // 8)
+    taken = None
+    for first, last in [(0, middle), (middle, steps)]:
+        if first == last:
+            continue
+        done = [] if taken is None else [taken]
+        span = (last - first) * some
+        taken = pl.pallas_call(
+            lambda *refs, start=first * some: taken_kernel(*refs, proposals=proposals, seqs=some, start=start),
+            out_shape=jax.ShapeDtypeStruct(state.shape, F32),
+            in_specs=[SMEM, HBM, HBM, HBM, VMEM] + [HBM] * len(done),
+            out_specs=HBM,
+            input_output_aliases={5: 0} if done else {},
+            scratch_shapes=[
+                pltpu.VMEM((span, *state.shape[1:]), F32),
+                pltpu.VMEM((span, *prev_forget.shape[1:]), BF16),
+                pltpu.VMEM((span, *prev_value.shape[1:]), BF16),
+                pltpu.SemaphoreType.DMA((last - first,)),
+                pltpu.SemaphoreType.DMA((last - first,)),
+                pltpu.SemaphoreType.DMA((2,)),
+            ],
+            compiler_params=room(24),
+            name="taken",
+        )(*in_hbm(accepted, state, prev_forget, prev_value, bounds, *done))
 
     def added(a, b):
         return (a.astype(F32) + b.astype(F32)).astype(BF16)

time: 182 us -> 185 us (1.016)
  Pallas kernels: 42.9 us -> 45.8 us
  other arithmetic: 4.99 us -> 6.96 us
    pallas_call x1 -> x2, Pallas kernels: 16.4 us -> 19.4 us  [on_device(): pl.pallas_call(lambda *refs, start=first * some: taken_kernel(*refs, prop...]
  transfers between devices with their start and end apart: 33 -> 33, of which waited for: 12 -> 12; matrix products, arithmetic and copies ran while one was open for 3% -> 4% of each run, Pallas kernels for 22% -> 23%
where the time goes in v3:
time: 185 us
  starting transfers between devices  65.9 us (36%)
  waiting for transfers between devices  62.7 us (34%)
  Pallas kernels  45.8 us (25%)
  other arithmetic  6.96 us (4%)
  local copies, waits for them, and re-layouts  2.33 us (1%)
    ppermute x8, starting transfers between devices, summed(): got = lax.ppermute(out, 'kv', mirrored(size, size - 1, size))  30.2 us
    pallas_call x2, Pallas kernels, on_device(): pl.pallas_call(lambda *refs, start=first * some: taken_kernel(*refs, prop...  19.4 us
    ppermute x4, waiting for transfers between devices, on_device(): lax.ppermute(weight, 'kv', around(t))  15.5 us
    ppermute x4, waiting for transfers between devices, summed(): got = lax.ppermute(out, 'kv', mirrored(size, hop - 1, hop))  13.2 us
    ppermute x4, starting transfers between devices, summed(): got = lax.ppermute(out, 'kv', mirrored(size, hop - 1, hop))  12.8 us
    ppermute x9, waiting for transfers between devices, swap(): return lax.ppermute(value, 'tp', [(t, t ^ bit) for t in range(tp)])  10.6 us
    pallas_call x4, Pallas kernels, on_device(): pl.pallas_call(lambda *refs, head=head, spare=spare: recur_kernel(*refs,...  10.3 us
    ppermute x3, waiting for transfers between devices, on_device(): lax.ppermute(mine[r - 1], 'kv', groups([(g, g ^ r) for g in range(ring)]))  9.76 us
  transfers between devices with their start and end apart: 33, of which 12 were waited for; matrix products, arithmetic and copies ran while one was open for 4% of the time, Pallas kernels for 23%

profile of v3, /device:TPU:0, one launch (start us, length us, event | category | flops | bytes accessed | tf_op | source)
XLA Modules:
  0.0 184.6 jit_solution(3303672854604744455)
XLA Ops:
  0.6 3.1 %collective-permute-start.28 = (bf16[1,256,1024]{2,1,0:T(8,128)(2,1)}, bf16[1,256,1024]{2,1,0:T(8,128)(2,1)S(1)}, u32[]{:S(2)}, u32[]{:S(2)}) collective-permute-start(bf16[1,256,1024]{2,1,0:T(8,128)(2,1)} %bitcast.14), channel_id=1, source_target_pairs={{0,8},{4,12},{8,0},{12,4},{16,24},{20,28},{24,16},{28,20},{1,9},{5... | collective-permute-start | bytes 1572872 | tf_op jit(solution)/shard_map/ppermute | solution.py:451
  3.7 4.6 %norm.1 = (bf16[2,256,512]{2,1,0:T(8,128)(2,1)S(1)}, bf16[2,128,512]{2,1,0:T(8,128)(2,1)S(1)}, bf16[2,128,512]{2,1,0:T(8,128)(2,1)S(1)}, bf16[2,128,512]{2,1,0:T...) custom-call(bf16[256,4096]{1,0:T(8,128)(2,1)} %refs_0_.4, ...), custom_call_target="tpu_custom_call" | custom-call | tf_op jit(solution)/shard_map/norm/pallas_call | solution.py:350
  8.5 3.0 %collective-permute-start.2 = (bf16[2,128,512]{2,1,0:T(8,128)(2,1)S(1)}, bf16[2,128,512]{2,1,0:T(8,128)(2,1)S(1)}, u32[]{:S(2)}, u32[]{:S(2)}) collective-permute-start(bf16[2,128,512]{2,1,0:T(8,128)(2,1)S(1)} %get-tuple-element.27), channel_id=1, source_target_pairs={{0,16},{4,20},{8,24},{12,28},{16,0},{20,4},{24,8},{28,12},{1,17},{... | collective-permute-start | bytes 786440 | tf_op jit(solution)/shard_map/ppermute | solution.py:370
  11.5 1.3 collective-permute-start.4
  12.8 1.5 collective-permute-start.6
  14.4 8.0 %collective-permute-done.28 = bf16[1,256,1024]{2,1,0:T(8,128)(2,1)S(1)} collective-permute-done((bf16[1,256,1024]{2,1,0:T(8,128)(2,1)}, bf16[1,256,1024]{2,1,0:T(8,128)(2,1)S(1)}, u32[]{:S(2)}, u32[]{:S(2)}) %collective-permute-start.28) | collective-permute-done | bytes 524320 | tf_op jit(solution)/shard_map/ppermute | solution.py:451
  22.4 1.1 pad_maximum_fusion.refs_9_
  23.5 1.7 collective-permute-start.30
  25.2 1.9 %collective-permute-done.refs_1_ = bf16[2,128,512]{2,1,0:T(8,128)(2,1)S(1)} collective-permute-done((bf16[2,128,512]{2,1,0:T(8,128)(2,1)S(1)}, bf16[2,128,512]{2,1,0:T(8,128)(2,1)S(1)}, u32[]{:S(2)}, u32[]{:S(2)}) %collective-permute-start) | collective-permute-done | bytes 262176 | tf_op jit(solution)/shard_map/ppermute | solution.py:370
  27.6 7.4 %collective-permute-done.4.refs_5_ = bf16[2,128,512]{2,1,0:T(8,128)(2,1)S(1)} collective-permute-done((bf16[2,128,512]{2,1,0:T(8,128)(2,1)S(1)}, bf16[2,128,512]{2,1,0:T(8,128)(2,1)S(1)}, u32[]{:S(2)}, u32[]{:S(2)}) %collective-permute-start.4) | collective-permute-done | bytes 262176 | tf_op jit(solution)/shard_map/ppermute | solution.py:370
  35.0 1.5 collective-permute-start.11
  37.1 1.5 collective-permute-start.7
  38.6 2.0 %project.4 = (f32[256,512]{1,0:T(8,128)S(1)}, bf16[1,256,512]{2,1,0:T(8,128)(2,1)S(1)}, bf16[2,256,512]{2,1,0:T(8,128)(2,1)}, bf16[1024,1024]{1,0:T(8,128)(2,1)S(1)}) custom-call(bf16[2,256,512]{2,1,0:T(8,128)(2,1)S(1)} %get-tuple-element.25.refs_0_, bf16[2,128,512]{2,1,0:T(8,128)(2,1)S(1)} %collective-permute-done.refs_1_, ...), custom_call_target="tpu_custom_call" | custom-call | tf_op jit(solution)/shard_map/project/pallas_call | solution.py:418
  41.4 4.1 %collective-permute-start.15 = (bf16[2,256,512]{2,1,0:T(8,128)(2,1)}, bf16[2,256,512]{2,1,0:T(8,128)(2,1)}, u32[]{:S(2)}, u32[]{:S(2)}) collective-permute-start(bf16[2,256,512]{2,1,0:T(8,128)(2,1)} %get-tuple-element.40), channel_id=1, source_target_pairs={{0,8},{4,12},{24,16},{28,20},{1,9},{5,13},{25,17},{29,21},{2,10},{... | collective-permute-start | bytes 1572872 | tf_op jit(solution)/shard_map/ppermute | solution.py:434
  45.4 4.4 %collective-permute-done.11.refs_2_ = bf16[512,512]{1,0:T(8,128)(2,1)S(1)} collective-permute-done((bf16[512,512]{1,0:T(8,128)(2,1)S(1)}, bf16[512,512]{1,0:T(8,128)(2,1)S(1)}, u32[]{:S(2)}, u32[]{:S(2)}) %collective-permute-start.11) | collective-permute-done | bytes 524320 | tf_op jit(solution)/shard_map/ppermute | solution.py:367
  49.8 1.8 project.6
  53.2 4.1 %collective-permute-start.12 = (bf16[2,256,512]{2,1,0:T(8,128)(2,1)}, bf16[2,256,512]{2,1,0:T(8,128)(2,1)}, u32[]{:S(2)}, u32[]{:S(2)}) collective-permute-start(bf16[2,256,512]{2,1,0:T(8,128)(2,1)} %get-tuple-element.37), channel_id=1, source_target_pairs={{0,8},{4,12},{24,16},{28,20},{1,9},{5,13},{25,17},{29,21},{2,10},{... | collective-permute-start | bytes 1572872 | tf_op jit(solution)/shard_map/ppermute | solution.py:434
  57.3 3.9 %collective-permute-done.21.refs_2_ = bf16[512,512]{1,0:T(8,128)(2,1)} collective-permute-done((bf16[512,512]{1,0:T(8,128)(2,1)}, bf16[512,512]{1,0:T(8,128)(2,1)}, u32[]{:S(2)}, u32[]{:S(2)}) %collective-permute-start.21) | collective-permute-done | bytes 524320 | tf_op jit(solution)/shard_map/ppermute | solution.py:367
  61.2 1.5 collective-permute-start.29
  62.7 2.4 %project.7 = (f32[256,512]{1,0:T(8,128)S(1)}, bf16[1,256,512]{2,1,0:T(8,128)(2,1)S(1)}, bf16[2,256,512]{2,1,0:T(8,128)(2,1)S(1)}) custom-call(bf16[1024,1024]{1,0:T(8,128)(2,1)S(1)} %get-tuple-element.30.refs_0_, bf16[512,512]{1,0:T(8,128)(2,1)} %get-tuple-element.43.refs_1_, bf16[512,512]{1,0:T(8,128)(2,1)} %collective-permute-done.21.refs_2_), custom_call_target="tpu_custom_call" | custom-call | tf_op jit(solution)/shard_map/project/pallas_call | solution.py:418
  65.1 7.3 %collective-permute-done.7.refs_2_ = bf16[512,512]{1,0:T(8,128)(2,1)} collective-permute-done((bf16[512,512]{1,0:T(8,128)(2,1)}, bf16[512,512]{1,0:T(8,128)(2,1)}, u32[]{:S(2)}, u32[]{:S(2)}) %collective-permute-start.7) | collective-permute-done | bytes 524320 | tf_op jit(solution)/shard_map/ppermute | solution.py:367
  72.4 3.3 %collective-permute-start.22 = (bf16[2,256,512]{2,1,0:T(8,128)(2,1)S(1)}, bf16[2,256,512]{2,1,0:T(8,128)(2,1)S(1)}, u32[]{:S(2)}, u32[]{:S(2)}) collective-permute-start(bf16[2,256,512]{2,1,0:T(8,128)(2,1)S(1)} %get-tuple-element.45), channel_id=1, source_target_pairs={{0,8},{4,12},{24,16},{28,20},{1,9},{5,13},{25,17},{29,21},{2,10},{... | collective-permute-start | bytes 1572872 | tf_op jit(solution)/shard_map/ppermute | solution.py:434
  75.7 2.5 %project.5 = (f32[256,512]{1,0:T(8,128)S(1)}, bf16[1,256,512]{2,1,0:T(8,128)(2,1)S(1)}, bf16[2,256,512]{2,1,0:T(8,128)(2,1)S(1)}) custom-call(bf16[1024,1024]{1,0:T(8,128)(2,1)S(1)} %get-tuple-element.30.refs_0_, bf16[512,512]{1,0:T(8,128)(2,1)} %get-tuple-element.31.refs_1_, bf16[512,512]{1,0:T(8,128)(2,1)} %collective-permute-done.7.refs_2_), custom_call_target="tpu_custom_call" | custom-call | tf_op jit(solution)/shard_map/project/pallas_call | solution.py:418
  78.2 1.3 collective-permute-start.8
  79.5 1.3 collective-permute-start.31
  80.8 1.3 add_convert_fusion.1
  82.9 1.3 add_convert_fusion.2
  84.2 13.2 %collective-permute-done.8 = bf16[2,256,512]{2,1,0:T(8,128)(2,1)S(1)} collective-permute-done((bf16[2,256,512]{2,1,0:T(8,128)(2,1)S(1)}, bf16[2,256,512]{2,1,0:T(8,128)(2,1)S(1)}, u32[]{:S(2)}, u32[]{:S(2)}) %collective-permute-start.8) | collective-permute-done | bytes 524320 | tf_op jit(solution)/shard_map/ppermute | solution.py:434
  99.1 0.9 collective-permute-start.23
  100.1 5.5 %collective-permute-done.31 = bf16[2,256,1024]{2,1,0:T(8,128)(2,1)S(1)} collective-permute-done((bf16[2,256,1024]{2,1,0:T(8,128)(2,1)}, bf16[2,256,1024]{2,1,0:T(8,128)(2,1)S(1)}, u32[]{:S(2)}, u32[]{:S(2)}) %collective-permute-start.31) | collective-permute-done | bytes 1048608 | tf_op jit(solution)/shard_map/ppermute | solution.py:455
  105.6 5.2 %collective-permute-start.17 = (bf16[1,256,512]{2,1,0:T(8,128)(2,1)S(1)}, bf16[1,256,512]{2,1,0:T(8,128)(2,1)S(1)}, u32[]{:S(2)}, u32[]{:S(2)}) collective-permute-start(bf16[1,256,512]{2,1,0:T(8,128)(2,1)S(1)} %add_convert_fusion.5), channel_id=1, source_target_pairs={{0,8},{4,12},{8,0},{12,4},{16,24},{20,28},{24,16},{28,20},{1,9},{5... | collective-permute-start | bytes 786440 | tf_op jit(solution)/shard_map/ppermute | solution.py:436
  110.8 1.6 add.52.refs_11_
  112.5 1.6 collective-permute-start.32
  114.0 1.0 add_convert_fusion.6
  115.1 13.2 %collective-permute-start.14 = (bf16[1,256,512]{2,1,0:T(8,128)(2,1)S(1)}, bf16[1,256,512]{2,1,0:T(8,128)(2,1)S(1)}, u32[]{:S(2)}, u32[]{:S(2)}) collective-permute-start(bf16[1,256,512]{2,1,0:T(8,128)(2,1)S(1)} %add_convert_fusion.6), channel_id=1, source_target_pairs={{0,8},{4,12},{8,0},{12,4},{16,24},{20,28},{24,16},{28,20},{1,9},{5... | collective-permute-start | bytes 786440 | tf_op jit(solution)/shard_map/ppermute | solution.py:436
  128.4 8.8 %collective-permute-start.10 = (bf16[1,256,512]{2,1,0:T(8,128)(2,1)S(1)}, bf16[1,256,512]{2,1,0:T(8,128)(2,1)S(1)}, u32[]{:S(2)}, u32[]{:S(2)}) collective-permute-start(bf16[1,256,512]{2,1,0:T(8,128)(2,1)S(1)} %add_convert_fusion.7), channel_id=1, source_target_pairs={{0,8},{4,12},{8,0},{12,4},{16,24},{20,28},{24,16},{28,20},{1,9},{5... | collective-permute-start | bytes 786440 | tf_op jit(solution)/shard_map/ppermute | solution.py:436
  137.2 11.2 %taken.2.refs_5_ = f32[64,4,128,128]{3,2,1,0:T(8,128)} custom-call(s32[64]{0:T(128)} %refs_0_.6, f32[64,4,128,128]{3,2,1,0:T(8,128)} %refs_1_.3, bf16[64,4,512]{2,1,0:T(4,128)(2,1)} %refs_2_.5, bf16[64,4,512]{2,1,0:T(4,128)(2,1)} %refs_3_.5, f32[1,512]{1,0:T(1,128)} %bitcast.4), custom_call_target="tpu_custom_call" | custom-call | tf_op jit(solution)/shard_map/taken/pallas_call | solution.py:386
  148.4 8.2 %taken.3.refs_3_.refs_6_ = f32[64,4,128,128]{3,2,1,0:T(8,128)} custom-call(s32[64]{0:T(128)} %refs_0_.6, f32[64,4,128,128]{3,2,1,0:T(8,128)} %refs_1_.3, bf16[64,4,512]{2,1,0:T(4,128)(2,1)} %refs_2_.5, bf16[64,4,512]{2,1,0:T(4,128)(2,1)} %refs_3_.5, f32[1,512]{1,0:T(1,128)} %bitcast.5, f32[64,4,128,128]{3,2,1,0:T(8,128)} %taken.2.refs_5_), custom_call_target="tpu_custom_call", output_to_operand_aliasing={{}: (5, {})} | custom-call | tf_op jit(solution)/shard_map/taken/pallas_call | solution.py:386
  156.8 4.1 %recur.4 = (bf16[256,128]{1,0:T(8,128)(2,1)S(1)}, bf16[64,1,128,128]{3,2,1,0:T(8,128)(2,1)S(1)}) custom-call(f32[256,512]{1,0:T(8,128)S(1)} %copy-done.1, bf16[2,256,512]{2,1,0:T(8,128)(2,1)S(1)} %collective-permute-done.16.refs_1_, bf16[1,256,512]{2,1,0:T(8,128)(2,1)S(1)} %collective-permute-done.17.refs_2_, f32[64,4,128,128]{3,2,1,0:T(8,128)} %taken.3.refs_3_.refs_6_, ...), custom_call_target="tpu_custom_call" | custom-call | tf_op jit(solution)/shard_map/recur/pallas_call | solution.py:511
  161.0 2.7 %recur.5.refs_6_ = bf16[256,256]{1,0:T(8,128)(2,1)S(1)} custom-call(f32[256,512]{1,0:T(8,128)S(1)} %copy-done.3, bf16[2,256,512]{2,1,0:T(8,128)(2,1)S(1)} %collective-permute-done.13.refs_1_, bf16[1,256,512]{2,1,0:T(8,128)(2,1)S(1)} %collective-permute-done.14.refs_2_, f32[64,4,128,128]{3,2,1,0:T(8,128)} %taken.3.refs_3_.refs_6_, f32[1,512]{1,0:T(1,128)S(1)} %bitcast.7, ...), custom_call_target="tpu_custom_call" | custom-call | tf_op jit(solution)/shard_map/recur/pallas_call | solution.py:511
  163.7 2.7 %recur.6.refs_1_ = bf16[256,384]{1,0:T(8,128)(2,1)S(1)} custom-call(f32[256,512]{1,0:T(8,128)S(1)} %get-tuple-element.32.refs_0_, bf16[2,256,512]{2,1,0:T(8,128)(2,1)S(1)} %collective-permute-done.9.refs_1_, bf16[1,256,512]{2,1,0:T(8,128)(2,1)S(1)} %collective-permute-done.10.refs_2_, f32[64,4,128,128]{3,2,1,0:T(8,128)} %taken.3.refs_3_.refs_6_, ...), custom_call_target="tpu_custom_call" | custom-call | tf_op jit(solution)/shard_map/recur/pallas_call | solution.py:511
  166.4 1.5 collective-permute-start.18
  167.9 4.2 %collective-permute-done.18.refs_2_ = bf16[256,384]{1,0:T(8,128)(2,1)S(1)} collective-permute-done((bf16[256,384]{1,0:T(8,128)(2,1)S(1)}, bf16[256,384]{1,0:T(8,128)(2,1)S(1)}, u32[]{:S(2)}, u32[]{:S(2)}) %collective-permute-start.18) | collective-permute-done | bytes 196640 | tf_op jit(solution)/shard_map/ppermute | solution.py:343
  172.1 0.8 recur.7.refs_5_
  173.0 1.5 collective-permute-start.25
  174.7 2.8 %collective-permute-done.25.refs_6_ = bf16[256,128]{1,0:T(8,128)(2,1)S(1)} collective-permute-done((bf16[256,128]{1,0:T(8,128)(2,1)S(1)}, bf16[256,128]{1,0:T(8,128)(2,1)S(1)}, u32[]{:S(2)}, u32[]{:S(2)}) %collective-permute-start.25) | collective-permute-done | bytes 65568 | tf_op jit(solution)/shard_map/ppermute | solution.py:343
  178.3 3.6 %collective-permute-done.27.refs_8_ = bf16[256,128]{1,0:T(8,128)(2,1)S(1)} collective-permute-done((bf16[256,128]{1,0:T(8,128)(2,1)S(1)}, bf16[256,128]{1,0:T(8,128)(2,1)S(1)}, u32[]{:S(2)}, u32[]{:S(2)}) %collective-permute-start.27) | collective-permute-done | bytes 65568 | tf_op jit(solution)/shard_map/ppermute | solution.py:343
  181.9 2.7 %mix.1 = bf16[256,1024]{1,0:T(8,128)(2,1)} custom-call(s32[4,4]{1,0:T(4,128)S(1)} %copy-done.7, bf16[256,384]{1,0:T(8,128)(2,1)S(1)} %recur.6.refs_1_, bf16[256,384]{1,0:T(8,128)(2,1)S(1)} %collective-permute-done.18.refs_2_, bf16[256,384]{1,0:T(8,128)(2,1)S(1)} %collective-permute-done.19.refs_3_, bf16[256,384]{1,0:T(8,128)(2,1)S(1)} %collective-permute-done.20.refs_4_, ...), custom_call_target="tpu_custom_call" | custom-call | tf_op jit(solution)/shard_map/mix/pallas_call | solution.py:537
  (56 shorter events, 7.1 us)
Async XLA Ops:
  0.6 21.7 %collective-permute-start.28 = (bf16[1,256,1024]{2,1,0:T(8,128)(2,1)}, bf16[1,256,1024]{2,1,0:T(8,128)(2,1)S(1)}, u32[]{:S(2)}, u32[]{:S(2)}) collective-permute-start(bf16[1,256,1024]{2,1,0:T(8,128)(2,1)} %bitcast.14), channel_id=1, source_target_pairs={{0,8},{4,12},{8,0},{12,4},{16,24},{20,28},{24,16},{28,20},{1,9},{5... | collective-permute-start | bytes 1572872 | tf_op jit(solution)/shard_map/ppermute | solution.py:451
  8.4 18.7 %collective-permute-start = (bf16[2,128,512]{2,1,0:T(8,128)(2,1)S(1)}, bf16[2,128,512]{2,1,0:T(8,128)(2,1)S(1)}, u32[]{:S(2)}, u32[]{:S(2)}) collective-permute-start(bf16[2,128,512]{2,1,0:T(8,128)(2,1)S(1)} %get-tuple-element.26), channel_id=1, source_target_pairs={{0,8},{4,12},{8,0},{12,4},{16,24},{20,28},{24,16},{28,20},{1,9},{5... | collective-permute-start | bytes 786440 | tf_op jit(solution)/shard_map/ppermute | solution.py:370
  8.5 19.1 %collective-permute-start.2 = (bf16[2,128,512]{2,1,0:T(8,128)(2,1)S(1)}, bf16[2,128,512]{2,1,0:T(8,128)(2,1)S(1)}, u32[]{:S(2)}, u32[]{:S(2)}) collective-permute-start(bf16[2,128,512]{2,1,0:T(8,128)(2,1)S(1)} %get-tuple-element.27), channel_id=1, source_target_pairs={{0,16},{4,20},{8,24},{12,28},{16,0},{20,4},{24,8},{28,12},{1,17},{... | collective-permute-start | bytes 786440 | tf_op jit(solution)/shard_map/ppermute | solution.py:370
  11.5 23.5 %collective-permute-start.4 = (bf16[2,128,512]{2,1,0:T(8,128)(2,1)S(1)}, bf16[2,128,512]{2,1,0:T(8,128)(2,1)S(1)}, u32[]{:S(2)}, u32[]{:S(2)}) collective-permute-start(bf16[2,128,512]{2,1,0:T(8,128)(2,1)S(1)} %get-tuple-element.28), channel_id=1, source_target_pairs={{0,24},{4,28},{8,16},{12,20},{16,8},{20,12},{24,0},{28,4},{1,25},{... | collective-permute-start | bytes 786440 | tf_op jit(solution)/shard_map/ppermute | solution.py:370
  12.8 25.7 %collective-permute-start.6 = (bf16[512,512]{1,0:T(8,128)(2,1)S(1)}, bf16[512,512]{1,0:T(8,128)(2,1)S(1)}, u32[]{:S(2)}, u32[]{:S(2)}) collective-permute-start(bf16[512,512]{1,0:T(8,128)(2,1)S(1)} %get-tuple-element.29.refs_7_), channel_id=1, source_target_pairs={{4,0},{0,4},{12,8},{8,12},{20,16},{16,20},{28,24},{24,28},{5,1},{1... | collective-permute-start | bytes 1572872 | tf_op jit(solution)/shard_map/ppermute | solution.py:367
  23.5 56.0 %collective-permute-start.30 = (bf16[2,256,1024]{2,1,0:T(8,128)(2,1)S(1)}, bf16[2,256,1024]{2,1,0:T(8,128)(2,1)}, u32[]{:S(2)}, u32[]{:S(2)}) collective-permute-start(bf16[2,256,1024]{2,1,0:T(8,128)(2,1)S(1)} %pad_maximum_fusion.refs_9_), channel_id=1, source_target_pairs={{8,16},{12,20},{16,8},{20,12},{9,17},{13,21},{17,9},{21,13},{10,18... | collective-permute-start | bytes 3145736 | tf_op jit(solution)/shard_map/ppermute | solution.py:451
  27.1 7.9 %collective-permute-start.1 = (bf16[2,128,512]{2,1,0:T(8,128)(2,1)S(1)}, bf16[2,128,512]{2,1,0:T(8,128)(2,1)S(1)}, u32[]{:S(2)}, u32[]{:S(2)}) collective-permute-start(bf16[2,128,512]{2,1,0:T(8,128)(2,1)S(1)} %collective-permute-done.refs_1_), channel_id=1, source_target_pairs={{0,1},{1,0},{2,3},{3,2},{4,5},{5,4},{6,7},{7,6},{8,9},{9,8},{10,11... | collective-permute-start | bytes 786440 | tf_op jit(solution)/shard_map/ppermute | solution.py:343
  27.6 9.0 %collective-permute-start.3 = (bf16[2,128,512]{2,1,0:T(8,128)(2,1)S(1)}, bf16[2,128,512]{2,1,0:T(8,128)(2,1)S(1)}, u32[]{:S(2)}, u32[]{:S(2)}) collective-permute-start(bf16[2,128,512]{2,1,0:T(8,128)(2,1)S(1)} %collective-permute-done.2.refs_3_), channel_id=1, source_target_pairs={{0,1},{1,0},{2,3},{3,2},{4,5},{5,4},{6,7},{7,6},{8,9},{9,8},{10,11... | collective-permute-start | bytes 786440 | tf_op jit(solution)/shard_map/ppermute | solution.py:343
  35.0 2.0 %collective-permute-start.5 = (bf16[2,128,512]{2,1,0:T(8,128)(2,1)S(1)}, bf16[2,128,512]{2,1,0:T(8,128)(2,1)S(1)}, u32[]{:S(2)}, u32[]{:S(2)}) collective-permute-start(bf16[2,128,512]{2,1,0:T(8,128)(2,1)S(1)} %collective-permute-done.4.refs_5_), channel_id=1, source_target_pairs={{0,1},{1,0},{2,3},{3,2},{4,5},{5,4},{6,7},{7,6},{8,9},{9,8},{10,11... | collective-permute-start | bytes 786440 | tf_op jit(solution)/shard_map/ppermute | solution.py:343
  35.0 14.8 %collective-permute-start.11 = (bf16[512,512]{1,0:T(8,128)(2,1)S(1)}, bf16[512,512]{1,0:T(8,128)(2,1)S(1)}, u32[]{:S(2)}, u32[]{:S(2)}) collective-permute-start(bf16[512,512]{1,0:T(8,128)(2,1)S(1)} %get-tuple-element.35.refs_1_), channel_id=1, source_target_pairs={{4,0},{0,4},{12,8},{8,12},{20,16},{16,20},{28,24},{24,28},{5,1},{1... | collective-permute-start | bytes 1572872 | tf_op jit(solution)/shard_map/ppermute | solution.py:367
  36.6 24.6 %collective-permute-start.21 = (bf16[512,512]{1,0:T(8,128)(2,1)}, bf16[512,512]{1,0:T(8,128)(2,1)}, u32[]{:S(2)}, u32[]{:S(2)}) collective-permute-start(bf16[512,512]{1,0:T(8,128)(2,1)} %get-tuple-element.43.refs_1_), channel_id=1, source_target_pairs={{4,0},{0,4},{12,8},{8,12},{20,16},{16,20},{28,24},{24,28},{5,1},{1... | collective-permute-start | bytes 1572872 | tf_op jit(solution)/shard_map/ppermute | solution.py:367
  37.1 35.3 %collective-permute-start.7 = (bf16[512,512]{1,0:T(8,128)(2,1)}, bf16[512,512]{1,0:T(8,128)(2,1)}, u32[]{:S(2)}, u32[]{:S(2)}) collective-permute-start(bf16[512,512]{1,0:T(8,128)(2,1)} %get-tuple-element.31.refs_1_), channel_id=1, source_target_pairs={{4,0},{0,4},{12,8},{8,12},{20,16},{16,20},{28,24},{24,28},{5,1},{1... | collective-permute-start | bytes 1572872 | tf_op jit(solution)/shard_map/ppermute | solution.py:367
  40.6 0.8 copy-start
  41.4 36.8 %collective-permute-start.15 = (bf16[2,256,512]{2,1,0:T(8,128)(2,1)}, bf16[2,256,512]{2,1,0:T(8,128)(2,1)}, u32[]{:S(2)}, u32[]{:S(2)}) collective-permute-start(bf16[2,256,512]{2,1,0:T(8,128)(2,1)} %get-tuple-element.40), channel_id=1, source_target_pairs={{0,8},{4,12},{24,16},{28,20},{1,9},{5,13},{25,17},{29,21},{2,10},{... | collective-permute-start | bytes 1572872 | tf_op jit(solution)/shard_map/ppermute | solution.py:434
  51.6 0.8 copy-start.2
  52.4 0.7 copy-start.4
  53.2 29.0 %collective-permute-start.12 = (bf16[2,256,512]{2,1,0:T(8,128)(2,1)}, bf16[2,256,512]{2,1,0:T(8,128)(2,1)}, u32[]{:S(2)}, u32[]{:S(2)}) collective-permute-start(bf16[2,256,512]{2,1,0:T(8,128)(2,1)} %get-tuple-element.37), channel_id=1, source_target_pairs={{0,8},{4,12},{24,16},{28,20},{1,9},{5,13},{25,17},{29,21},{2,10},{... | collective-permute-start | bytes 1572872 | tf_op jit(solution)/shard_map/ppermute | solution.py:434
  61.2 113.3 %collective-permute-start.29 = (bf16[2,256,1024]{2,1,0:T(8,128)(2,1)S(1)}, bf16[2,256,1024]{2,1,0:T(8,128)(2,1)S(1)}, u32[]{:S(2)}, u32[]{:S(2)}) collective-permute-start(bf16[2,256,1024]{2,1,0:T(8,128)(2,1)S(1)} %pad_maximum_fusion.refs_9_), channel_id=1, source_target_pairs={{4,0},{0,4},{12,8},{8,12},{20,16},{16,20},{28,24},{24,28},{5,1},{1... | collective-permute-start | bytes 3145736 | tf_op jit(solution)/shard_map/ppermute | solution.py:471
  72.4 25.9 %collective-permute-start.22 = (bf16[2,256,512]{2,1,0:T(8,128)(2,1)S(1)}, bf16[2,256,512]{2,1,0:T(8,128)(2,1)S(1)}, u32[]{:S(2)}, u32[]{:S(2)}) collective-permute-start(bf16[2,256,512]{2,1,0:T(8,128)(2,1)S(1)} %get-tuple-element.45), channel_id=1, source_target_pairs={{0,8},{4,12},{24,16},{28,20},{1,9},{5,13},{25,17},{29,21},{2,10},{... | collective-permute-start | bytes 1572872 | tf_op jit(solution)/shard_map/ppermute | solution.py:434
  78.2 19.2 %collective-permute-start.8 = (bf16[2,256,512]{2,1,0:T(8,128)(2,1)S(1)}, bf16[2,256,512]{2,1,0:T(8,128)(2,1)S(1)}, u32[]{:S(2)}, u32[]{:S(2)}) collective-permute-start(bf16[2,256,512]{2,1,0:T(8,128)(2,1)S(1)} %get-tuple-element.33), channel_id=1, source_target_pairs={{0,8},{4,12},{24,16},{28,20},{1,9},{5,13},{25,17},{29,21},{2,10},{... | collective-permute-start | bytes 1572872 | tf_op jit(solution)/shard_map/ppermute | solution.py:434
  79.5 26.1 %collective-permute-start.31 = (bf16[2,256,1024]{2,1,0:T(8,128)(2,1)}, bf16[2,256,1024]{2,1,0:T(8,128)(2,1)S(1)}, u32[]{:S(2)}, u32[]{:S(2)}) collective-permute-start(bf16[2,256,1024]{2,1,0:T(8,128)(2,1)} %collective-permute-done.30), channel_id=1, source_target_pairs={{8,0},{12,4},{16,24},{20,28},{9,1},{13,5},{17,25},{21,29},{10,2},{... | collective-permute-start | bytes 3145736 | tf_op jit(solution)/shard_map/ppermute | solution.py:455
  82.2 16.9 %collective-permute-start.16 = (bf16[2,256,512]{2,1,0:T(8,128)(2,1)S(1)}, bf16[2,256,512]{2,1,0:T(8,128)(2,1)S(1)}, u32[]{:S(2)}, u32[]{:S(2)}) collective-permute-start(bf16[2,256,512]{2,1,0:T(8,128)(2,1)S(1)} %add_convert_fusion.1), channel_id=1, source_target_pairs={{8,16},{12,20},{16,8},{20,12},{9,17},{13,21},{17,9},{21,13},{10,18... | collective-permute-start | bytes 1572872 | tf_op jit(solution)/shard_map/ppermute | solution.py:436
  97.4 15.0 %collective-permute-start.13 = (bf16[2,256,512]{2,1,0:T(8,128)(2,1)S(1)}, bf16[2,256,512]{2,1,0:T(8,128)(2,1)S(1)}, u32[]{:S(2)}, u32[]{:S(2)}) collective-permute-start(bf16[2,256,512]{2,1,0:T(8,128)(2,1)S(1)} %add_convert_fusion.2), channel_id=1, source_target_pairs={{8,16},{12,20},{16,8},{20,12},{9,17},{13,21},{17,9},{21,13},{10,18... | collective-permute-start | bytes 1572872 | tf_op jit(solution)/shard_map/ppermute | solution.py:436
  98.3 16.8 %collective-permute-start.9 = (bf16[2,256,512]{2,1,0:T(8,128)(2,1)S(1)}, bf16[2,256,512]{2,1,0:T(8,128)(2,1)S(1)}, u32[]{:S(2)}, u32[]{:S(2)}) collective-permute-start(bf16[2,256,512]{2,1,0:T(8,128)(2,1)S(1)} %add_convert_fusion.3), channel_id=1, source_target_pairs={{8,16},{12,20},{16,8},{20,12},{9,17},{13,21},{17,9},{21,13},{10,18... | collective-permute-start | bytes 1572872 | tf_op jit(solution)/shard_map/ppermute | solution.py:436
  99.1 29.2 %collective-permute-start.23 = (bf16[2,256,512]{2,1,0:T(8,128)(2,1)S(1)}, bf16[2,256,512]{2,1,0:T(8,128)(2,1)S(1)}, u32[]{:S(2)}, u32[]{:S(2)}) collective-permute-start(bf16[2,256,512]{2,1,0:T(8,128)(2,1)S(1)} %add_convert_fusion), channel_id=1, source_target_pairs={{8,16},{12,20},{16,8},{20,12},{9,17},{13,21},{17,9},{21,13},{10,18... | collective-permute-start | bytes 1572872 | tf_op jit(solution)/shard_map/ppermute | solution.py:436
  105.6 51.1 %collective-permute-start.17 = (bf16[1,256,512]{2,1,0:T(8,128)(2,1)S(1)}, bf16[1,256,512]{2,1,0:T(8,128)(2,1)S(1)}, u32[]{:S(2)}, u32[]{:S(2)}) collective-permute-start(bf16[1,256,512]{2,1,0:T(8,128)(2,1)S(1)} %add_convert_fusion.5), channel_id=1, source_target_pairs={{0,8},{4,12},{8,0},{12,4},{16,24},{20,28},{24,16},{28,20},{1,9},{5... | collective-permute-start | bytes 786440 | tf_op jit(solution)/shard_map/ppermute | solution.py:436
  112.5 69.5 %collective-permute-start.32 = (bf16[2,256,1024]{2,1,0:T(8,128)(2,1)S(1)}, bf16[2,256,1024]{2,1,0:T(8,128)(2,1)S(1)}, u32[]{:S(2)}, u32[]{:S(2)}) collective-permute-start(bf16[2,256,1024]{2,1,0:T(8,128)(2,1)S(1)} %add.52.refs_11_), channel_id=1, source_target_pairs={{4,0},{0,4},{12,8},{8,12},{20,16},{16,20},{28,24},{24,28},{5,1},{1... | collective-permute-start | bytes 3145736 | tf_op jit(solution)/shard_map/ppermute | solution.py:471
  115.1 45.9 %collective-permute-start.14 = (bf16[1,256,512]{2,1,0:T(8,128)(2,1)S(1)}, bf16[1,256,512]{2,1,0:T(8,128)(2,1)S(1)}, u32[]{:S(2)}, u32[]{:S(2)}) collective-permute-start(bf16[1,256,512]{2,1,0:T(8,128)(2,1)S(1)} %add_convert_fusion.6), channel_id=1, source_target_pairs={{0,8},{4,12},{8,0},{12,4},{16,24},{20,28},{24,16},{28,20},{1,9},{5... | collective-permute-start | bytes 786440 | tf_op jit(solution)/shard_map/ppermute | solution.py:436
  128.4 35.3 %collective-permute-start.10 = (bf16[1,256,512]{2,1,0:T(8,128)(2,1)S(1)}, bf16[1,256,512]{2,1,0:T(8,128)(2,1)S(1)}, u32[]{:S(2)}, u32[]{:S(2)}) collective-permute-start(bf16[1,256,512]{2,1,0:T(8,128)(2,1)S(1)} %add_convert_fusion.7), channel_id=1, source_target_pairs={{0,8},{4,12},{8,0},{12,4},{16,24},{20,28},{24,16},{28,20},{1,9},{5... | collective-permute-start | bytes 786440 | tf_op jit(solution)/shard_map/ppermute | solution.py:436
  148.4 8.4 %copy-start.1 = (f32[256,512]{1,0:T(8,128)S(1)}, f32[256,512]{1,0:T(8,128)}, u32[]{:S(2)}) copy-start(f32[256,512]{1,0:T(8,128)} %copy-done) | copy-start | bytes 1572868
  148.4 8.4 %copy-start.5 = (f32[512]{0:T(512)S(1)}, f32[512]{0:T(512)}, u32[]{:S(2)}) copy-start(f32[512]{0:T(512)} %param.20) | copy-start | bytes 6148
  148.4 8.4 %copy-start.6 = (f32[512]{0:T(512)S(1)}, f32[512]{0:T(512)}, u32[]{:S(2)}) copy-start(f32[512]{0:T(512)} %param.21) | copy-start | bytes 6148
  156.7 15.4 %collective-permute-start.24 = (bf16[1,256,512]{2,1,0:T(8,128)(2,1)S(1)}, bf16[1,256,512]{2,1,0:T(8,128)(2,1)S(1)}, u32[]{:S(2)}, u32[]{:S(2)}) collective-permute-start(bf16[1,256,512]{2,1,0:T(8,128)(2,1)S(1)} %add_convert_fusion.4), channel_id=1, source_target_pairs={{0,8},{4,12},{8,0},{12,4},{16,24},{20,28},{24,16},{28,20},{1,9},{5... | collective-permute-start | bytes 786440 | tf_op jit(solution)/shard_map/ppermute | solution.py:436
  156.8 4.1 %copy-start.3 = (f32[256,512]{1,0:T(8,128)S(1)}, f32[256,512]{1,0:T(8,128)}, u32[]{:S(2)}) copy-start(f32[256,512]{1,0:T(8,128)} %copy-done.2) | copy-start | bytes 1572868
  161.0 21.0 %copy-start.7 = (s32[4,4]{1,0:T(4,128)S(1)}, s32[4,4]{1,0:T(4,128)}, u32[]{:S(2)}) copy-start(s32[4,4]{1,0:T(4,128)} %constant.54.clone.refs_0_) | copy-start | bytes 196
  166.4 5.7 %collective-permute-start.18 = (bf16[256,384]{1,0:T(8,128)(2,1)S(1)}, bf16[256,384]{1,0:T(8,128)(2,1)S(1)}, u32[]{:S(2)}, u32[]{:S(2)}) collective-permute-start(bf16[256,384]{1,0:T(8,128)(2,1)S(1)} %recur.6.refs_1_), channel_id=1, source_target_pairs={{0,2},{1,3},{2,0},{3,1},{4,6},{5,7},{6,4},{7,5},{8,10},{9,11},{10,... | collective-permute-start | bytes 589832 | tf_op jit(solution)/shard_map/ppermute | solution.py:343
  167.9 14.0 %collective-permute-start.19 = (bf16[256,384]{1,0:T(8,128)(2,1)S(1)}, bf16[256,384]{1,0:T(8,128)(2,1)S(1)}, u32[]{:S(2)}, u32[]{:S(2)}) collective-permute-start(bf16[256,384]{1,0:T(8,128)(2,1)S(1)} %recur.6.refs_1_), channel_id=1, source_target_pairs={{0,1},{1,0},{2,3},{3,2},{4,5},{5,4},{6,7},{7,6},{8,9},{9,8},{10,11... | collective-permute-start | bytes 589832 | tf_op jit(solution)/shard_map/ppermute | solution.py:343
  172.1 9.8 %collective-permute-start.20 = (bf16[256,384]{1,0:T(8,128)(2,1)S(1)}, bf16[256,384]{1,0:T(8,128)(2,1)S(1)}, u32[]{:S(2)}, u32[]{:S(2)}) collective-permute-start(bf16[256,384]{1,0:T(8,128)(2,1)S(1)} %collective-permute-done.18.refs_2_), channel_id=1, source_target_pairs={{0,1},{1,0},{2,3},{3,2},{4,5},{5,4},{6,7},{7,6},{8,9},{9,8},{10,11... | collective-permute-start | bytes 589832 | tf_op jit(solution)/shard_map/ppermute | solution.py:343
  173.0 4.6 %collective-permute-start.25 = (bf16[256,128]{1,0:T(8,128)(2,1)S(1)}, bf16[256,128]{1,0:T(8,128)(2,1)S(1)}, u32[]{:S(2)}, u32[]{:S(2)}) collective-permute-start(bf16[256,128]{1,0:T(8,128)(2,1)S(1)} %recur.7.refs_5_), channel_id=1, source_target_pairs={{0,2},{1,3},{2,0},{3,1},{4,6},{5,7},{6,4},{7,5},{8,10},{9,11},{10,... | collective-permute-start | bytes 196616 | tf_op jit(solution)/shard_map/ppermute | solution.py:343
  174.5 3.8 %collective-permute-start.26 = (bf16[256,128]{1,0:T(8,128)(2,1)S(1)}, bf16[256,128]{1,0:T(8,128)(2,1)S(1)}, u32[]{:S(2)}, u32[]{:S(2)}) collective-permute-start(bf16[256,128]{1,0:T(8,128)(2,1)S(1)} %recur.7.refs_5_), channel_id=1, source_target_pairs={{0,1},{1,0},{2,3},{3,2},{4,5},{5,4},{6,7},{7,6},{8,9},{9,8},{10,11... | collective-permute-start | bytes 196616 | tf_op jit(solution)/shard_map/ppermute | solution.py:343
  177.5 4.4 %collective-permute-start.27 = (bf16[256,128]{1,0:T(8,128)(2,1)S(1)}, bf16[256,128]{1,0:T(8,128)(2,1)S(1)}, u32[]{:S(2)}, u32[]{:S(2)}) collective-permute-start(bf16[256,128]{1,0:T(8,128)(2,1)S(1)} %recur.7.refs_5_), channel_id=1, source_target_pairs={{0,3},{1,2},{2,1},{3,0},{4,7},{5,6},{6,5},{7,4},{8,11},{9,10},{10,... | collective-permute-start | bytes 196616 | tf_op jit(solution)/shard_map/ppermute | solution.py:343
